TPU v7x, 32 devices: a whole 2x2x4 slice. The times are simulated.
32 devices in a mesh: sp: 4 (over z), tp: 8 (over y, x, core).
Axes of the slice: x: 2, y: 2, z: 4, core: 2. Of those that a mesh axis runs over, the one named last changes fastest.
Arguments:
- target_rows: bfloat16 [768, 2048], P(('sp', 'tp')), may hold values from -6 to 6
- source_rows: bfloat16 [4096, 2048], P(('sp', 'tp')), may hold values from -6 to 6
- target_gain: float32 [2048], replicated, may hold values from 0.55 to 9
- source_gain: float32 [2048], replicated, may hold values from 0.55 to 9
- query_weight: bfloat16 [2048, 2048], P(None, 'tp'), may hold values from -0.125 to 0.125
- key_weight: bfloat16 [2048, 512], P('tp'), may hold values from -0.125 to 0.125
- value_weight: bfloat16 [2048, 512], P('tp'), may hold values from -0.125 to 0.125
- out_weight: bfloat16 [2048, 2048], P('tp'), may hold values from -0.125 to 0.125
- out_cotangent: bfloat16 [768, 2048], P(('sp', 'tp')), may hold values from -6 to 6
Outputs:
- target_grad: float32 [768, 2048], P(('sp', 'tp'))
- source_grad: float32 [4096, 2048], P(('sp', 'tp'))
- out_weight_grad: float32 [2048, 2048], P('tp')
All inputs are finite; a program needn't handle non-finite values.
Results may differ from a plain program's by a relative error of at most 0.03.
Values may be sent and summed in bfloat16 or wider, within the bound.
No kernel may reach another device: no remote copies, remote signals or barrier semaphores. Data moves between devices by JAX's collectives and lax.ppermute only.
A program may use at most 64 MiB of HBM per device.

v0:
```python
import jax
import jax.numpy as jnp
from jax import lax
from jax.experimental import pallas as pl
from jax.experimental.pallas import tpu as pltpu
from jax.sharding import PartitionSpec as P


HEAD_DIM = 64
KV_HEADS = 8
EPSILON = 1e-06
SCALE = HEAD_DIM**-0.5


F32 = jnp.float32
BF16 = jnp.bfloat16


def shape_of(shape, dtype):
    return jax.ShapeDtypeStruct(shape, dtype)


def normalize(matrix, gain_vector):
    widened = matrix.astype(F32)
    factor = lax.rsqrt(jnp.mean(widened * widened, axis=-1, keepdims=True) + EPSILON)
    return (widened * factor * gain_vector).astype(BF16)


def norm_back(matrix, gain_vector, upstream):
    widened = matrix.astype(F32)
    factor = lax.rsqrt(jnp.mean(widened * widened, axis=-1, keepdims=True) + EPSILON)
    weighted = upstream * gain_vector
    inner_sum = jnp.mean(weighted * widened, axis=-1, keepdims=True)
    return factor * weighted - widened * factor**3 * inner_sum


def swap(array, axis, mask):
    size = lax.axis_size(axis)
    return lax.ppermute(array, axis, [(i, i ^ mask) for i in range(size)])


def doubling(array, axis, bits):
    blocks = {0: array}
    for bit in bits:
        received = {key ^ bit: swap(value, axis, bit) for key, value in blocks.items()}
        blocks.update(received)
    return blocks


def dot(a, b):
    return jnp.dot(a, b, preferred_element_type=F32)


def nt_dot(a, b):
    return lax.dot_general(a, b, (((1,), (1,)), ((), ())), preferred_element_type=F32)


def tn_dot(a, b):
    return lax.dot_general(a, b, (((0,), (0,)), ((), ())), preferred_element_type=F32)


def chunk_for(rows):
    return 256 if rows % 256 == 0 else rows


def pad_to(extent, multiple):
    return -(-extent // multiple) * multiple


def transposed(matrix):
    rows, columns = matrix.shape
    more_rows, more_columns = pad_to(rows, 128) - rows, pad_to(columns, 128) - columns
    if more_columns:
        matrix = jnp.concatenate([matrix, jnp.zeros((rows, more_columns), F32)], axis=1)
    if more_rows:
        filler = jnp.zeros((more_rows, columns + more_columns), F32)
        matrix = jnp.concatenate([matrix, filler], axis=0)
    return matrix.T[:columns, :rows]


def stacked(matrix):
    heads = matrix.shape[0] // HEAD_DIM
    pieces = [matrix[g * HEAD_DIM : (g + 1) * HEAD_DIM, :] for g in range(heads)]
    return jnp.concatenate(pieces, axis=1) if heads > 1 else pieces[0]


def unstacked(matrix, heads):
    rows = matrix.shape[1] // heads
    pieces = [matrix[:, g * rows : (g + 1) * rows] for g in range(heads)]
    return jnp.concatenate(pieces, axis=0) if heads > 1 else pieces[0]


SCALAR = pl.BlockSpec(memory_space=pltpu.SMEM)
WHOLE = pl.BlockSpec(memory_space=pltpu.VMEM)


def split_norm(tp_at, source_rows, gain, weight_rows, tp_count):
    rows, width = source_rows.shape
    half = width // 2
    masks = range(0, tp_count, 2)
    if weight_rows % 128:
        normed = normalize(source_rows, gain)

        def columns(parity):
            return jnp.concatenate(
                [
                    lax.dynamic_slice_in_dim(
                        normed, (tp_at ^ m ^ parity) * weight_rows, weight_rows, 1
                    )
                    for m in masks
                ],
                axis=1,
            )

        return columns(0), columns(1)

    def kernel(at_ref, rows_ref, gain_ref, own_ref, other_ref):
        widened = rows_ref[...].astype(F32)
        factor = lax.rsqrt(jnp.mean(widened * widened, axis=-1, keepdims=True) + EPSILON)
        for parity, out_ref in ((0, own_ref), (1, other_ref)):
            for place, m in enumerate(masks):
                start = pl.multiple_of((at_ref[0] ^ (m + parity)) * weight_rows, 128)
                at = pl.ds(start, weight_rows)
                piece = rows_ref[:, at].astype(F32) * factor * gain_ref[:, at]
                out_ref[:, place * weight_rows : (place + 1) * weight_rows] = piece.astype(BF16)

    return pl.pallas_call(
        kernel,
        out_shape=(shape_of((rows, half), BF16), shape_of((rows, half), BF16)),
        in_specs=[SCALAR, WHOLE, WHOLE],
        cost_estimate=pl.CostEstimate(flops=8 * rows * width, bytes_accessed=4 * rows * width, transcendentals=0),
        name="split_norm",
    )(tp_at[None], source_rows, gain[None])


def project_kv(own, other, key_blocks, value_blocks):
    rows = own.shape[0]
    count = len(key_blocks)
    weight_rows, kv_width = key_blocks[0].shape

    def kernel(own_ref, other_ref, *refs):
        keys, values = refs[:count], refs[count : 2 * count]
        near_ref, far_ref = refs[-2:]
        lhs = jnp.concatenate([own_ref[...], other_ref[...]], axis=0)
        sums = []
        for weights in (keys, values):
            total = None
            for place, weight in enumerate(weights):
                term = dot(lhs[:, place * weight_rows : (place + 1) * weight_rows], weight[...])
                total = term if total is None else total + term
            sums.append(total)
        for head in range(KV_HEADS):
            at = slice(head * HEAD_DIM, (head + 1) * HEAD_DIM)
            packed = jnp.concatenate([sums[0][:, at], sums[1][:, at]], axis=1)
            near_ref[head] = packed[:rows]
            far_ref[head] = packed[rows:]

    return pl.pallas_call(
        kernel,
        out_shape=(shape_of((KV_HEADS, rows, 2 * HEAD_DIM), F32),) * 2,
        cost_estimate=pl.CostEstimate(
            flops=8 * rows * count * weight_rows * kv_width,
            bytes_accessed=4 * count * weight_rows * kv_width,
            transcendentals=0,
        ),
        name="project_kv",
    )(own, other, *key_blocks, *value_blocks)


def project_queries(pieces, query_weight):
    count = sum(piece.shape[0] for piece in pieces)
    heads = query_weight.shape[1] // HEAD_DIM

    def kernel(*refs):
        piece_refs, weight_ref, out_ref = refs[:-2], refs[-2], refs[-1]
        rows = jnp.concatenate([ref[...] for ref in piece_refs], axis=0)
        queries = dot(rows, weight_ref[...])
        out_ref[...] = stacked(transposed(queries)).astype(BF16) * jnp.asarray(SCALE, BF16)

    return pl.pallas_call(
        kernel,
        out_shape=shape_of((HEAD_DIM, heads * count), BF16),
        cost_estimate=pl.CostEstimate(
            flops=2 * count * query_weight.size, bytes_accessed=2 * query_weight.size, transcendentals=0
        ),
        name="project_queries",
    )(*pieces, query_weight)


def project_grads(pieces, out_weight):
    blocks, piece_rows, width = pieces[0].shape
    count = piece_rows * len(pieces)
    heads = out_weight.shape[0] // HEAD_DIM

    def kernel(*refs):
        piece_refs, weight_ref, out_ref, cot_ref = refs[:-3], refs[-3], refs[-2], refs[-1]
        for block in range(blocks):
            rows = jnp.concatenate([ref[block] for ref in piece_refs], axis=0)
            cot_ref[block * count : (block + 1) * count, :] = rows
            out_ref[block] = stacked(nt_dot(weight_ref[...], rows)).astype(BF16)

    return pl.pallas_call(
        kernel,
        out_shape=(
            shape_of((blocks, HEAD_DIM, heads * count), BF16),
            shape_of((blocks * count, width), BF16),
        ),
        cost_estimate=pl.CostEstimate(
            flops=2 * blocks * count * out_weight.size, bytes_accessed=2 * blocks * count * width, transcendentals=0
        ),
        name="project_grads",
    )(*pieces, out_weight)


def forward_all(queries, grads, kv):
    blocks = len(queries)
    lanes = queries[0].shape[1]
    rows = kv.shape[0]
    chunk = chunk_for(rows)

    def kernel(*refs):
        query_refs, (grad_ref, kv_ref) = refs[:blocks], refs[blocks : blocks + 2]
        out_ref, stat_ref, score_ref = refs[blocks + 2 :]
        zeros = jnp.zeros((HEAD_DIM, lanes), BF16)
        for block, query_ref in enumerate(query_refs):
            query = jnp.concatenate([query_ref[...], zeros], axis=0)
            slot = block % 2
            peak = jnp.full((8, lanes), -jnp.inf, F32)
            for start in range(0, rows, chunk):
                scores = dot(kv_ref[start : start + chunk, :], query)
                score_ref[slot, start : start + chunk, :] = scores
                peak = jnp.maximum(peak, jnp.max(scores.reshape(chunk // 8, 8, lanes), axis=0))
            row_max = jnp.max(peak, axis=0, keepdims=True)
            total = jnp.zeros((8, lanes), F32)
            summed = jnp.zeros((HEAD_DIM, lanes), F32)
            for start in range(0, rows, chunk):
                weights = jnp.exp(score_ref[slot, start : start + chunk, :] - row_max)
                total = total + jnp.sum(weights.reshape(chunk // 8, 8, lanes), axis=0)
                values = kv_ref[start : start + chunk, HEAD_DIM:]
                summed = summed + tn_dot(values, weights.astype(BF16))
            total = jnp.sum(total, axis=0, keepdims=True)
            part = summed / total
            out_ref[block] = part
            stat_ref[2 * block : 2 * block + 1, :] = row_max + jnp.log(total)
            stat_ref[2 * block + 1 : 2 * block + 2, :] = jnp.sum(
                grad_ref[block].astype(F32) * part, axis=0, keepdims=True
            )

    return pl.pallas_call(
        kernel,
        out_shape=(
            shape_of((blocks, HEAD_DIM, lanes), F32),
            shape_of((2 * blocks, lanes), F32),
        ),
        scratch_shapes=[pltpu.VMEM((2, rows, lanes), F32)],
        cost_estimate=pl.CostEstimate(
            flops=8 * blocks * rows * lanes * HEAD_DIM,
            bytes_accessed=4 * blocks * rows * HEAD_DIM,
            transcendentals=blocks * rows * lanes,
        ),
        name="forward_all",
    )(*queries, grads, kv)


def combine_stats(stats, parts):
    blocks, _, lanes = parts.shape

    def kernel(*refs):
        stat_refs, part_ref, out_ref, share_ref = refs[:blocks], refs[blocks], refs[-2], refs[-1]
        for block in range(blocks):
            logs, deltas = [], []
            for peer, stat_ref in enumerate(stat_refs):
                at = 2 * (block ^ peer)
                logs.append(stat_ref[at : at + 1, :])
                deltas.append(stat_ref[at + 1 : at + 2, :])
            peak = logs[0]
            for log in logs[1:]:
                peak = jnp.maximum(peak, log)
            shares = [jnp.exp(log - peak) for log in logs]
            total = shares[0]
            delta = shares[0] * deltas[0]
            for share, term in zip(shares[1:], deltas[1:]):
                total = total + share
                delta = delta + share * term
            out_ref[2 * block : 2 * block + 1, :] = peak + jnp.log(total)
            out_ref[2 * block + 1 : 2 * block + 2, :] = delta / total
            share_ref[block] = (part_ref[block] * (shares[0] / total)).astype(BF16)

    return pl.pallas_call(
        kernel,
        out_shape=(
            shape_of((2 * blocks, lanes), F32),
            shape_of((blocks, HEAD_DIM, lanes), BF16),
        ),
        name="combine_stats",
    )(*stats, parts)


def backward_some(order, queries, grads, stats, kv, sums, sum_type):
    count = len(order)
    lanes = queries[0].shape[1]
    rows = kv.shape[0]
    chunk = chunk_for(rows)
    started = [] if sums is None else [sums]

    def kernel(*refs):
        query_refs = refs[:count]
        grad_ref, stat_ref, kv_ref = refs[count : count + 3]
        start_refs = refs[count + 3 : count + 3 + len(started)]
        outs = refs[count + 3 + len(started) : -1]
        sum_ref = refs[-1]
        zeros = jnp.zeros((HEAD_DIM, lanes), BF16)
        for place, block in enumerate(order):
            query = jnp.concatenate([query_refs[place][...], zeros], axis=0)
            grad = jnp.concatenate([zeros, grad_ref[block]], axis=0)
            log_total = stat_ref[2 * block : 2 * block + 1, :]
            delta = stat_ref[2 * block + 1 : 2 * block + 2, :]
            d_query = jnp.zeros((HEAD_DIM, lanes), F32)
            for start in range(0, rows, chunk):
                at = slice(start, start + chunk)
                pair = kv_ref[at, :]
                probs = jnp.exp(dot(pair, query) - log_total)
                d_scores = (probs * (dot(pair, grad) - delta)).astype(BF16)
                terms = nt_dot(d_scores, query) + nt_dot(probs.astype(BF16), grad)
                if place:
                    terms = terms + sum_ref[at, :]
                elif started:
                    terms = terms + start_refs[0][at, :]
                sum_ref[at, :] = terms
                d_query = d_query + tn_dot(pair[:, :HEAD_DIM], d_scores)
            outs[place][...] = (d_query * SCALE).astype(BF16)
        outs[-1][...] = sum_ref[...].astype(sum_type)

    outs = pl.pallas_call(
        kernel,
        out_shape=tuple(shape_of((HEAD_DIM, lanes), BF16) for _ in order)
        + (shape_of((rows, 2 * HEAD_DIM), sum_type),),
        scratch_shapes=[pltpu.VMEM((rows, 2 * HEAD_DIM), F32)],
        cost_estimate=pl.CostEstimate(
            flops=20 * count * rows * lanes * HEAD_DIM,
            bytes_accessed=8 * count * rows * HEAD_DIM,
            transcendentals=count * rows * lanes,
        ),
        name="backward_some",
    )(*[queries[block] for block in order], grads, stats, kv, *started)
    return outs[:-1], outs[-1]


def query_back(parts, query_weight, heads):
    width = query_weight.shape[0]
    count = parts[0].shape[1] // heads
    half = count // 2

    def kernel(*refs):
        part_refs, weight_ref, own_ref, other_ref = refs[:-3], refs[-3], refs[-2], refs[-1]
        total = part_refs[0][...].astype(F32)
        for part_ref in part_refs[1:]:
            total = total + part_ref[...].astype(F32)
        grad = transposed(unstacked(total, heads)).astype(BF16)
        upstream = nt_dot(grad, weight_ref[...])
        own_ref[...] = upstream[:half]
        other_ref[...] = upstream[half:].astype(BF16)

    return pl.pallas_call(
        kernel,
        out_shape=(shape_of((half, width), F32), shape_of((half, width), BF16)),
        cost_estimate=pl.CostEstimate(
            flops=2 * count * query_weight.size, bytes_accessed=2 * query_weight.size, transcendentals=0
        ),
        name="query_back",
    )(*parts, query_weight)


def share_rows(own, theirs, count):
    rows, width = own.shape
    piece = rows // count

    def kernel(own_ref, theirs_ref, kept_ref, *out_refs):
        kept_ref[...] = own_ref[:piece, :] + theirs_ref[:piece, :].astype(F32)
        for place, out_ref in enumerate(out_refs):
            at = slice((place + 1) * piece, (place + 2) * piece)
            out_ref[...] = (own_ref[at, :] + theirs_ref[at, :].astype(F32)).astype(BF16)

    return pl.pallas_call(
        kernel,
        out_shape=(shape_of((piece, width), F32),)
        + tuple(shape_of((piece, width), BF16) for _ in range(count - 1)),
        name="share_rows",
    )(own, theirs)


def target_finish(kept, received, target_rows, cotangent, gain):
    def kernel(kept_ref, *refs):
        received_refs, (rows_ref, cot_ref, gain_ref, out_ref) = refs[:-4], refs[-4:]
        total = kept_ref[...]
        for ref in received_refs:
            total = total + ref[...].astype(F32)
        back = norm_back(rows_ref[...], gain_ref[...], total)
        out_ref[...] = cot_ref[...].astype(F32) + back

    return pl.pallas_call(
        kernel,
        out_shape=shape_of(kept.shape, F32),
        name="target_finish",
    )(kept, *received, target_rows, cotangent, gain[None])


def attend_sum(parts):
    def kernel(*refs):
        own_ref, out_ref = refs[0], refs[-1]
        total = own_ref[0].astype(F32)
        for ref in refs[1:-1]:
            total = total + ref[...].astype(F32)
        out_ref[...] = total.astype(BF16)

    return pl.pallas_call(
        kernel, out_shape=shape_of(parts[0].shape[1:], BF16), name="attend_sum"
    )(*parts)


def weight_grad(attended, cot_all, heads):
    blocks = len(attended)
    count = cot_all.shape[0] // blocks
    width = cot_all.shape[1]
    step = 512 if width % 512 == 0 else width

    def kernel(*refs):
        attended_refs, cot_ref, out_ref, wide_ref = refs[:blocks], refs[-3], refs[-2], refs[-1]

        @pl.when(pl.program_id(0) == 0)
        def _():
            for block, attended_ref in enumerate(attended_refs):
                wide_ref[block] = unstacked(attended_ref[...].astype(F32), heads).astype(BF16)

        total = None
        for block in range(blocks):
            term = dot(wide_ref[block], cot_ref[block * count : (block + 1) * count, :])
            total = term if total is None else total + term
        out_ref[...] = total

    part_spec = pl.BlockSpec(attended[0].shape, lambda i: (0, 0))
    return pl.pallas_call(
        kernel,
        grid=(width // step,),
        in_specs=[part_spec] * blocks + [pl.BlockSpec((cot_all.shape[0], step), lambda i: (0, i))],
        out_specs=pl.BlockSpec((heads * HEAD_DIM, step), lambda i: (0, i)),
        out_shape=shape_of((heads * HEAD_DIM, width), F32),
        scratch_shapes=[pltpu.VMEM((blocks, heads * HEAD_DIM, count), BF16)],
        cost_estimate=pl.CostEstimate(
            flops=2 * heads * HEAD_DIM * cot_all.size, bytes_accessed=2 * cot_all.size, transcendentals=0
        ),
        name="weight_grad",
    )(*attended, cot_all)


def source_back(tp_at, back, key_blocks, value_blocks, others, source_rows, gain):
    rows, width = source_rows.shape
    count = len(key_blocks)
    weight_rows = key_blocks[0].shape[0]

    def kernel(at_ref, back_ref, *refs):
        keys, values = refs[:count], refs[count : 2 * count]
        other_ref, rows_ref, gain_ref, out_ref = refs[2 * count :]
        key_grad = jnp.concatenate([back_ref[h][:, :HEAD_DIM] for h in range(KV_HEADS)], axis=1)
        value_grad = jnp.concatenate([back_ref[h][:, HEAD_DIM:] for h in range(KV_HEADS)], axis=1)
        inner = jnp.zeros((rows, 1), F32)
        square = jnp.zeros((rows, 1), F32)
        for place in range(count):
            for parity in (0, 1):
                if parity:
                    key, value = other_ref[0, place], other_ref[1, place]
                else:
                    key, value = keys[place][...], values[place][...]
                start = pl.multiple_of((at_ref[0] ^ (2 * place + parity)) * weight_rows, 128)
                at = pl.ds(start, weight_rows)
                weighted = (nt_dot(key_grad, key) + nt_dot(value_grad, value)) * gain_ref[:, at]
                widened = rows_ref[:, at].astype(F32)
                inner = inner + jnp.sum(weighted * widened, axis=-1, keepdims=True)
                square = square + jnp.sum(widened * widened, axis=-1, keepdims=True)
                out_ref[:, at] = weighted
        factor = lax.rsqrt(square / width + EPSILON)
        pull = factor**3 * (inner / width)
        out_ref[...] = factor * out_ref[...] - rows_ref[...].astype(F32) * pull

    return pl.pallas_call(
        kernel,
        out_shape=shape_of((rows, width), F32),
        in_specs=[SCALAR] + [WHOLE] * (2 * count + 4),
        cost_estimate=pl.CostEstimate(
            flops=4 * rows * width * KV_HEADS * HEAD_DIM,
            bytes_accessed=4 * width * KV_HEADS * HEAD_DIM,
            transcendentals=0,
        ),
        name="source_back",
    )(tp_at[None], back, *key_blocks, *value_blocks, others, source_rows, gain[None])


def source_back_plain(tp_at, back, key_blocks, value_blocks, others, source_rows, gain):
    rows, width = source_rows.shape
    weight_rows = key_blocks[0].shape[0]
    total = jnp.zeros((rows, width), F32)
    fulls = []
    for kind, blocks in enumerate((key_blocks, value_blocks)):
        full = jnp.zeros((width, KV_HEADS * HEAD_DIM), BF16)
        for place, block in enumerate(blocks):
            start = (tp_at ^ (2 * place)) * weight_rows
            full = lax.dynamic_update_slice_in_dim(full, block, start, 0)
            start = (tp_at ^ (2 * place + 1)) * weight_rows
            full = lax.dynamic_update_slice_in_dim(full, others[kind, place], start, 0)
        fulls.append(full)
    turned = back.transpose(1, 0, 2)
    key_grad = turned[:, :, :HEAD_DIM].reshape(rows, KV_HEADS * HEAD_DIM)
    value_grad = turned[:, :, HEAD_DIM:].reshape(rows, KV_HEADS * HEAD_DIM)
    total = nt_dot(key_grad, fulls[0]) + nt_dot(value_grad, fulls[1])
    return norm_back(source_rows, gain, total)


def body(
    target_rows,
    source_rows,
    target_gain,
    source_gain,
    query_weight,
    key_weight,
    value_weight,
    out_weight,
    out_cotangent,
):
    tp_count = lax.axis_size("tp")
    sp_count = lax.axis_size("sp")
    tp_at = lax.axis_index("tp").astype(jnp.int32)
    own_source = source_rows.shape[0]
    weight_rows = key_weight.shape[0]
    heads = query_weight.shape[1] // HEAD_DIM
    copies = max(1, tp_count // KV_HEADS)
    chips = tp_count // 2
    chip_bits = [1 << b for b in range(1, tp_count.bit_length() - 1)]
    near, far = chip_bits[: len(chip_bits) // 2], chip_bits[len(chip_bits) // 2 :]
    chip_masks = range(0, tp_count, 2)

    normed_t = normalize(target_rows, target_gain)
    near_rows = [normed_t if m == 0 else swap(normed_t, "tp", m) for m in chip_masks]
    far_rows = [swap(rows, "tp", 1) for rows in near_rows]
    queries = project_queries(near_rows + far_rows, query_weight)
    all_queries = [queries if k == 0 else swap(queries, "sp", k) for k in range(sp_count)]

    key_found = doubling(key_weight, "tp", far + near)
    value_found = doubling(value_weight, "tp", near + far)
    key_blocks = [key_found[m] for m in chip_masks]
    value_blocks = [value_found[m] for m in chip_masks]

    own_part, other_part = split_norm(tp_at, source_rows, source_gain, weight_rows, tp_count)
    other_part = swap(other_part, "tp", 1)
    own_sum, other_sum = project_kv(own_part, other_part, key_blocks, value_blocks)
    packed = (own_sum + swap(other_sum, "tp", 1)).astype(BF16)
    packed = jnp.repeat(packed, copies, axis=0)
    kv = lax.all_to_all(packed, "tp", split_axis=0, concat_axis=0, tiled=True)
    kv = kv.reshape(tp_count * own_source, 2 * HEAD_DIM)

    cot_z = jnp.stack(
        [out_cotangent if k == 0 else swap(out_cotangent, "sp", k) for k in range(sp_count)]
    )
    cot_near = [cot_z if m == 0 else swap(cot_z, "tp", m) for m in chip_masks]
    cot_far = [swap(rows, "tp", 1) for rows in cot_near]
    all_grads, cot_all = project_grads(cot_near + cot_far, out_weight)

    parts, own_stats = forward_all(all_queries, all_grads, kv)
    stats = [own_stats if k == 0 else swap(own_stats, "sp", k) for k in range(sp_count)]
    stats, shares = combine_stats(stats, parts)
    order = list(range(sp_count // 2, sp_count)) + list(range(sp_count // 2 - 1, -1, -1))
    first, second = order[: sp_count // 2], order[sp_count // 2 :]
    found, kv_sums = backward_some(first, all_queries, all_grads, stats, kv, None, F32)
    query_parts = [swap(part, "sp", k) for k, part in zip(first, found)]
    found, kv_sums = backward_some(second, all_queries, all_grads, stats, kv, kv_sums, BF16)
    query_parts += [part if k == 0 else swap(part, "sp", k) for k, part in zip(second, found)]

    others = jnp.stack([jnp.stack(key_blocks), jnp.stack(value_blocks)])
    others = swap(others, "tp", 1)
    back = lax.all_to_all(
        kv_sums.reshape(tp_count, own_source, 2 * HEAD_DIM),
        "tp",
        split_axis=0,
        concat_axis=0,
        tiled=True,
    )
    if copies > 1:
        back = back.reshape(KV_HEADS, copies, own_source, 2 * HEAD_DIM)
        back = back.astype(F32).sum(1).astype(BF16)
    finish = source_back_plain if weight_rows % 128 else source_back
    source_grad = finish(tp_at, back, key_blocks, value_blocks, others, source_rows, source_gain)

    mine, theirs = query_back(query_parts, query_weight, heads)
    theirs = swap(theirs, "tp", 1)
    kept, *given = share_rows(mine, theirs, chips)
    received = [swap(piece, "tp", m) for m, piece in zip(list(chip_masks)[1:], given)]
    target_grad = target_finish(kept, received, target_rows, out_cotangent, target_gain)

    attended = [shares] + [swap(shares[k], "sp", k) for k in range(1, sp_count)]
    attended = attend_sum(attended)
    attended = [attended if k == 0 else swap(attended, "sp", k) for k in range(sp_count)]
    out_weight_grad = weight_grad(attended, cot_all, heads)
    return (target_grad, source_grad, out_weight_grad)


def solution(mesh):
    return jax.shard_map(
        body,
        mesh=mesh,
        in_specs=(
            P(("sp", "tp"), None),
            P(("sp", "tp"), None),
            P(),
            P(),
            P(None, "tp"),
            P("tp", None),
            P("tp", None),
            P("tp", None),
            P(("sp", "tp"), None),
        ),
        out_specs=(P(("sp", "tp"), None), P(("sp", "tp"), None), P("tp", None)),
        check_vma=False,
    )
```

profile of v0, /device:TPU:0, one launch (start us, length us, event | category | flops | bytes accessed | tf_op | source)
XLA Modules:
  0.0 168.0 jit_solution(1649653345634865973)
XLA Ops:
  0.6 3.1 %collective-permute-start.22 = (bf16[256,512]{1,0:T(8,128)(2,1)}, bf16[256,512]{1,0:T(8,128)(2,1)S(1)}, u32[]{:S(2)}, u32[]{:S(2)}) collective-permute-start(bf16[256,512]{1,0:T(8,128)(2,1)} %refs_0_.3), channel_id=1, source_target_pairs={{0,4},{1,5},{2,6},{3,7},{4,0},{5,1},{6,2},{7,3},{8,12},{9,13},{10,... | collective-permute-start | bytes 786440 | tf_op jit(solution)/shard_map/ppermute | solution.py:39
  3.7 1.5 collective-permute-start.21
  5.2 0.5 collective-permute-start.25
  5.8 1.0 fusion
  6.8 4.2 %collective-permute-done.22.refs_2_ = bf16[256,512]{1,0:T(8,128)(2,1)S(1)} collective-permute-done((bf16[256,512]{1,0:T(8,128)(2,1)}, bf16[256,512]{1,0:T(8,128)(2,1)S(1)}, u32[]{:S(2)}, u32[]{:S(2)}) %collective-permute-start.22) | collective-permute-done | bytes 262176 | tf_op jit(solution)/shard_map/ppermute | solution.py:39
  11.1 2.0 %collective-permute-start.23 = (bf16[256,512]{1,0:T(8,128)(2,1)S(1)}, bf16[256,512]{1,0:T(8,128)(2,1)S(1)}, u32[]{:S(2)}, u32[]{:S(2)}) collective-permute-start(bf16[256,512]{1,0:T(8,128)(2,1)S(1)} %collective-permute-done.22.refs_2_), channel_id=1, source_target_pairs={{0,2},{1,3},{2,0},{3,1},{4,6},{5,7},{6,4},{7,5},{8,10},{9,11},{10,... | collective-permute-start | bytes 786440 | tf_op jit(solution)/shard_map/ppermute | solution.py:39
  13.1 5.6 %collective-permute-done.24.refs_5_ = bf16[256,512]{1,0:T(8,128)(2,1)S(1)} collective-permute-done((bf16[256,512]{1,0:T(8,128)(2,1)}, bf16[256,512]{1,0:T(8,128)(2,1)S(1)}, u32[]{:S(2)}, u32[]{:S(2)}) %collective-permute-start.24) | collective-permute-done | bytes 262176 | tf_op jit(solution)/shard_map/ppermute | solution.py:39
  18.8 1.0 fusion.2.refs_0_
  19.9 2.1 %split_norm.1 = (bf16[128,1024]{1,0:T(8,128)(2,1)}, bf16[128,1024]{1,0:T(8,128)(2,1)}) custom-call(s32[1]{0:T(128)} %bitcast.4.at_ref, bf16[128,2048]{1,0:T(8,128)(2,1)} %refs_9_.1, f32[1,2048]{1,0:T(1,128)} %bitcast.40), custom_call_target="tpu_custom_call" | custom-call | flops 2097152 | bytes 1048576 | tf_op jit(solution)/shard_map/split_norm/pallas_call | solution.py:127
  22.0 2.9 %collective-permute-start.2 = (bf16[24,2048]{1,0:T(8,128)(2,1)S(1)}, bf16[24,2048]{1,0:T(8,128)(2,1)S(1)}, u32[]{:S(2)}, u32[]{:S(2)}) collective-permute-start(bf16[24,2048]{1,0:T(8,128)(2,1)S(1)} %fusion.2.refs_0_), channel_id=1, source_target_pairs={{0,6},{1,7},{2,4},{3,5},{4,2},{5,3},{6,0},{7,1},{8,14},{9,15},{10,... | collective-permute-start | bytes 294920 | tf_op jit(solution)/shard_map/ppermute | solution.py:39
  25.1 1.2 maximum_bitcast_fusion.1
  26.8 1.6 collective-permute-start
  28.6 2.7 %collective-permute-start.10 = (bf16[24,2048]{1,0:T(8,128)(2,1)S(1)}, bf16[24,2048]{1,0:T(8,128)(2,1)S(1)}, u32[]{:S(2)}, u32[]{:S(2)}) collective-permute-start(bf16[24,2048]{1,0:T(8,128)(2,1)S(1)} %copy-done.13), channel_id=1, source_target_pairs={{0,16},{8,24},{16,0},{24,8},{1,17},{9,25},{17,1},{25,9},{2,18},{10... | collective-permute-start | bytes 294920 | tf_op jit(solution)/shard_map/ppermute | solution.py:39
  31.3 1.6 collective-permute-start.9
  33.1 1.5 pad_maximum_fusion
  34.6 3.6 %project_kv.1 = (f32[8,128,128]{2,1,0:T(8,128)}, f32[8,128,128]{2,1,0:T(8,128)}) custom-call(bf16[128,1024]{1,0:T(8,128)(2,1)} %get-tuple-element.26.own_ref, bf16[128,1024]{1,0:T(8,128)(2,1)} %copy-done.16, bf16[256,512]{1,0:T(8,128)(2,1)} %refs_0_.3, bf16[256,512]{1,0:T(8,128)(2,1)} %copy-done.2, bf16[256,512]{1,0:T(8,128)(2,1)} %copy-done.1, ...), custom_call_target="tpu_custom_call" | custom-call | flops 536870912 | bytes 2097152 | tf_op jit(solution)/shard_map/project_kv/pallas_call | solution.py:158
  39.5 2.0 %collective-permute-start.14 = (bf16[4,24,2048]{2,1,0:T(8,128)(2,1)S(1)}, bf16[4,24,2048]{2,1,0:T(8,128)(2,1)S(1)}, u32[]{:S(2)}, u32[]{:S(2)}) collective-permute-start(bf16[4,24,2048]{2,1,0:T(8,128)(2,1)S(1)} %pad_maximum_fusion.1.refs_0_), channel_id=1, source_target_pairs={{0,6},{1,7},{2,4},{3,5},{4,2},{5,3},{6,0},{7,1},{8,14},{9,15},{10,... | collective-permute-start | bytes 1179656 | tf_op jit(solution)/shard_map/ppermute | solution.py:39
  41.5 0.6 collective-permute-start.13
  42.1 1.0 collective-permute-start.12
  43.1 9.4 %collective-permute-done.14.refs_3_ = bf16[4,24,2048]{2,1,0:T(8,128)(2,1)S(1)} collective-permute-done((bf16[4,24,2048]{2,1,0:T(8,128)(2,1)S(1)}, bf16[4,24,2048]{2,1,0:T(8,128)(2,1)S(1)}, u32[]{:S(2)}, u32[]{:S(2)}) %collective-permute-start.14) | collective-permute-done | bytes 393248 | tf_op jit(solution)/shard_map/ppermute | solution.py:39
  52.5 7.9 %collective-permute-done.13.refs_2_ = bf16[4,24,2048]{2,1,0:T(8,128)(2,1)S(1)} collective-permute-done((bf16[4,24,2048]{2,1,0:T(8,128)(2,1)S(1)}, bf16[4,24,2048]{2,1,0:T(8,128)(2,1)S(1)}, u32[]{:S(2)}, u32[]{:S(2)}) %collective-permute-start.13) | collective-permute-done | bytes 393248 | tf_op jit(solution)/shard_map/ppermute | solution.py:39
  61.1 1.8 %add_convert_fusion = bf16[8,128,128]{2,1,0:T(8,128)(2,1)} fusion(f32[8,128,128]{2,1,0:T(8,128)} %get-tuple-element.28, f32[8,128,128]{2,1,0:T(8,128)S(1)} %collective-permute-done.27), kind=kLoop, calls=%fused_computation.3 | loop fusion | flops 262144 | bytes 1310720 | tf_op jit(solution)/shard_map/convert_element_type | solution.py:555
  62.9 4.2 %all-to-all-start = ((bf16[8,128,128]{2,1,0:T(8,128)(2,1)}), bf16[8,128,128]{2,1,0:T(8,128)(2,1)}, u32[]{:S(2)}, u32[]{:S(2)}) async-start(bf16[8,128,128]{2,1,0:T(8,128)(2,1)} %add_convert_fusion), calls=%async_computation | async-start | bytes 524288 | tf_op jit(solution)/shard_map/all_to_all | solution.py:557
  67.2 2.8 %project_queries.1.refs_0_.refs_1_ = bf16[64,768]{1,0:T(8,128)(2,1)} custom-call(bf16[24,2048]{1,0:T(8,128)(2,1)} %copy-done.15, bf16[24,2048]{1,0:T(8,128)(2,1)} %collective-permute-done.refs_1_, bf16[24,2048]{1,0:T(8,128)(2,1)} %copy-done.28, bf16[24,2048]{1,0:T(8,128)(2,1)} %copy-done.27, bf16[24,2048]{1,0:T(8,128)(2,1)} %copy-done.26, ...), custom_call_target="tpu_custom_call" | custom-call | flops 201326592 | bytes 1048576 | tf_op jit(solution)/shard_map/project_queries/pallas_call | solution.py:180
  69.9 1.8 %collective-permute-start.19 = (bf16[64,768]{1,0:T(8,128)(2,1)}, bf16[64,768]{1,0:T(8,128)(2,1)S(1)}, u32[]{:S(2)}, u32[]{:S(2)}) collective-permute-start(bf16[64,768]{1,0:T(8,128)(2,1)} %project_queries.1.refs_0_.refs_1_), channel_id=1, source_target_pairs={{0,8},{8,0},{16,24},{24,16},{1,9},{9,1},{17,25},{25,17},{2,10},{10... | collective-permute-start | bytes 294920 | tf_op jit(solution)/shard_map/ppermute | solution.py:39
  71.7 3.4 %collective-permute-start.8 = (bf16[64,768]{1,0:T(8,128)(2,1)}, bf16[64,768]{1,0:T(8,128)(2,1)S(1)}, u32[]{:S(2)}, u32[]{:S(2)}) collective-permute-start(bf16[64,768]{1,0:T(8,128)(2,1)} %project_queries.1.refs_0_.refs_1_), channel_id=1, source_target_pairs={{0,24},{8,16},{16,8},{24,0},{1,25},{9,17},{17,9},{25,1},{2,26},{10... | collective-permute-start | bytes 294920 | tf_op jit(solution)/shard_map/ppermute | solution.py:39
  75.1 5.0 %project_grads.1 = (bf16[4,64,768]{2,1,0:T(8,128)(2,1)}, bf16[768,2048]{1,0:T(8,128)(2,1)}) custom-call(bf16[4,24,2048]{2,1,0:T(8,128)(2,1)} %copy-done.8, bf16[4,24,2048]{2,1,0:T(8,128)(2,1)} %collective-permute-done.12.refs_1_, bf16[4,24,2048]{2,1,0:T(8,128)(2,1)} %copy-done.12, bf16[4,24,2048]{2,1,0:T(8,128)(2,1)} %copy-done.11, ...), custom_call_target="tpu_custom_call" | custom-call | flops 805306368 | bytes 3145728 | tf_op jit(solution)/shard_map/project_grads/pallas_call | solution.py:202
  80.2 1.0 collective-permute-done.8.refs_3_.refs_1_
  81.1 3.3 %collective-permute-done.7.refs_2_.refs_0_ = bf16[64,768]{1,0:T(8,128)(2,1)} collective-permute-done((bf16[64,768]{1,0:T(8,128)(2,1)}, bf16[64,768]{1,0:T(8,128)(2,1)}, u32[]{:S(2)}, u32[]{:S(2)}) %collective-permute-start.7) | collective-permute-done | bytes 98336 | tf_op jit(solution)/shard_map/ppermute | solution.py:39
  84.4 6.8 %forward_all.1 = (f32[4,64,768]{2,1,0:T(8,128)}, f32[8,768]{1,0:T(8,128)}) custom-call(bf16[64,768]{1,0:T(8,128)(2,1)} %project_queries.1.refs_0_.refs_1_, bf16[64,768]{1,0:T(8,128)(2,1)} %copy-done.38, bf16[64,768]{1,0:T(8,128)(2,1)} %collective-permute-done.7.refs_2_.refs_0_, bf16[64,768]{1,0:T(8,128)(2,1)} %copy-done.39, ...), custom_call_target="tpu_custom_call" | custom-call | flops 1610612736 | bytes 1048576 | tf_op jit(solution)/shard_map/forward_all/pallas_call | solution.py:249
  91.2 1.8 %collective-permute-start.30 = (f32[8,768]{1,0:T(8,128)}, f32[8,768]{1,0:T(8,128)S(1)}, u32[]{:S(2)}, u32[]{:S(2)}) collective-permute-start(f32[8,768]{1,0:T(8,128)} %get-tuple-element.30.refs_0_), channel_id=1, source_target_pairs={{0,24},{8,16},{16,8},{24,0},{1,25},{9,17},{17,9},{25,1},{2,26},{10... | collective-permute-start | bytes 73736 | tf_op jit(solution)/shard_map/ppermute | solution.py:39
  93.0 2.6 %collective-permute-start.28 = (f32[8,768]{1,0:T(8,128)}, f32[8,768]{1,0:T(8,128)S(1)}, u32[]{:S(2)}, u32[]{:S(2)}) collective-permute-start(f32[8,768]{1,0:T(8,128)} %get-tuple-element.30.refs_0_), channel_id=1, source_target_pairs={{0,8},{8,0},{16,24},{24,16},{1,9},{9,1},{17,25},{25,17},{2,10},{10... | collective-permute-start | bytes 73736 | tf_op jit(solution)/shard_map/ppermute | solution.py:39
  95.6 1.6 collective-permute-done.30.refs_3_
  97.2 0.7 collective-permute-done.29.refs_2_
  98.0 0.6 copy-done.36
  98.6 2.1 %combine_stats.1 = (f32[8,768]{1,0:T(8,128)}, bf16[4,64,768]{2,1,0:T(8,128)(2,1)}) custom-call(f32[8,768]{1,0:T(8,128)} %get-tuple-element.30.refs_0_, f32[8,768]{1,0:T(8,128)} %copy-done.37, f32[8,768]{1,0:T(8,128)} %copy-done.36, f32[8,768]{1,0:T(8,128)} %copy-done.35, f32[4,64,768]{2,1,0:T(8,128)} %get-tuple-element.31.refs_4_), custom_call_target="tpu_custom_call" | custom-call | tf_op jit(solution)/shard_map/combine_stats/pallas_call | solution.py:289
  100.6 6.2 %backward_some.2 = (bf16[64,768]{1,0:T(8,128)(2,1)}, bf16[64,768]{1,0:T(8,128)(2,1)}, f32[1024,128]{1,0:T(8,128)}) custom-call(bf16[64,768]{1,0:T(8,128)(2,1)} %collective-permute-done.7.refs_2_.refs_0_, bf16[64,768]{1,0:T(8,128)(2,1)} %copy-done.39, bf16[4,64,768]{2,1,0:T(8,128)(2,1)} %get-tuple-element.25.refs_4_.refs_2_, ...), custom_call_target="tpu_custom_call" | custom-call | flops 2013265920 | bytes 1048576 | tf_op jit(solution)/shard_map/backward_some/pallas_call | solution.py:334
  106.9 2.0 %collective-permute-start.31 = (bf16[64,768]{1,0:T(8,128)(2,1)}, bf16[64,768]{1,0:T(8,128)(2,1)S(1)}, u32[]{:S(2)}, u32[]{:S(2)}) collective-permute-start(bf16[64,768]{1,0:T(8,128)(2,1)} %get-tuple-element.33), channel_id=1, source_target_pairs={{0,16},{8,24},{16,0},{24,8},{1,17},{9,25},{17,1},{25,9},{2,18},{10... | collective-permute-start | bytes 294920 | tf_op jit(solution)/shard_map/ppermute | solution.py:39
  108.9 2.0 %collective-permute-start.32 = (bf16[64,768]{1,0:T(8,128)(2,1)}, bf16[64,768]{1,0:T(8,128)(2,1)S(1)}, u32[]{:S(2)}, u32[]{:S(2)}) collective-permute-start(bf16[64,768]{1,0:T(8,128)(2,1)} %get-tuple-element.34), channel_id=1, source_target_pairs={{0,24},{8,16},{16,8},{24,0},{1,25},{9,17},{17,9},{25,1},{2,26},{10... | collective-permute-start | bytes 294920 | tf_op jit(solution)/shard_map/ppermute | solution.py:39
  110.9 6.7 %backward_some.3 = (bf16[64,768]{1,0:T(8,128)(2,1)}, bf16[64,768]{1,0:T(8,128)(2,1)}, bf16[1024,128]{1,0:T(8,128)(2,1)}) custom-call(bf16[64,768]{1,0:T(8,128)(2,1)} %copy-done.38, bf16[64,768]{1,0:T(8,128)(2,1)} %project_queries.1.refs_0_.refs_1_, bf16[4,64,768]{2,1,0:T(8,128)(2,1)} %get-tuple-element.25.refs_4_.refs_2_, ...), custom_call_target="tpu_custom_call" | custom-call | flops 2013265920 | bytes 1048576 | tf_op jit(solution)/shard_map/backward_some/pallas_call | solution.py:334
  117.6 4.8 %collective-permute-done.33.refs_2_ = bf16[64,768]{1,0:T(8,128)(2,1)S(1)} collective-permute-done((bf16[64,768]{1,0:T(8,128)(2,1)}, bf16[64,768]{1,0:T(8,128)(2,1)S(1)}, u32[]{:S(2)}, u32[]{:S(2)}) %collective-permute-start.33) | collective-permute-done | bytes 98336 | tf_op jit(solution)/shard_map/ppermute | solution.py:39
  122.4 0.6 copy-done.25
  123.0 3.0 %query_back.1 = (f32[96,2048]{1,0:T(8,128)}, bf16[96,2048]{1,0:T(8,128)(2,1)}) custom-call(bf16[64,768]{1,0:T(8,128)(2,1)} %copy-done.18, bf16[64,768]{1,0:T(8,128)(2,1)} %copy-done.20, bf16[64,768]{1,0:T(8,128)(2,1)} %copy-done.25, bf16[64,768]{1,0:T(8,128)(2,1)} %get-tuple-element.37.refs_3_, bf16[2048,256]{1,0:T(8,128)(2,1)} %refs_4_.5), custom_call_target="tpu_custom_call" | custom-call | flops 201326592 | bytes 1048576 | tf_op jit(solution)/shard_map/query_back/pallas_call | solution.py:364
  126.1 1.9 %collective-permute-start.41 = (bf16[64,768]{1,0:T(8,128)(2,1)S(1)}, bf16[64,768]{1,0:T(8,128)(2,1)S(1)}, u32[]{:S(2)}, u32[]{:S(2)}) collective-permute-start(bf16[64,768]{1,0:T(8,128)(2,1)S(1)} %get-tuple-element.47), channel_id=1, source_target_pairs={{0,24},{8,16},{16,8},{24,0},{1,25},{9,17},{17,9},{25,1},{2,26},{10... | collective-permute-start | bytes 294920 | tf_op jit(solution)/shard_map/ppermute | solution.py:39
  128.0 2.6 %collective-permute-start.39 = (bf16[64,768]{1,0:T(8,128)(2,1)S(1)}, bf16[64,768]{1,0:T(8,128)(2,1)S(1)}, u32[]{:S(2)}, u32[]{:S(2)}) collective-permute-start(bf16[64,768]{1,0:T(8,128)(2,1)S(1)} %get-tuple-element.49), channel_id=1, source_target_pairs={{0,8},{8,0},{16,24},{24,16},{1,9},{9,1},{17,25},{25,17},{2,10},{10... | collective-permute-start | bytes 294920 | tf_op jit(solution)/shard_map/ppermute | solution.py:39
  130.5 3.7 %all-to-all-start.1 = ((bf16[8,128,128]{2,1,0:T(8,128)(2,1)}), bf16[8,128,128]{2,1,0:T(8,128)(2,1)S(1)}, u32[]{:S(2)}, u32[]{:S(2)}) async-start(bf16[8,128,128]{2,1,0:T(8,128)(2,1)} %bitcast.36), calls=%async_computation.1 | async-start | bytes 524288 | tf_op jit(solution)/shard_map/all_to_all | solution.py:579
  134.2 3.1 %collective-permute-done.40.refs_2_ = bf16[64,768]{1,0:T(8,128)(2,1)S(1)} collective-permute-done((bf16[64,768]{1,0:T(8,128)(2,1)S(1)}, bf16[64,768]{1,0:T(8,128)(2,1)S(1)}, u32[]{:S(2)}, u32[]{:S(2)}) %collective-permute-start.40) | collective-permute-done | bytes 98336 | tf_op jit(solution)/shard_map/ppermute | solution.py:39
  137.4 0.6 copy-done.23
  138.0 0.6 copy-done.24
  138.6 1.8 %attend_sum.1.refs_0_ = bf16[64,768]{1,0:T(8,128)(2,1)} custom-call(bf16[4,64,768]{2,1,0:T(8,128)(2,1)} %get-tuple-element.45.refs_0_, bf16[64,768]{1,0:T(8,128)(2,1)} %copy-done.24, bf16[64,768]{1,0:T(8,128)(2,1)} %copy-done.23, bf16[64,768]{1,0:T(8,128)(2,1)} %copy-done.21), custom_call_target="tpu_custom_call" | custom-call | tf_op jit(solution)/shard_map/attend_sum/pallas_call | solution.py:416
  140.4 1.8 %collective-permute-start.44 = (bf16[64,768]{1,0:T(8,128)(2,1)}, bf16[64,768]{1,0:T(8,128)(2,1)S(1)}, u32[]{:S(2)}, u32[]{:S(2)}) collective-permute-start(bf16[64,768]{1,0:T(8,128)(2,1)} %attend_sum.1.refs_0_), channel_id=1, source_target_pairs={{0,24},{8,16},{16,8},{24,0},{1,25},{9,17},{17,9},{25,1},{2,26},{10... | collective-permute-start | bytes 294920 | tf_op jit(solution)/shard_map/ppermute | solution.py:39
  142.3 2.6 %collective-permute-start.42 = (bf16[64,768]{1,0:T(8,128)(2,1)}, bf16[64,768]{1,0:T(8,128)(2,1)S(1)}, u32[]{:S(2)}, u32[]{:S(2)}) collective-permute-start(bf16[64,768]{1,0:T(8,128)(2,1)} %attend_sum.1.refs_0_), channel_id=1, source_target_pairs={{0,8},{8,0},{16,24},{24,16},{1,9},{9,1},{17,25},{25,17},{2,10},{10... | collective-permute-start | bytes 294920 | tf_op jit(solution)/shard_map/ppermute | solution.py:39
  144.8 0.7 copy-done.14
  145.6 2.0 %share_rows.1 = (f32[24,2048]{1,0:T(8,128)}, bf16[24,2048]{1,0:T(8,128)(2,1)}, bf16[24,2048]{1,0:T(8,128)(2,1)}, bf16[24,2048]{1,0:T(8,128)(2,1)}) custom-call(f32[96,2048]{1,0:T(8,128)} %get-tuple-element.38.own_ref, bf16[96,2048]{1,0:T(8,128)(2,1)} %copy-done.14), custom_call_target="tpu_custom_call" | custom-call | tf_op jit(solution)/shard_map/share_rows/pallas_call | solution.py:384
  147.6 1.5 collective-permute-start.35
  149.1 1.5 collective-permute-start.36
  150.6 0.8 collective-permute-done.43.refs_2_
  151.4 2.4 %collective-permute-start.37 = (bf16[24,2048]{1,0:T(8,128)(2,1)}, bf16[24,2048]{1,0:T(8,128)(2,1)S(1)}, u32[]{:S(2)}, u32[]{:S(2)}) collective-permute-start(bf16[24,2048]{1,0:T(8,128)(2,1)} %get-tuple-element.43), channel_id=1, source_target_pairs={{0,6},{1,7},{2,4},{3,5},{4,2},{5,3},{6,0},{7,1},{8,14},{9,15},{10,... | collective-permute-start | bytes 294920 | tf_op jit(solution)/shard_map/ppermute | solution.py:39
  153.9 0.6 copy-done.34
  154.5 5.0 %weight_grad.1 = f32[256,2048]{1,0:T(8,128)} custom-call(bf16[64,768]{1,0:T(8,128)(2,1)} %attend_sum.1.refs_0_, bf16[64,768]{1,0:T(8,128)(2,1)} %copy-done.34, bf16[64,768]{1,0:T(8,128)(2,1)} %copy-done.33, bf16[64,768]{1,0:T(8,128)(2,1)} %copy-done.32, bf16[768,2048]{1,0:T(8,128)(2,1)} %get-tuple-element.46.refs_4_), custom_call_target="tpu_custom_call" | custom-call | flops 805306368 | bytes 3145728 | tf_op jit(solution)/shard_map/weight_grad/pallas_call | solution.py:442
  159.5 0.6 copy-done.17
  160.2 2.0 %target_finish.1 = f32[24,2048]{1,0:T(8,128)} custom-call(f32[24,2048]{1,0:T(8,128)} %get-tuple-element.40.kept_ref, bf16[24,2048]{1,0:T(8,128)(2,1)} %copy-done.17, bf16[24,2048]{1,0:T(8,128)(2,1)} %copy-done.19, bf16[24,2048]{1,0:T(8,128)(2,1)} %copy-done.22, bf16[24,2048]{1,0:T(8,128)(2,1)} %refs_3_.1, bf16[24,2048]{1,0:T(8,128)(2,1)} %refs_4_.6, ...), custom_call_target="tpu_custom_call" | custom-call | tf_op jit(solution)/shard_map/target_finish/pallas_call | solution.py:401
  162.2 0.7 copy-done.10
  162.9 5.1 %source_back.1 = f32[128,2048]{1,0:T(8,128)} custom-call(s32[1]{0:T(128)} %bitcast.4.at_ref, bf16[8,128,128]{2,1,0:T(8,128)(2,1)} %copy-done.10, bf16[256,512]{1,0:T(8,128)(2,1)} %refs_0_.3, bf16[256,512]{1,0:T(8,128)(2,1)} %copy-done.2, bf16[256,512]{1,0:T(8,128)(2,1)} %copy-done.1, bf16[256,512]{1,0:T(8,128)(2,1)} %copy-done.5, bf16[256,512]{1,0:T(8,128)(2,1)} %refs_4_.7, ...), custom_call_target="tpu_custom_call" | custom-call | flops 536870912 | bytes 4194304 | tf_op jit(solution)/shard_map/source_back/pallas_call | solution.py:485
  (133 shorter events, 3.7 us)
Async XLA Ops:
  0.6 27.7 %copy-start = (bf16[256,512]{1,0:T(8,128)(2,1)S(1)}, bf16[256,512]{1,0:T(8,128)(2,1)}, u32[]{:S(2)}) copy-start(bf16[256,512]{1,0:T(8,128)(2,1)} %refs_0_.3) | copy-start | bytes 786436
  0.6 10.4 %collective-permute-start.22 = (bf16[256,512]{1,0:T(8,128)(2,1)}, bf16[256,512]{1,0:T(8,128)(2,1)S(1)}, u32[]{:S(2)}, u32[]{:S(2)}) collective-permute-start(bf16[256,512]{1,0:T(8,128)(2,1)} %refs_0_.3), channel_id=1, source_target_pairs={{0,4},{1,5},{2,6},{3,7},{4,0},{5,1},{6,2},{7,3},{8,12},{9,13},{10,... | collective-permute-start | bytes 786440 | tf_op jit(solution)/shard_map/ppermute | solution.py:39
  3.7 22.6 %collective-permute-start.21 = (bf16[256,512]{1,0:T(8,128)(2,1)}, bf16[256,512]{1,0:T(8,128)(2,1)S(1)}, u32[]{:S(2)}, u32[]{:S(2)}) collective-permute-start(bf16[256,512]{1,0:T(8,128)(2,1)} %refs_0_.3), channel_id=1, source_target_pairs={{0,2},{1,3},{2,0},{3,1},{4,6},{5,7},{6,4},{7,5},{8,10},{9,11},{10,... | collective-permute-start | bytes 786440 | tf_op jit(solution)/shard_map/ppermute | solution.py:39
  5.2 16.8 %collective-permute-start.25 = (bf16[256,512]{1,0:T(8,128)(2,1)}, bf16[256,512]{1,0:T(8,128)(2,1)S(1)}, u32[]{:S(2)}, u32[]{:S(2)}) collective-permute-start(bf16[256,512]{1,0:T(8,128)(2,1)} %refs_4_.7), channel_id=1, source_target_pairs={{0,4},{1,5},{2,6},{3,7},{4,0},{5,1},{6,2},{7,3},{8,12},{9,13},{10,... | collective-permute-start | bytes 786440 | tf_op jit(solution)/shard_map/ppermute | solution.py:39
  5.7 13.0 %collective-permute-start.24 = (bf16[256,512]{1,0:T(8,128)(2,1)}, bf16[256,512]{1,0:T(8,128)(2,1)S(1)}, u32[]{:S(2)}, u32[]{:S(2)}) collective-permute-start(bf16[256,512]{1,0:T(8,128)(2,1)} %refs_4_.7), channel_id=1, source_target_pairs={{0,2},{1,3},{2,0},{3,1},{4,6},{5,7},{6,4},{7,5},{8,10},{9,11},{10,... | collective-permute-start | bytes 786440 | tf_op jit(solution)/shard_map/ppermute | solution.py:39
  11.1 17.4 %copy-start.1 = (bf16[256,512]{1,0:T(8,128)(2,1)}, bf16[256,512]{1,0:T(8,128)(2,1)S(1)}, u32[]{:S(2)}) copy-start(bf16[256,512]{1,0:T(8,128)(2,1)S(1)} %collective-permute-done.22.refs_2_) | copy-start | bytes 786436
  11.1 15.7 %collective-permute-start.23 = (bf16[256,512]{1,0:T(8,128)(2,1)S(1)}, bf16[256,512]{1,0:T(8,128)(2,1)S(1)}, u32[]{:S(2)}, u32[]{:S(2)}) collective-permute-start(bf16[256,512]{1,0:T(8,128)(2,1)S(1)} %collective-permute-done.22.refs_2_), channel_id=1, source_target_pairs={{0,2},{1,3},{2,0},{3,1},{4,6},{5,7},{6,4},{7,5},{8,10},{9,11},{10,... | collective-permute-start | bytes 786440 | tf_op jit(solution)/shard_map/ppermute | solution.py:39
  18.7 9.8 %copy-start.4 = (bf16[256,512]{1,0:T(8,128)(2,1)}, bf16[256,512]{1,0:T(8,128)(2,1)S(1)}, u32[]{:S(2)}) copy-start(bf16[256,512]{1,0:T(8,128)(2,1)S(1)} %collective-permute-done.24.refs_5_) | copy-start | bytes 786436
  18.7 6.4 %collective-permute-start.26 = (bf16[256,512]{1,0:T(8,128)(2,1)S(1)}, bf16[256,512]{1,0:T(8,128)(2,1)S(1)}, u32[]{:S(2)}, u32[]{:S(2)}) collective-permute-start(bf16[256,512]{1,0:T(8,128)(2,1)S(1)} %collective-permute-done.24.refs_5_), channel_id=1, source_target_pairs={{0,4},{1,5},{2,6},{3,7},{4,0},{5,1},{6,2},{7,3},{8,12},{9,13},{10,... | collective-permute-start | bytes 786440 | tf_op jit(solution)/shard_map/ppermute | solution.py:39
  19.8 8.7 %copy-start.15 = (bf16[24,2048]{1,0:T(8,128)(2,1)}, bf16[24,2048]{1,0:T(8,128)(2,1)S(1)}, u32[]{:S(2)}) copy-start(bf16[24,2048]{1,0:T(8,128)(2,1)S(1)} %fusion.2.refs_0_) | copy-start | bytes 294916
  19.8 8.7 %collective-permute-start.3 = (bf16[24,2048]{1,0:T(8,128)(2,1)S(1)}, bf16[24,2048]{1,0:T(8,128)(2,1)S(1)}, u32[]{:S(2)}, u32[]{:S(2)}) collective-permute-start(bf16[24,2048]{1,0:T(8,128)(2,1)S(1)} %fusion.2.refs_0_), channel_id=1, source_target_pairs={{0,1},{1,0},{2,3},{3,2},{4,5},{5,4},{6,7},{7,6},{8,9},{9,8},{10,11... | collective-permute-start | bytes 294920 | tf_op jit(solution)/shard_map/ppermute | solution.py:39
  22.0 6.6 %copy-start.3 = (bf16[256,512]{1,0:T(8,128)(2,1)}, bf16[256,512]{1,0:T(8,128)(2,1)S(1)}, u32[]{:S(2)}) copy-start(bf16[256,512]{1,0:T(8,128)(2,1)S(1)} %collective-permute-done.25.refs_6_) | copy-start | bytes 786436
  22.0 9.3 %collective-permute-start.2 = (bf16[24,2048]{1,0:T(8,128)(2,1)S(1)}, bf16[24,2048]{1,0:T(8,128)(2,1)S(1)}, u32[]{:S(2)}, u32[]{:S(2)}) collective-permute-start(bf16[24,2048]{1,0:T(8,128)(2,1)S(1)} %fusion.2.refs_0_), channel_id=1, source_target_pairs={{0,6},{1,7},{2,4},{3,5},{4,2},{5,3},{6,0},{7,1},{8,14},{9,15},{10,... | collective-permute-start | bytes 294920 | tf_op jit(solution)/shard_map/ppermute | solution.py:39
  25.1 7.7 %collective-permute-start.20 = (bf16[128,1024]{1,0:T(8,128)(2,1)}, bf16[128,1024]{1,0:T(8,128)(2,1)S(1)}, u32[]{:S(2)}, u32[]{:S(2)}) collective-permute-start(bf16[128,1024]{1,0:T(8,128)(2,1)} %get-tuple-element.27), channel_id=1, source_target_pairs={{0,1},{1,0},{2,3},{3,2},{4,5},{5,4},{6,7},{7,6},{8,9},{9,8},{10,11... | collective-permute-start | bytes 786440 | tf_op jit(solution)/shard_map/ppermute | solution.py:39
  26.3 8.3 %copy-start.2 = (bf16[256,512]{1,0:T(8,128)(2,1)}, bf16[256,512]{1,0:T(8,128)(2,1)S(1)}, u32[]{:S(2)}) copy-start(bf16[256,512]{1,0:T(8,128)(2,1)S(1)} %collective-permute-done.21.refs_1_) | copy-start | bytes 786436
  26.3 11.9 %collective-permute-start.1 = (bf16[24,2048]{1,0:T(8,128)(2,1)S(1)}, bf16[24,2048]{1,0:T(8,128)(2,1)S(1)}, u32[]{:S(2)}, u32[]{:S(2)}) collective-permute-start(bf16[24,2048]{1,0:T(8,128)(2,1)S(1)} %fusion.2.refs_0_), channel_id=1, source_target_pairs={{0,4},{1,5},{2,6},{3,7},{4,0},{5,1},{6,2},{7,3},{8,12},{9,13},{10,... | collective-permute-start | bytes 294920 | tf_op jit(solution)/shard_map/ppermute | solution.py:39
  26.8 7.8 %copy-start.5 = (bf16[256,512]{1,0:T(8,128)(2,1)}, bf16[256,512]{1,0:T(8,128)(2,1)S(1)}, u32[]{:S(2)}) copy-start(bf16[256,512]{1,0:T(8,128)(2,1)S(1)} %collective-permute-done.23.refs_3_) | copy-start | bytes 786436
  26.8 11.5 %collective-permute-start = (bf16[24,2048]{1,0:T(8,128)(2,1)S(1)}, bf16[24,2048]{1,0:T(8,128)(2,1)}, u32[]{:S(2)}, u32[]{:S(2)}) collective-permute-start(bf16[24,2048]{1,0:T(8,128)(2,1)S(1)} %fusion.2.refs_0_), channel_id=1, source_target_pairs={{0,2},{1,3},{2,0},{3,1},{4,6},{5,7},{6,4},{7,5},{8,10},{9,11},{10,... | collective-permute-start | bytes 294920 | tf_op jit(solution)/shard_map/ppermute | solution.py:39
  28.6 6.0 %copy-start.26 = (bf16[24,2048]{1,0:T(8,128)(2,1)}, bf16[24,2048]{1,0:T(8,128)(2,1)S(1)}, u32[]{:S(2)}) copy-start(bf16[24,2048]{1,0:T(8,128)(2,1)S(1)} %collective-permute-done.3.refs_4_) | copy-start | bytes 294916
  28.6 10.2 %collective-permute-start.10 = (bf16[24,2048]{1,0:T(8,128)(2,1)S(1)}, bf16[24,2048]{1,0:T(8,128)(2,1)S(1)}, u32[]{:S(2)}, u32[]{:S(2)}) collective-permute-start(bf16[24,2048]{1,0:T(8,128)(2,1)S(1)} %copy-done.13), channel_id=1, source_target_pairs={{0,16},{8,24},{16,0},{24,8},{1,17},{9,25},{17,1},{25,9},{2,18},{10... | collective-permute-start | bytes 294920 | tf_op jit(solution)/shard_map/ppermute | solution.py:39
  31.2 6.9 %copy-start.27 = (bf16[24,2048]{1,0:T(8,128)(2,1)}, bf16[24,2048]{1,0:T(8,128)(2,1)S(1)}, u32[]{:S(2)}) copy-start(bf16[24,2048]{1,0:T(8,128)(2,1)S(1)} %collective-permute-done.2.refs_3_) | copy-start | bytes 294916
  31.3 7.6 %collective-permute-start.9 = (bf16[24,2048]{1,0:T(8,128)(2,1)S(1)}, bf16[24,2048]{1,0:T(8,128)(2,1)S(1)}, u32[]{:S(2)}, u32[]{:S(2)}) collective-permute-start(bf16[24,2048]{1,0:T(8,128)(2,1)S(1)} %copy-done.13), channel_id=1, source_target_pairs={{0,8},{8,0},{16,24},{24,16},{1,9},{9,1},{17,25},{25,17},{2,10},{10... | collective-permute-start | bytes 294920 | tf_op jit(solution)/shard_map/ppermute | solution.py:39
  32.8 6.5 %collective-permute-start.11 = (bf16[24,2048]{1,0:T(8,128)(2,1)S(1)}, bf16[24,2048]{1,0:T(8,128)(2,1)S(1)}, u32[]{:S(2)}, u32[]{:S(2)}) collective-permute-start(bf16[24,2048]{1,0:T(8,128)(2,1)S(1)} %copy-done.13), channel_id=1, source_target_pairs={{0,24},{8,16},{16,8},{24,0},{1,25},{9,17},{17,9},{25,1},{2,26},{10... | collective-permute-start | bytes 294920 | tf_op jit(solution)/shard_map/ppermute | solution.py:39
  38.2 1.4 collective-permute-start.6
  38.3 3.2 %collective-permute-start.5 = (bf16[24,2048]{1,0:T(8,128)(2,1)S(1)}, bf16[24,2048]{1,0:T(8,128)(2,1)S(1)}, u32[]{:S(2)}, u32[]{:S(2)}) collective-permute-start(bf16[24,2048]{1,0:T(8,128)(2,1)S(1)} %collective-permute-done.1.refs_2_), channel_id=1, source_target_pairs={{0,1},{1,0},{2,3},{3,2},{4,5},{5,4},{6,7},{7,6},{8,9},{9,8},{10,11... | collective-permute-start | bytes 294920 | tf_op jit(solution)/shard_map/ppermute | solution.py:39
  38.8 3.3 %collective-permute-start.4 = (bf16[24,2048]{1,0:T(8,128)(2,1)}, bf16[24,2048]{1,0:T(8,128)(2,1)S(1)}, u32[]{:S(2)}, u32[]{:S(2)}) collective-permute-start(bf16[24,2048]{1,0:T(8,128)(2,1)} %collective-permute-done.refs_1_), channel_id=1, source_target_pairs={{0,1},{1,0},{2,3},{3,2},{4,5},{5,4},{6,7},{7,6},{8,9},{9,8},{10,11... | collective-permute-start | bytes 294920 | tf_op jit(solution)/shard_map/ppermute | solution.py:39
  38.8 22.0 %collective-permute-start.27 = (f32[8,128,128]{2,1,0:T(8,128)}, f32[8,128,128]{2,1,0:T(8,128)S(1)}, u32[]{:S(2)}, u32[]{:S(2)}) collective-permute-start(f32[8,128,128]{2,1,0:T(8,128)} %get-tuple-element.29), channel_id=1, source_target_pairs={{0,1},{1,0},{2,3},{3,2},{4,5},{5,4},{6,7},{7,6},{8,9},{9,8},{10,11... | collective-permute-start | bytes 1572872 | tf_op jit(solution)/shard_map/ppermute | solution.py:39
  39.4 122.8 %collective-permute-start.38 = (bf16[2,4,256,512]{3,2,1,0:T(8,128)(2,1)S(1)}, bf16[2,4,256,512]{3,2,1,0:T(8,128)(2,1)}, u32[]{:S(2)}, u32[]{:S(2)}) collective-permute-start(bf16[2,4,256,512]{3,2,1,0:T(8,128)(2,1)S(1)} %copy-done.7), channel_id=1, source_target_pairs={{0,1},{1,0},{2,3},{3,2},{4,5},{5,4},{6,7},{7,6},{8,9},{9,8},{10,11... | collective-permute-start | bytes 6291464 | tf_op jit(solution)/shard_map/ppermute | solution.py:39
  39.4 35.7 %copy-start.8 = (bf16[4,24,2048]{2,1,0:T(8,128)(2,1)}, bf16[4,24,2048]{2,1,0:T(8,128)(2,1)S(1)}, u32[]{:S(2)}) copy-start(bf16[4,24,2048]{2,1,0:T(8,128)(2,1)S(1)} %pad_maximum_fusion.1.refs_0_) | copy-start | bytes 1179652
  39.5 21.4 %copy-start.29 = (bf16[24,2048]{1,0:T(8,128)(2,1)}, bf16[24,2048]{1,0:T(8,128)(2,1)S(1)}, u32[]{:S(2)}) copy-start(bf16[24,2048]{1,0:T(8,128)(2,1)S(1)} %collective-permute-done.6.refs_7_) | copy-start | bytes 294916
  39.5 12.9 %collective-permute-start.14 = (bf16[4,24,2048]{2,1,0:T(8,128)(2,1)S(1)}, bf16[4,24,2048]{2,1,0:T(8,128)(2,1)S(1)}, u32[]{:S(2)}, u32[]{:S(2)}) collective-permute-start(bf16[4,24,2048]{2,1,0:T(8,128)(2,1)S(1)} %pad_maximum_fusion.1.refs_0_), channel_id=1, source_target_pairs={{0,6},{1,7},{2,4},{3,5},{4,2},{5,3},{6,0},{7,1},{8,14},{9,15},{10,... | collective-permute-start | bytes 1179656 | tf_op jit(solution)/shard_map/ppermute | solution.py:39
  41.5 25.7 %copy-start.30 = (bf16[24,2048]{1,0:T(8,128)(2,1)}, bf16[24,2048]{1,0:T(8,128)(2,1)S(1)}, u32[]{:S(2)}) copy-start(bf16[24,2048]{1,0:T(8,128)(2,1)S(1)} %collective-permute-done.5.refs_6_) | copy-start | bytes 294916
  41.5 18.9 %collective-permute-start.13 = (bf16[4,24,2048]{2,1,0:T(8,128)(2,1)S(1)}, bf16[4,24,2048]{2,1,0:T(8,128)(2,1)S(1)}, u32[]{:S(2)}, u32[]{:S(2)}) collective-permute-start(bf16[4,24,2048]{2,1,0:T(8,128)(2,1)S(1)} %pad_maximum_fusion.1.refs_0_), channel_id=1, source_target_pairs={{0,4},{1,5},{2,6},{3,7},{4,0},{5,1},{6,2},{7,3},{8,12},{9,13},{10,... | collective-permute-start | bytes 1179656 | tf_op jit(solution)/shard_map/ppermute | solution.py:39
  42.1 19.0 %copy-start.31 = (bf16[24,2048]{1,0:T(8,128)(2,1)}, bf16[24,2048]{1,0:T(8,128)(2,1)S(1)}, u32[]{:S(2)}) copy-start(bf16[24,2048]{1,0:T(8,128)(2,1)S(1)} %collective-permute-done.4.refs_5_) | copy-start | bytes 294916
  42.1 18.5 %collective-permute-start.12 = (bf16[4,24,2048]{2,1,0:T(8,128)(2,1)S(1)}, bf16[4,24,2048]{2,1,0:T(8,128)(2,1)}, u32[]{:S(2)}, u32[]{:S(2)}) collective-permute-start(bf16[4,24,2048]{2,1,0:T(8,128)(2,1)S(1)} %pad_maximum_fusion.1.refs_0_), channel_id=1, source_target_pairs={{0,2},{1,3},{2,0},{3,1},{4,6},{5,7},{6,4},{7,5},{8,10},{9,11},{10,... | collective-permute-start | bytes 1179656 | tf_op jit(solution)/shard_map/ppermute | solution.py:39
  52.5 22.6 %copy-start.11 = (bf16[4,24,2048]{2,1,0:T(8,128)(2,1)}, bf16[4,24,2048]{2,1,0:T(8,128)(2,1)S(1)}, u32[]{:S(2)}) copy-start(bf16[4,24,2048]{2,1,0:T(8,128)(2,1)S(1)} %collective-permute-done.14.refs_3_) | copy-start | bytes 1179652
  52.5 17.5 %collective-permute-start.15 = (bf16[4,24,2048]{2,1,0:T(8,128)(2,1)S(1)}, bf16[4,24,2048]{2,1,0:T(8,128)(2,1)}, u32[]{:S(2)}, u32[]{:S(2)}) collective-permute-start(bf16[4,24,2048]{2,1,0:T(8,128)(2,1)S(1)} %pad_maximum_fusion.1.refs_0_), channel_id=1, source_target_pairs={{0,1},{1,0},{2,3},{3,2},{4,5},{5,4},{6,7},{7,6},{8,9},{9,8},{10,11... | collective-permute-start | bytes 1179656 | tf_op jit(solution)/shard_map/ppermute | solution.py:39
  60.4 14.8 %copy-start.12 = (bf16[4,24,2048]{2,1,0:T(8,128)(2,1)}, bf16[4,24,2048]{2,1,0:T(8,128)(2,1)S(1)}, u32[]{:S(2)}) copy-start(bf16[4,24,2048]{2,1,0:T(8,128)(2,1)S(1)} %collective-permute-done.13.refs_2_) | copy-start | bytes 1179652
  60.4 11.3 %collective-permute-start.18 = (bf16[4,24,2048]{2,1,0:T(8,128)(2,1)S(1)}, bf16[4,24,2048]{2,1,0:T(8,128)(2,1)}, u32[]{:S(2)}, u32[]{:S(2)}) collective-permute-start(bf16[4,24,2048]{2,1,0:T(8,128)(2,1)S(1)} %collective-permute-done.14.refs_3_), channel_id=1, source_target_pairs={{0,1},{1,0},{2,3},{3,2},{4,5},{5,4},{6,7},{7,6},{8,9},{9,8},{10,11... | collective-permute-start | bytes 1179656 | tf_op jit(solution)/shard_map/ppermute | solution.py:39
  60.6 14.5 %collective-permute-start.17 = (bf16[4,24,2048]{2,1,0:T(8,128)(2,1)S(1)}, bf16[4,24,2048]{2,1,0:T(8,128)(2,1)}, u32[]{:S(2)}, u32[]{:S(2)}) collective-permute-start(bf16[4,24,2048]{2,1,0:T(8,128)(2,1)S(1)} %collective-permute-done.13.refs_2_), channel_id=1, source_target_pairs={{0,1},{1,0},{2,3},{3,2},{4,5},{5,4},{6,7},{7,6},{8,9},{9,8},{10,11... | collective-permute-start | bytes 1179656 | tf_op jit(solution)/shard_map/ppermute | solution.py:39
  60.9 14.2 %collective-permute-start.16 = (bf16[4,24,2048]{2,1,0:T(8,128)(2,1)}, bf16[4,24,2048]{2,1,0:T(8,128)(2,1)}, u32[]{:S(2)}, u32[]{:S(2)}) collective-permute-start(bf16[4,24,2048]{2,1,0:T(8,128)(2,1)} %collective-permute-done.12.refs_1_), channel_id=1, source_target_pairs={{0,1},{1,0},{2,3},{3,2},{4,5},{5,4},{6,7},{7,6},{8,9},{9,8},{10,11... | collective-permute-start | bytes 1179656 | tf_op jit(solution)/shard_map/ppermute | solution.py:39
  62.9 21.5 %all-to-all-start = ((bf16[8,128,128]{2,1,0:T(8,128)(2,1)}), bf16[8,128,128]{2,1,0:T(8,128)(2,1)}, u32[]{:S(2)}, u32[]{:S(2)}) async-start(bf16[8,128,128]{2,1,0:T(8,128)(2,1)} %add_convert_fusion), calls=%async_computation | async-start | bytes 524288 | tf_op jit(solution)/shard_map/all_to_all | solution.py:557
  69.9 10.2 %collective-permute-start.19 = (bf16[64,768]{1,0:T(8,128)(2,1)}, bf16[64,768]{1,0:T(8,128)(2,1)S(1)}, u32[]{:S(2)}, u32[]{:S(2)}) collective-permute-start(bf16[64,768]{1,0:T(8,128)(2,1)} %project_queries.1.refs_0_.refs_1_), channel_id=1, source_target_pairs={{0,8},{8,0},{16,24},{24,16},{1,9},{9,1},{17,25},{25,17},{2,10},{10... | collective-permute-start | bytes 294920 | tf_op jit(solution)/shard_map/ppermute | solution.py:39
  71.7 9.4 %collective-permute-start.8 = (bf16[64,768]{1,0:T(8,128)(2,1)}, bf16[64,768]{1,0:T(8,128)(2,1)S(1)}, u32[]{:S(2)}, u32[]{:S(2)}) collective-permute-start(bf16[64,768]{1,0:T(8,128)(2,1)} %project_queries.1.refs_0_.refs_1_), channel_id=1, source_target_pairs={{0,24},{8,16},{16,8},{24,0},{1,25},{9,17},{17,9},{25,1},{2,26},{10... | collective-permute-start | bytes 294920 | tf_op jit(solution)/shard_map/ppermute | solution.py:39
  75.1 9.3 %collective-permute-start.7 = (bf16[64,768]{1,0:T(8,128)(2,1)}, bf16[64,768]{1,0:T(8,128)(2,1)}, u32[]{:S(2)}, u32[]{:S(2)}) collective-permute-start(bf16[64,768]{1,0:T(8,128)(2,1)} %project_queries.1.refs_0_.refs_1_), channel_id=1, source_target_pairs={{0,16},{8,24},{16,0},{24,8},{1,17},{9,25},{17,1},{25,9},{2,18},{10... | collective-permute-start | bytes 294920 | tf_op jit(solution)/shard_map/ppermute | solution.py:39
  91.2 6.0 %collective-permute-start.30 = (f32[8,768]{1,0:T(8,128)}, f32[8,768]{1,0:T(8,128)S(1)}, u32[]{:S(2)}, u32[]{:S(2)}) collective-permute-start(f32[8,768]{1,0:T(8,128)} %get-tuple-element.30.refs_0_), channel_id=1, source_target_pairs={{0,24},{8,16},{16,8},{24,0},{1,25},{9,17},{17,9},{25,1},{2,26},{10... | collective-permute-start | bytes 73736 | tf_op jit(solution)/shard_map/ppermute | solution.py:39
  93.0 4.9 %collective-permute-start.29 = (f32[8,768]{1,0:T(8,128)}, f32[8,768]{1,0:T(8,128)S(1)}, u32[]{:S(2)}, u32[]{:S(2)}) collective-permute-start(f32[8,768]{1,0:T(8,128)} %get-tuple-element.30.refs_0_), channel_id=1, source_target_pairs={{0,16},{8,24},{16,0},{24,8},{1,17},{9,25},{17,1},{25,9},{2,18},{10... | collective-permute-start | bytes 73736 | tf_op jit(solution)/shard_map/ppermute | solution.py:39
  93.0 4.9 %collective-permute-start.28 = (f32[8,768]{1,0:T(8,128)}, f32[8,768]{1,0:T(8,128)S(1)}, u32[]{:S(2)}, u32[]{:S(2)}) collective-permute-start(f32[8,768]{1,0:T(8,128)} %get-tuple-element.30.refs_0_), channel_id=1, source_target_pairs={{0,8},{8,0},{16,24},{24,16},{1,9},{9,1},{17,25},{25,17},{2,10},{10... | collective-permute-start | bytes 73736 | tf_op jit(solution)/shard_map/ppermute | solution.py:39
  106.9 10.7 %collective-permute-start.31 = (bf16[64,768]{1,0:T(8,128)(2,1)}, bf16[64,768]{1,0:T(8,128)(2,1)S(1)}, u32[]{:S(2)}, u32[]{:S(2)}) collective-permute-start(bf16[64,768]{1,0:T(8,128)(2,1)} %get-tuple-element.33), channel_id=1, source_target_pairs={{0,16},{8,24},{16,0},{24,8},{1,17},{9,25},{17,1},{25,9},{2,18},{10... | collective-permute-start | bytes 294920 | tf_op jit(solution)/shard_map/ppermute | solution.py:39
  108.9 8.7 %collective-permute-start.32 = (bf16[64,768]{1,0:T(8,128)(2,1)}, bf16[64,768]{1,0:T(8,128)(2,1)S(1)}, u32[]{:S(2)}, u32[]{:S(2)}) collective-permute-start(bf16[64,768]{1,0:T(8,128)(2,1)} %get-tuple-element.34), channel_id=1, source_target_pairs={{0,24},{8,16},{16,8},{24,0},{1,25},{9,17},{17,9},{25,1},{2,26},{10... | collective-permute-start | bytes 294920 | tf_op jit(solution)/shard_map/ppermute | solution.py:39
  110.9 15.1 %copy-start.9 = (bf16[4,64,768]{2,1,0:T(8,128)(2,1)S(1)}, bf16[4,64,768]{2,1,0:T(8,128)(2,1)}, u32[]{:S(2)}) copy-start(bf16[4,64,768]{2,1,0:T(8,128)(2,1)} %get-tuple-element.45.refs_0_) | copy-start | bytes 1179652
  117.6 4.8 %collective-permute-start.33 = (bf16[64,768]{1,0:T(8,128)(2,1)}, bf16[64,768]{1,0:T(8,128)(2,1)S(1)}, u32[]{:S(2)}, u32[]{:S(2)}) collective-permute-start(bf16[64,768]{1,0:T(8,128)(2,1)} %get-tuple-element.36), channel_id=1, source_target_pairs={{0,8},{8,0},{16,24},{24,16},{1,9},{9,1},{17,25},{25,17},{2,10},{10... | collective-permute-start | bytes 294920 | tf_op jit(solution)/shard_map/ppermute | solution.py:39
  117.6 4.8 %copy-start.18 = (bf16[64,768]{1,0:T(8,128)(2,1)}, bf16[64,768]{1,0:T(8,128)(2,1)S(1)}, u32[]{:S(2)}) copy-start(bf16[64,768]{1,0:T(8,128)(2,1)S(1)} %collective-permute-done.31.refs_0_) | copy-start | bytes 294916
  126.0 18.8 %collective-permute-start.34 = (bf16[96,2048]{1,0:T(8,128)(2,1)}, bf16[96,2048]{1,0:T(8,128)(2,1)S(1)}, u32[]{:S(2)}, u32[]{:S(2)}) collective-permute-start(bf16[96,2048]{1,0:T(8,128)(2,1)} %get-tuple-element.39), channel_id=1, source_target_pairs={{0,1},{1,0},{2,3},{3,2},{4,5},{5,4},{6,7},{7,6},{8,9},{9,8},{10,11... | collective-permute-start | bytes 1179656 | tf_op jit(solution)/shard_map/ppermute | solution.py:39
  126.1 8.2 %collective-permute-start.41 = (bf16[64,768]{1,0:T(8,128)(2,1)S(1)}, bf16[64,768]{1,0:T(8,128)(2,1)S(1)}, u32[]{:S(2)}, u32[]{:S(2)}) collective-permute-start(bf16[64,768]{1,0:T(8,128)(2,1)S(1)} %get-tuple-element.47), channel_id=1, source_target_pairs={{0,24},{8,16},{16,8},{24,0},{1,25},{9,17},{17,9},{25,1},{2,26},{10... | collective-permute-start | bytes 294920 | tf_op jit(solution)/shard_map/ppermute | solution.py:39
  128.0 9.4 %collective-permute-start.40 = (bf16[64,768]{1,0:T(8,128)(2,1)S(1)}, bf16[64,768]{1,0:T(8,128)(2,1)S(1)}, u32[]{:S(2)}, u32[]{:S(2)}) collective-permute-start(bf16[64,768]{1,0:T(8,128)(2,1)S(1)} %get-tuple-element.48), channel_id=1, source_target_pairs={{0,16},{8,24},{16,0},{24,8},{1,17},{9,25},{17,1},{25,9},{2,18},{10... | collective-permute-start | bytes 294920 | tf_op jit(solution)/shard_map/ppermute | solution.py:39
  128.0 9.4 %collective-permute-start.39 = (bf16[64,768]{1,0:T(8,128)(2,1)S(1)}, bf16[64,768]{1,0:T(8,128)(2,1)S(1)}, u32[]{:S(2)}, u32[]{:S(2)}) collective-permute-start(bf16[64,768]{1,0:T(8,128)(2,1)S(1)} %get-tuple-element.49), channel_id=1, source_target_pairs={{0,8},{8,0},{16,24},{24,16},{1,9},{9,1},{17,25},{25,17},{2,10},{10... | collective-permute-start | bytes 294920 | tf_op jit(solution)/shard_map/ppermute | solution.py:39
  130.5 31.7 %all-to-all-start.1 = ((bf16[8,128,128]{2,1,0:T(8,128)(2,1)}), bf16[8,128,128]{2,1,0:T(8,128)(2,1)S(1)}, u32[]{:S(2)}, u32[]{:S(2)}) async-start(bf16[8,128,128]{2,1,0:T(8,128)(2,1)} %bitcast.36), calls=%async_computation.1 | async-start | bytes 524288 | tf_op jit(solution)/shard_map/all_to_all | solution.py:579
  140.4 8.7 %collective-permute-start.44 = (bf16[64,768]{1,0:T(8,128)(2,1)}, bf16[64,768]{1,0:T(8,128)(2,1)S(1)}, u32[]{:S(2)}, u32[]{:S(2)}) collective-permute-start(bf16[64,768]{1,0:T(8,128)(2,1)} %attend_sum.1.refs_0_), channel_id=1, source_target_pairs={{0,24},{8,16},{16,8},{24,0},{1,25},{9,17},{17,9},{25,1},{2,26},{10... | collective-permute-start | bytes 294920 | tf_op jit(solution)/shard_map/ppermute | solution.py:39
  142.3 9.1 %collective-permute-start.43 = (bf16[64,768]{1,0:T(8,128)(2,1)}, bf16[64,768]{1,0:T(8,128)(2,1)S(1)}, u32[]{:S(2)}, u32[]{:S(2)}) collective-permute-start(bf16[64,768]{1,0:T(8,128)(2,1)} %attend_sum.1.refs_0_), channel_id=1, source_target_pairs={{0,16},{8,24},{16,0},{24,8},{1,17},{9,25},{17,1},{25,9},{2,18},{10... | collective-permute-start | bytes 294920 | tf_op jit(solution)/shard_map/ppermute | solution.py:39
  142.3 11.6 %collective-permute-start.42 = (bf16[64,768]{1,0:T(8,128)(2,1)}, bf16[64,768]{1,0:T(8,128)(2,1)S(1)}, u32[]{:S(2)}, u32[]{:S(2)}) collective-permute-start(bf16[64,768]{1,0:T(8,128)(2,1)} %attend_sum.1.refs_0_), channel_id=1, source_target_pairs={{0,8},{8,0},{16,24},{24,16},{1,9},{9,1},{17,25},{25,17},{2,10},{10... | collective-permute-start | bytes 294920 | tf_op jit(solution)/shard_map/ppermute | solution.py:39
  147.6 11.9 %collective-permute-start.35 = (bf16[24,2048]{1,0:T(8,128)(2,1)}, bf16[24,2048]{1,0:T(8,128)(2,1)S(1)}, u32[]{:S(2)}, u32[]{:S(2)}) collective-permute-start(bf16[24,2048]{1,0:T(8,128)(2,1)} %get-tuple-element.41), channel_id=1, source_target_pairs={{0,2},{1,3},{2,0},{3,1},{4,6},{5,7},{6,4},{7,5},{8,10},{9,11},{10,... | collective-permute-start | bytes 294920 | tf_op jit(solution)/shard_map/ppermute | solution.py:39
  149.1 10.4 %collective-permute-start.36 = (bf16[24,2048]{1,0:T(8,128)(2,1)}, bf16[24,2048]{1,0:T(8,128)(2,1)S(1)}, u32[]{:S(2)}, u32[]{:S(2)}) collective-permute-start(bf16[24,2048]{1,0:T(8,128)(2,1)} %get-tuple-element.42), channel_id=1, source_target_pairs={{0,4},{1,5},{2,6},{3,7},{4,0},{5,1},{6,2},{7,3},{8,12},{9,13},{10,... | collective-permute-start | bytes 294920 | tf_op jit(solution)/shard_map/ppermute | solution.py:39
  151.4 8.1 %collective-permute-start.37 = (bf16[24,2048]{1,0:T(8,128)(2,1)}, bf16[24,2048]{1,0:T(8,128)(2,1)S(1)}, u32[]{:S(2)}, u32[]{:S(2)}) collective-permute-start(bf16[24,2048]{1,0:T(8,128)(2,1)} %get-tuple-element.43), channel_id=1, source_target_pairs={{0,6},{1,7},{2,4},{3,5},{4,2},{5,3},{6,0},{7,1},{8,14},{9,15},{10,... | collective-permute-start | bytes 294920 | tf_op jit(solution)/shard_map/ppermute | solution.py:39
  (23 other events, 47.4 us)
where the time goes:
time: 169 us; the launch traced here: 168 us
  starting transfers between devices  57.8 us (34%)
  Pallas kernels  54.1 us (32%)
  waiting for transfers between devices  43 us (25%)
  other arithmetic  6.73 us (4%)
  local copies, waits for them, and re-layouts  5.39 us (3%)
    ppermute x45, starting transfers between devices, swap(): return lax.ppermute(array, axis, [(i, i ^ mask) for i in range(size)])  49.8 us
    ppermute x45, waiting for transfers between devices, swap(): return lax.ppermute(array, axis, [(i, i ^ mask) for i in range(size)])  43 us
    pallas_call x2, Pallas kernels, backward_some(): pl.pallas_call(kernel, out_shape=tuple((shape_of((HEAD_DIM, lanes), BF16)...  12.9 us
    pallas_call x1, Pallas kernels, forward_all(): pl.pallas_call(kernel, out_shape=(shape_of((blocks, HEAD_DIM, lanes), F32...  6.77 us
    unnamed x80, local copies, waits for them, and re-layouts  5.37 us
    pallas_call x1, Pallas kernels, source_back(): pl.pallas_call(kernel, out_shape=shape_of((rows, width), F32), in_specs=[...  5.08 us
    pallas_call x1, Pallas kernels, project_grads(): pl.pallas_call(kernel, out_shape=(shape_of((blocks, HEAD_DIM, heads * cou...  5.04 us
    pallas_call x1, Pallas kernels, weight_grad(): pl.pallas_call(kernel, grid=(width // step,), in_specs=[part_spec] * bloc...  4.99 us
  transfers between devices with their start and end apart: 47, of which 15 were waited for; matrix products, arithmetic and copies ran while one was open for 4% of the time, Pallas kernels for 29%

commit v1 on v0

v1 whole, which is shorter than its diff:
```python
import jax
import jax.numpy as jnp
from jax import lax
from jax.experimental import pallas as pl
from jax.experimental.pallas import tpu as pltpu
from jax.sharding import PartitionSpec as P


HEAD_DIM = 64
KV_HEADS = 8
EPSILON = 1e-06
SCALE = HEAD_DIM**-0.5


F32 = jnp.float32
BF16 = jnp.bfloat16


def shape_of(shape, dtype):
    return jax.ShapeDtypeStruct(shape, dtype)


def normalize(matrix, gain_vector):
    widened = matrix.astype(F32)
    factor = lax.rsqrt(jnp.mean(widened * widened, axis=-1, keepdims=True) + EPSILON)
    return (widened * factor * gain_vector).astype(BF16)


def norm_back(matrix, gain_vector, upstream):
    widened = matrix.astype(F32)
    factor = lax.rsqrt(jnp.mean(widened * widened, axis=-1, keepdims=True) + EPSILON)
    weighted = upstream * gain_vector
    inner_sum = jnp.mean(weighted * widened, axis=-1, keepdims=True)
    return factor * weighted - widened * factor**3 * inner_sum


def swap(array, axis, mask):
    size = lax.axis_size(axis)
    return lax.ppermute(array, axis, [(i, i ^ mask) for i in range(size)])


def doubling(array, axis, bits):
    blocks = {0: array}
    for bit in bits:
        received = {key ^ bit: swap(value, axis, bit) for key, value in blocks.items()}
        blocks.update(received)
    return blocks


def dot(a, b):
    return jnp.dot(a, b, preferred_element_type=F32)


def nt_dot(a, b):
    return lax.dot_general(a, b, (((1,), (1,)), ((), ())), preferred_element_type=F32)


def tn_dot(a, b):
    return lax.dot_general(a, b, (((0,), (0,)), ((), ())), preferred_element_type=F32)


def chunk_for(rows):
    return 256 if rows % 256 == 0 else rows


def pad_to(extent, multiple):
    return -(-extent // multiple) * multiple


def transposed(matrix):
    rows, columns = matrix.shape
    more_rows, more_columns = pad_to(rows, 128) - rows, pad_to(columns, 128) - columns
    if more_columns:
        matrix = jnp.concatenate([matrix, jnp.zeros((rows, more_columns), F32)], axis=1)
    if more_rows:
        filler = jnp.zeros((more_rows, columns + more_columns), F32)
        matrix = jnp.concatenate([matrix, filler], axis=0)
    return matrix.T[:columns, :rows]


def stacked(matrix):
    heads = matrix.shape[0] // HEAD_DIM
    pieces = [matrix[g * HEAD_DIM : (g + 1) * HEAD_DIM, :] for g in range(heads)]
    return jnp.concatenate(pieces, axis=1) if heads > 1 else pieces[0]


def unstacked(matrix, heads):
    rows = matrix.shape[1] // heads
    pieces = [matrix[:, g * rows : (g + 1) * rows] for g in range(heads)]
    return jnp.concatenate(pieces, axis=0) if heads > 1 else pieces[0]


SCALAR = pl.BlockSpec(memory_space=pltpu.SMEM)
WHOLE = pl.BlockSpec(memory_space=pltpu.VMEM)
ROOM = 16 << 20


def resident(
    kernel,
    out_shape,
    *args,
    scalar=None,
    kept=None,
    loaded=0,
    fetched=0,
    far=0,
    scratch=(),
    room=ROOM,
    **costs,
):
    single = not isinstance(out_shape, tuple)
    outs = (out_shape,) if single else out_shape
    kept = len(outs) if kept is None else kept
    outs = tuple(
        (pltpu.VMEM if at < kept else pltpu.HBM)(out.shape, out.dtype)
        for at, out in enumerate(outs)
    )
    near = len(args) - far
    specs = [WHOLE] * near + [pl.BlockSpec(memory_space=pltpu.HBM)] * far
    held = near - fetched

    def placed(at, arg):
        if at < held - loaded:
            return pltpu.with_memory_space_constraint(arg, pltpu.VMEM)
        return arg if at < held else pltpu.with_memory_space_constraint(arg, pltpu.HBM)

    args = [placed(at, arg) for at, arg in enumerate(args)]
    if scalar is not None:
        args, specs = [scalar[None]] + args, [SCALAR] + specs
    return pl.pallas_call(
        kernel,
        out_shape=outs[0] if single else outs,
        in_specs=specs,
        out_specs=WHOLE if single else (WHOLE,) * len(outs),
        scratch_shapes=list(scratch),
        cost_estimate=pl.CostEstimate(
            flops=costs.get("flops", 1 << 20),
            bytes_accessed=costs.get("moved", 1 << 20),
            transcendentals=costs.get("exps", 0),
        ),
        compiler_params=pltpu.CompilerParams(vmem_limit_bytes=room),
    )(*args)


def split_norm(tp_at, source_rows, gain, weight_rows, tp_count, carried):
    rows, width = source_rows.shape
    half = width // 2
    masks = range(0, tp_count, 2)
    count = len(carried)
    if weight_rows % 128:
        normed = normalize(source_rows, gain)

        def columns(parity):
            return jnp.concatenate(
                [
                    lax.dynamic_slice_in_dim(
                        normed, (tp_at ^ m ^ parity) * weight_rows, weight_rows, 1
                    )
                    for m in masks
                ],
                axis=1,
            )

        return columns(0), columns(1), *carried

    def kernel(at_ref, rows_far, gain_far, *refs):
        far_refs, (own_ref, other_ref), near_refs = refs[:count], refs[count : count + 2], refs[count + 2 : -3]
        rows_ref, gain_ref, done = refs[-3:]
        pairs = [(rows_far, rows_ref), (gain_far, gain_ref), *zip(far_refs, near_refs)]
        copies = [
            pltpu.make_async_copy(source, target, done.at[at])
            for at, (source, target) in enumerate(pairs)
        ]
        for copy in copies:
            copy.start()
        copies[0].wait()
        copies[1].wait()
        widened = rows_ref[...].astype(F32)
        factor = lax.rsqrt(jnp.mean(widened * widened, axis=-1, keepdims=True) + EPSILON)
        for parity, out_ref in ((0, own_ref), (1, other_ref)):
            for place, m in enumerate(masks):
                start = pl.multiple_of((at_ref[0] ^ (m + parity)) * weight_rows, 128)
                at = pl.ds(start, weight_rows)
                piece = rows_ref[:, at].astype(F32) * factor * gain_ref[:, at]
                out_ref[:, place * weight_rows : (place + 1) * weight_rows] = piece.astype(BF16)
        for copy in copies[2:]:
            copy.wait()

    outs = (shape_of((rows, half), BF16), shape_of((rows, half), BF16))
    outs += tuple(shape_of(array.shape, array.dtype) for array in carried)
    return resident(
        kernel,
        outs,
        source_rows,
        gain[None],
        *carried,
        scalar=tp_at,
        far=2 + count,
        scratch=[
            pltpu.VMEM((rows, width), BF16),
            pltpu.VMEM((1, width), F32),
            pltpu.SemaphoreType.DMA((2 + count,)),
        ],
        flops=8 * rows * width,
    )


def project_some(own, other, places, weights):
    rows = own.shape[0]
    weight_rows, kv_width = weights[0][0].shape
    counts = [len(kind) for kind in weights]
    flat = [block for kind in weights for block in kind]

    def kernel(own_ref, other_ref, *refs):
        block_refs, out_refs = refs[: len(flat)], refs[len(flat) :]
        lhs = jnp.concatenate([own_ref[...], other_ref[...]], axis=0)
        for kind, out_ref in enumerate(out_refs):
            start = sum(counts[:kind])
            total = None
            for place, ref in zip(places[kind], block_refs[start : start + counts[kind]]):
                term = dot(lhs[:, place * weight_rows : (place + 1) * weight_rows], ref[...])
                total = term if total is None else total + term
            out_ref[...] = total

    outs = (shape_of((2 * rows, kv_width), F32),) * 2
    flops = 4 * rows * len(flat) * weight_rows * kv_width
    return resident(kernel, outs, own, other, *flat, flops=flops)


def project_rest(own, other, places, early, weights):
    rows = own.shape[0]
    weight_rows, kv_width = weights[0][0].shape
    counts = [len(kind) for kind in weights]
    flat = [block for kind in weights for block in kind]

    def kernel(own_ref, other_ref, *refs):
        early_refs, block_refs, (near_ref, far_ref) = refs[:2], refs[2:-2], refs[-2:]
        lhs = jnp.concatenate([own_ref[...], other_ref[...]], axis=0)
        sums = []
        for kind in range(2):
            total = early_refs[kind][...]
            start = sum(counts[:kind])
            for place, ref in zip(places[kind], block_refs[start : start + counts[kind]]):
                columns = lhs[:, place * weight_rows : (place + 1) * weight_rows]
                total = total + dot(columns, ref[...])
            sums.append(total)
        for head in range(KV_HEADS):
            at = slice(head * HEAD_DIM, (head + 1) * HEAD_DIM)
            packed = jnp.concatenate([sums[0][:, at], sums[1][:, at]], axis=1)
            near_ref[head] = packed[:rows]
            far_ref[head] = packed[rows:]

    outs = (
        shape_of((KV_HEADS, rows, 2 * HEAD_DIM), F32),
        shape_of((KV_HEADS, rows, 2 * HEAD_DIM), F32),
    )
    return resident(
        kernel, outs, own, other, *early, *flat, flops=4 * rows * len(flat) * weight_rows * kv_width
    )


def stack(arrays, lead=()):
    lead = lead or (len(arrays),)

    def kernel(*refs):
        for at, ref in enumerate(refs[:-1]):
            place = (at // lead[1], at % lead[1]) if len(lead) == 2 else (at,)
            refs[-1][place] = ref[...]

    out = shape_of((*lead, *arrays[0].shape), arrays[0].dtype)
    return resident(kernel, out, *arrays, kept=0, loaded=len(arrays))


def add_parts(own, theirs):
    def kernel(own_ref, theirs_ref, out_ref):
        out_ref[...] = (own_ref[...] + theirs_ref[...]).astype(BF16)

    return resident(kernel, shape_of(own.shape, BF16), own, theirs)


def pack_target(target_rows, cotangent, gain):
    def kernel(rows_far, gain_far, cot_far, out_ref, rows_ref, gain_ref, done):
        pairs = ((rows_far, rows_ref), (gain_far, gain_ref), (cot_far, out_ref.at[1]))
        copies = [
            pltpu.make_async_copy(source, target, done.at[at])
            for at, (source, target) in enumerate(pairs)
        ]
        for copy in copies:
            copy.start()
        copies[0].wait()
        copies[1].wait()
        out_ref[0] = normalize(rows_ref[...], gain_ref[...])
        copies[2].wait()

    return resident(
        kernel,
        shape_of((2, *target_rows.shape), BF16),
        target_rows,
        gain[None],
        cotangent,
        far=3,
        scratch=[
            pltpu.VMEM(target_rows.shape, BF16),
            pltpu.VMEM((1, target_rows.shape[1]), F32),
            pltpu.SemaphoreType.DMA((3,)),
        ],
    )


def project_target(pieces, query_weight, out_weight):
    count = sum(piece.shape[1] for piece in pieces)
    heads = query_weight.shape[1] // HEAD_DIM

    def kernel(*refs):
        piece_refs, (query_ref, weight_ref, out_ref, cot_ref) = refs[:-4], refs[-4:]
        rows = jnp.concatenate([ref[0] for ref in piece_refs], axis=0)
        queries = stacked(transposed(dot(rows, query_ref[...]))).astype(BF16)
        out_ref[0:HEAD_DIM, :] = queries * jnp.asarray(SCALE, BF16)
        cot = jnp.concatenate([ref[1] for ref in piece_refs], axis=0)
        cot_ref[...] = cot
        out_ref[HEAD_DIM:, :] = stacked(nt_dot(weight_ref[...], cot)).astype(BF16)

    out = (
        shape_of((2 * HEAD_DIM, heads * count), BF16),
        shape_of((count, pieces[0].shape[2]), BF16),
    )
    flops = 4 * count * query_weight.size
    return resident(kernel, out, *pieces, query_weight, out_weight, kept=0, flops=flops)


def gather_cotangents(pieces):
    blocks, piece_rows, width = pieces[0].shape
    count = piece_rows * len(pieces)

    def kernel(*refs):
        piece_refs, out_ref = (refs[-2], *refs[:-2]), refs[-1]
        for block in range(blocks):
            rows = jnp.concatenate([ref[block] for ref in piece_refs], axis=0)
            out_ref[block * count : (block + 1) * count, :] = rows

    out = shape_of((blocks * count, width), BF16)
    return resident(kernel, out, *pieces[1:], pieces[0], kept=0, fetched=1)


def forward_all(pairs, kv):
    blocks = len(pairs)
    lanes = pairs[0].shape[1]
    rows = kv.shape[0]
    chunk = chunk_for(rows)

    def kernel(*refs):
        pair_refs, kv_ref = refs[:blocks], refs[blocks]
        out_ref, stat_ref, *score_refs = refs[blocks + 1 :]
        zeros = jnp.zeros((HEAD_DIM, lanes), BF16)
        for block, pair_ref in enumerate(pair_refs):
            query = jnp.concatenate([pair_ref[0:HEAD_DIM, :], zeros], axis=0)
            score_ref = score_refs[block]
            peak = jnp.full((8, lanes), -jnp.inf, F32)
            for start in range(0, rows, chunk):
                scores = dot(kv_ref[start : start + chunk, :], query)
                score_ref[start : start + chunk, :] = scores
                peak = jnp.maximum(peak, jnp.max(scores.reshape(chunk // 8, 8, lanes), axis=0))
            row_max = jnp.max(peak, axis=0, keepdims=True)
            total = jnp.zeros((8, lanes), F32)
            summed = jnp.zeros((HEAD_DIM, lanes), F32)
            for start in range(0, rows, chunk):
                weights = jnp.exp(score_ref[start : start + chunk, :] - row_max)
                total = total + jnp.sum(weights.reshape(chunk // 8, 8, lanes), axis=0)
                values = kv_ref[start : start + chunk, HEAD_DIM:]
                summed = summed + tn_dot(values, weights.astype(BF16))
            total = jnp.sum(total, axis=0, keepdims=True)
            part = summed / total
            out_ref[block] = part
            stat_ref[2 * block : 2 * block + 1, :] = row_max + jnp.log(total)
            stat_ref[2 * block + 1 : 2 * block + 2, :] = jnp.sum(
                pair_ref[HEAD_DIM:, :].astype(F32) * part, axis=0, keepdims=True
            )

    outs = (shape_of((blocks, HEAD_DIM, lanes), F32), shape_of((2 * blocks, lanes), F32))
    outs += (shape_of((rows, lanes), F32),) * blocks
    return resident(
        kernel,
        outs,
        *pairs,
        kv,
        room=ROOM,
        flops=8 * blocks * rows * lanes * HEAD_DIM,
        exps=blocks * rows * lanes,
    )


def combine_stats(stats, parts):
    blocks, _, lanes = parts.shape

    def kernel(*refs):
        stat_refs, part_ref = refs[:blocks], refs[blocks]
        out_ref, *share_refs = refs[blocks + 1 :]
        for block in range(blocks):
            logs, deltas = [], []
            for peer, stat_ref in enumerate(stat_refs):
                at = 2 * (block ^ peer)
                logs.append(stat_ref[at : at + 1, :])
                deltas.append(stat_ref[at + 1 : at + 2, :])
            peak = logs[0]
            for log in logs[1:]:
                peak = jnp.maximum(peak, log)
            shares = [jnp.exp(log - peak) for log in logs]
            total = shares[0]
            delta = shares[0] * deltas[0]
            for share, term in zip(shares[1:], deltas[1:]):
                total = total + share
                delta = delta + share * term
            out_ref[2 * block : 2 * block + 1, :] = peak + jnp.log(total)
            out_ref[2 * block + 1 : 2 * block + 2, :] = delta / total
            share_refs[block][...] = (part_ref[block] * (shares[0] / total)).astype(BF16)

    outs = (shape_of((2 * blocks, lanes), F32),)
    outs += (shape_of((HEAD_DIM, lanes), BF16),) * blocks
    return resident(kernel, outs, *stats, parts, kept=1)


def backward_some(order, pairs, scores, stats, kv, sums, slots):
    count = len(order)
    lanes = pairs[0].shape[1]
    rows = kv.shape[0]
    chunk = chunk_for(rows)
    started = [] if sums is None else [sums]

    def kernel(*refs):
        pair_refs, score_refs = refs[:count], refs[count : 2 * count]
        stat_ref, kv_ref = refs[2 * count : 2 * count + 2]
        start_refs = refs[2 * count + 2 : 2 * count + 2 + len(started)]
        outs = refs[2 * count + 2 + len(started) : -1]
        sum_ref = refs[-1]
        zeros = jnp.zeros((HEAD_DIM, lanes), BF16)
        for place, block in enumerate(order):
            query = jnp.concatenate([pair_refs[place][0:HEAD_DIM, :], zeros], axis=0)
            grad = jnp.concatenate([zeros, pair_refs[place][HEAD_DIM:, :]], axis=0)
            log_total = stat_ref[2 * block : 2 * block + 1, :]
            delta = stat_ref[2 * block + 1 : 2 * block + 2, :]
            d_query = jnp.zeros((HEAD_DIM, lanes), F32)
            for start in range(0, rows, chunk):
                at = slice(start, start + chunk)
                pair = kv_ref[at, :]
                probs = jnp.exp(score_refs[place][at, :] - log_total)
                d_scores = (probs * (dot(pair, grad) - delta)).astype(BF16)
                terms = nt_dot(d_scores, query) + nt_dot(probs.astype(BF16), grad)
                if place:
                    terms = terms + sum_ref[at, :]
                elif started:
                    terms = terms + start_refs[0][at, :]
                sum_ref[at, :] = terms
                d_query = d_query + tn_dot(pair[:, :HEAD_DIM], d_scores)
            outs[1 + place][...] = (d_query * SCALE).astype(BF16)
        outs[0][...] = sum_ref[...].astype(outs[0].dtype).reshape(outs[0].shape)

    if slots:
        sum_shape = shape_of((slots, rows // slots, 2 * HEAD_DIM), BF16)
    else:
        sum_shape = shape_of((rows, 2 * HEAD_DIM), F32)
    outs = resident(
        kernel,
        (sum_shape,) + (shape_of((HEAD_DIM, lanes), BF16),) * count,
        *[pairs[block] for block in order],
        *[scores[block] for block in order],
        stats,
        kv,
        *started,
        kept=0 if slots else 1,
        scratch=[pltpu.VMEM((rows, 2 * HEAD_DIM), F32)],
        flops=20 * count * rows * lanes * HEAD_DIM,
        exps=count * rows * lanes,
    )
    return outs[1:], outs[0]


def query_back(parts, query_weight, heads):
    width = query_weight.shape[0]
    count = parts[0].shape[1] // heads
    half = count // 2

    def kernel(*refs):
        part_refs, (weight_ref, last_ref, own_ref, other_ref) = refs[:-4], refs[-4:]
        total = part_refs[0][...].astype(F32)
        for part_ref in (*part_refs[1:], last_ref):
            total = total + part_ref[...].astype(F32)
        grad = transposed(unstacked(total, heads)).astype(BF16)
        upstream = nt_dot(grad, weight_ref[...])
        own_ref[...] = upstream[:half]
        other_ref[...] = upstream[half:].astype(BF16)

    outs = (shape_of((half, width), F32), shape_of((half, width), BF16))
    flops = 2 * count * query_weight.size
    return resident(kernel, outs, *parts[:-1], query_weight, parts[-1], fetched=1, flops=flops)


def share_rows(own, theirs, count):
    rows, width = own.shape
    piece = rows // count

    def kernel(own_ref, theirs_ref, kept_ref, *out_refs):
        kept_ref[...] = own_ref[:piece, :] + theirs_ref[:piece, :].astype(F32)
        for place, out_ref in enumerate(out_refs):
            at = slice((place + 1) * piece, (place + 2) * piece)
            out_ref[...] = (own_ref[at, :] + theirs_ref[at, :].astype(F32)).astype(BF16)

    outs = (shape_of((piece, width), F32),) + (shape_of((piece, width), BF16),) * (count - 1)
    return resident(kernel, outs, own, theirs, kept=0)


def target_finish(kept, received, target_rows, cotangent, gain):
    def kernel(*refs):
        received_refs, (kept_ref, rows_ref, cot_ref, gain_ref, out_ref) = refs[:-5], refs[-5:]
        total = kept_ref[...]
        for ref in received_refs:
            total = total + ref[...].astype(F32)
        back = norm_back(rows_ref[...], gain_ref[...], total)
        out_ref[...] = cot_ref[...].astype(F32) + back

    out = shape_of(kept.shape, F32)
    args = (*received, kept, target_rows, cotangent, gain[None])
    return resident(kernel, out, *args, kept=0, loaded=len(args) - 4, fetched=4)


def attend_sum(parts):
    def kernel(*refs):
        out_ref = refs[-1]
        total = refs[0][...].astype(F32)
        for ref in refs[1:-1]:
            total = total + ref[...].astype(F32)
        out_ref[...] = total.astype(BF16)

    return resident(
        kernel, shape_of(parts[0].shape, BF16), *parts[1:], parts[0], loaded=len(parts) - 1, fetched=1
    )


def weight_grad(attended, cot_parts, heads):
    blocks = len(attended)
    count, width = cot_parts[0].shape
    half = count // 2
    step = 512 if width % 512 == 0 else width

    def kernel(*refs):
        attended_refs, cot_refs, (out_ref, wide_ref) = refs[:blocks], refs[blocks:-2], refs[-2:]

        @pl.when(pl.program_id(0) == 0)
        def _():
            for block, attended_ref in enumerate(attended_refs):
                part = unstacked(attended_ref[...].astype(F32), heads).astype(BF16)
                if not block:
                    wide_ref[:, 0:count] = part
                for core in range(2) if block else ():
                    start = count + (core * (blocks - 1) + block - 1) * half
                    wide_ref[:, start : start + half] = part[:, core * half : (core + 1) * half]

        rows = jnp.concatenate([ref[...] for ref in cot_refs], axis=0)
        out_ref[...] = dot(wide_ref[...], rows)

    specs = [pl.BlockSpec(attended[0].shape, lambda i: (0, 0))] * blocks
    specs += [pl.BlockSpec((part.shape[0], step), lambda i: (0, i)) for part in cot_parts]
    return pl.pallas_call(
        kernel,
        grid=(width // step,),
        in_specs=specs,
        out_specs=pl.BlockSpec((heads * HEAD_DIM, step), lambda i: (0, i)),
        out_shape=shape_of((heads * HEAD_DIM, width), F32),
        scratch_shapes=[pltpu.VMEM((heads * HEAD_DIM, blocks * count), BF16)],
        cost_estimate=pl.CostEstimate(
            flops=2 * heads * HEAD_DIM * blocks * count * width,
            bytes_accessed=2 * blocks * count * width,
            transcendentals=0,
        ),
        compiler_params=pltpu.CompilerParams(vmem_limit_bytes=ROOM),
        name="weight_grad",
    )(*attended, *[pltpu.with_memory_space_constraint(part, pltpu.HBM) for part in cot_parts])


def source_back(tp_at, back, held, others, source_rows, gain):
    rows, width = source_rows.shape
    _, count, weight_rows, _ = held.shape

    def kernel(at_ref, back_ref, held_ref, other_ref, rows_ref, gain_ref, out_ref):
        key_grad = jnp.concatenate([back_ref[h][:, :HEAD_DIM] for h in range(KV_HEADS)], axis=1)
        value_grad = jnp.concatenate([back_ref[h][:, HEAD_DIM:] for h in range(KV_HEADS)], axis=1)
        inner = jnp.zeros((rows, 1), F32)
        square = jnp.zeros((rows, 1), F32)
        for place in range(count):
            for parity in (0, 1):
                from_ref = other_ref if parity else held_ref
                key, value = from_ref[0, place], from_ref[1, place]
                start = pl.multiple_of((at_ref[0] ^ (2 * place + parity)) * weight_rows, 128)
                at = pl.ds(start, weight_rows)
                upstream = nt_dot(key_grad, key) + nt_dot(value_grad, value)
                weighted = upstream * gain_ref[:, at]
                widened = rows_ref[:, at].astype(F32)
                inner = inner + jnp.sum(weighted * widened, axis=-1, keepdims=True)
                square = square + jnp.sum(widened * widened, axis=-1, keepdims=True)
                out_ref[:, at] = weighted
        factor = lax.rsqrt(square / width + EPSILON)
        pull = factor**3 * (inner / width)
        out_ref[...] = factor * out_ref[...] - rows_ref[...].astype(F32) * pull

    return resident(
        kernel,
        shape_of((rows, width), F32),
        back,
        held,
        others,
        source_rows,
        gain[None],
        scalar=tp_at,
        kept=0,
        loaded=3,
        fetched=2,
        flops=4 * rows * width * KV_HEADS * HEAD_DIM,
    )


def source_back_plain(tp_at, back, held, others, source_rows, gain):
    rows, width = source_rows.shape
    _, count, weight_rows, _ = held.shape
    fulls = []
    for kind in range(2):
        full = jnp.zeros((width, KV_HEADS * HEAD_DIM), BF16)
        for place in range(count):
            start = (tp_at ^ (2 * place)) * weight_rows
            full = lax.dynamic_update_slice_in_dim(full, held[kind, place], start, 0)
            start = (tp_at ^ (2 * place + 1)) * weight_rows
            full = lax.dynamic_update_slice_in_dim(full, others[kind, place], start, 0)
        fulls.append(full)
    turned = back.transpose(1, 0, 2)
    key_grad = turned[:, :, :HEAD_DIM].reshape(rows, KV_HEADS * HEAD_DIM)
    value_grad = turned[:, :, HEAD_DIM:].reshape(rows, KV_HEADS * HEAD_DIM)
    total = nt_dot(key_grad, fulls[0]) + nt_dot(value_grad, fulls[1])
    return norm_back(source_rows, gain, total)


def body(
    target_rows,
    source_rows,
    target_gain,
    source_gain,
    query_weight,
    key_weight,
    value_weight,
    out_weight,
    out_cotangent,
):
    tp_count = lax.axis_size("tp")
    sp_count = lax.axis_size("sp")
    tp_at = lax.axis_index("tp").astype(jnp.int32)
    own_source = source_rows.shape[0]
    weight_rows = key_weight.shape[0]
    heads = query_weight.shape[1] // HEAD_DIM
    copies = max(1, tp_count // KV_HEADS)
    chips = tp_count // 2
    chip_bits = [1 << b for b in range(1, tp_count.bit_length() - 1)]
    near, far = chip_bits[: len(chip_bits) // 2], chip_bits[len(chip_bits) // 2 :]
    chip_masks = range(0, tp_count, 2)

    packed_t = pack_target(target_rows, out_cotangent, target_gain)
    own_part, other_part, query_near, out_near = split_norm(
        tp_at, source_rows, source_gain, weight_rows, tp_count, (query_weight, out_weight)
    )

    near_rows = [packed_t if m == 0 else swap(packed_t, "tp", m) for m in chip_masks]
    far_rows = [swap(rows, "tp", 1) for rows in near_rows]
    own_pieces = near_rows + far_rows
    pair, own_cot = project_target(own_pieces, query_near, out_near)
    pairs = [pair if k == 0 else swap(pair, "sp", k) for k in range(sp_count)]

    key_found = doubling(key_weight, "tp", far + near)
    value_found = doubling(value_weight, "tp", near + far)
    key_blocks = [key_found[m] for m in chip_masks]
    value_blocks = [value_found[m] for m in chip_masks]

    other_part = swap(other_part, "tp", 1)
    places = [], []
    rest = [], []
    for place, mask in enumerate(chip_masks):
        for kind, late_bits in enumerate((near, far)):
            group = rest if any(mask & bit for bit in late_bits) else places
            group[kind].append(place)
    soon = [[key_blocks[p] for p in places[0]], [value_blocks[p] for p in places[1]]]
    early = project_some(own_part, other_part, places, soon)
    late = [[key_blocks[p] for p in rest[0]], [value_blocks[p] for p in rest[1]]]
    own_sum, other_sum = project_rest(own_part, other_part, rest, early, late)
    held = stack(key_blocks + value_blocks, (2, chips))
    other_sum = swap(other_sum, "tp", 1)
    packed = add_parts(own_sum, other_sum)
    packed = jnp.repeat(packed, copies, axis=0)
    kv = lax.all_to_all(packed, "tp", split_axis=0, concat_axis=0, tiled=True)
    kv = kv.reshape(tp_count * own_source, 2 * HEAD_DIM)

    cot_z = [swap(out_cotangent, "sp", k) for k in range(1, sp_count)]
    cot_z = stack(cot_z)
    cot_near = [cot_z if m == 0 else swap(cot_z, "tp", m) for m in chip_masks]
    near_cot = gather_cotangents(cot_near)
    cot_all = [own_cot, near_cot, swap(near_cot, "tp", 1)]

    parts, own_stats, *scores = forward_all(pairs, kv)
    stats = [own_stats if k == 0 else swap(own_stats, "sp", k) for k in range(sp_count)]
    stats, *shares = combine_stats(stats, parts)
    order = list(range(sp_count // 2, sp_count)) + list(range(sp_count // 2 - 1, -1, -1))
    first, second = order[: sp_count // 2], order[sp_count // 2 :]
    found, kv_sums = backward_some(first, pairs, scores, stats, kv, None, 0)
    query_parts = [swap(part, "sp", k) for k, part in zip(first, found)]
    found, kv_sums = backward_some(second, pairs, scores, stats, kv, kv_sums, tp_count)
    query_parts += [part if k == 0 else swap(part, "sp", k) for k, part in zip(second, found)]

    others = swap(held, "tp", 1)
    back = lax.all_to_all(
        kv_sums,
        "tp",
        split_axis=0,
        concat_axis=0,
        tiled=True,
    )
    if copies > 1:
        back = back.reshape(KV_HEADS, copies, own_source, 2 * HEAD_DIM)
        back = back.astype(F32).sum(1).astype(BF16)
    finish = source_back_plain if weight_rows % 128 else source_back
    source_grad = finish(tp_at, back, held, others, source_rows, source_gain)

    mine, theirs = query_back(query_parts, query_near, heads)
    theirs = swap(theirs, "tp", 1)
    kept, *given = share_rows(mine, theirs, chips)
    received = [swap(piece, "tp", m) for m, piece in zip(list(chip_masks)[1:], given)]
    target_grad = target_finish(kept, received, target_rows, out_cotangent, target_gain)

    attended = shares[:1] + [swap(shares[k], "sp", k) for k in range(1, sp_count)]
    attended = attend_sum(attended)
    attended = [attended if k == 0 else swap(attended, "sp", k) for k in range(sp_count)]
    out_weight_grad = weight_grad(attended, cot_all, heads)
    return (target_grad, source_grad, out_weight_grad)


def solution(mesh):
    return jax.shard_map(
        body,
        mesh=mesh,
        in_specs=(
            P(("sp", "tp"), None),
            P(("sp", "tp"), None),
            P(),
            P(),
            P(None, "tp"),
            P("tp", None),
            P("tp", None),
            P("tp", None),
            P(("sp", "tp"), None),
        ),
        out_specs=(P(("sp", "tp"), None), P(("sp", "tp"), None), P("tp", None)),
        check_vma=False,
    )
```

time: 169 us -> 143 us (0.85)
  Pallas kernels: 54.1 us -> 38.8 us
  other arithmetic: 6.73 us -> 0 us
  waiting for transfers between devices: 43 us -> 40.1 us
  starting transfers between devices: 57.8 us -> 56 us
    pallas_call x14 -> x19, Pallas kernels: 54.1 us -> 38.8 us  [the longest x18 33.6 us: resident(): pl.pallas_call(kernel, out_shape=outs[0] if single else outs, in_specs=sp...]
    ppermute x45 -> x42, waiting for transfers between devices: 43 us -> 40.1 us  [swap(): return lax.ppermute(array, axis, [(i, i ^ mask) for i in range(size)])]
    another operation x4 -> x0, other arithmetic: 2.87 us -> none  [the longest x3 2.82 us: body(): others = jnp.stack([jnp.stack(key_blocks), jnp.stack(value_blocks)])]
    convert_element_type x2 -> x0, other arithmetic: 2.83 us -> none  [the longest x1 1.82 us: body(): packed = (own_sum + swap(other_sum, 'tp', 1)).astype(BF16)]
    unnamed x80 -> x34, local copies, waits for them, and re-layouts: 5.37 us -> 6.71 us
    ppermute x45 -> x42, starting transfers between devices: 49.8 us -> 48.6 us  [swap(): return lax.ppermute(array, axis, [(i, i ^ mask) for i in range(size)])]
  transfers between devices with their start and end apart: 47 -> 44, of which waited for: 15 -> 14; matrix products, arithmetic and copies ran while one was open for 4% -> 0% of each run, Pallas kernels for 29% -> 24%
where the time goes in v1:
time: 143 us
  starting transfers between devices  56 us (39%)
  waiting for transfers between devices  40.1 us (28%)
  Pallas kernels  38.8 us (27%)
  local copies, waits for them, and re-layouts  6.71 us (5%)
    ppermute x42, starting transfers between devices, swap(): return lax.ppermute(array, axis, [(i, i ^ mask) for i in range(size)])  48.6 us
    ppermute x42, waiting for transfers between devices, swap(): return lax.ppermute(array, axis, [(i, i ^ mask) for i in range(size)])  40.1 us
    pallas_call x18, Pallas kernels, resident(): pl.pallas_call(kernel, out_shape=outs[0] if single else outs, in_specs=sp...  33.6 us
    unnamed x34, local copies, waits for them, and re-layouts  6.71 us
    pallas_call x1, Pallas kernels, weight_grad(): pl.pallas_call(kernel, grid=(width // step,), in_specs=specs, out_specs=p...  5.2 us
    all_to_all x1, starting transfers between devices, body(): lax.all_to_all(kv_sums, 'tp', split_axis=0, concat_axis=0, tiled=True)  3.85 us
    all_to_all x1, starting transfers between devices, body(): kv = lax.all_to_all(packed, 'tp', split_axis=0, concat_axis=0, tiled=True)  3.59 us
  transfers between devices with their start and end apart: 44, of which 14 were waited for; matrix products, arithmetic and copies ran while one was open for 0% of the time, Pallas kernels for 24%

profile of v1, /device:TPU:0, one launch (start us, length us, event | category | flops | bytes accessed | tf_op | source)
XLA Modules:
  0.0 142.5 jit_solution(12035342598257278007)
XLA Ops:
  0.7 3.1 %collective-permute-start.11 = (bf16[256,512]{1,0:T(8,128)(2,1)}, bf16[256,512]{1,0:T(8,128)(2,1)S(1)}, u32[]{:S(2)}, u32[]{:S(2)}) collective-permute-start(bf16[256,512]{1,0:T(8,128)(2,1)} %refs_0_.5), channel_id=1, source_target_pairs={{0,4},{1,5},{2,6},{3,7},{4,0},{5,1},{6,2},{7,3},{8,12},{9,13},{10,... | collective-permute-start | bytes 786440 | tf_op jit(solution)/shard_map/ppermute | solution.py:39
  3.7 1.5 %collective-permute-start.12 = (bf16[256,512]{1,0:T(8,128)(2,1)}, bf16[256,512]{1,0:T(8,128)(2,1)S(1)}, u32[]{:S(2)}, u32[]{:S(2)}) collective-permute-start(bf16[256,512]{1,0:T(8,128)(2,1)} %refs_4_.3), channel_id=1, source_target_pairs={{0,2},{1,3},{2,0},{3,1},{4,6},{5,7},{6,4},{7,5},{8,10},{9,11},{10,... | collective-permute-start | bytes 786440 | tf_op jit(solution)/shard_map/ppermute | solution.py:39
  5.2 1.8 %shard_map.113 = (bf16[128,1024]{1,0:T(8,128)(2,1)S(1)}, bf16[128,1024]{1,0:T(8,128)(2,1)S(1)}, bf16[2048,256]{1,0:T(8,128)(2,1)S(1)}, bf16[256,2048]{1,0:T(8,128)(2,1)S(1)}) custom-call(s32[1]{0:T(128)} %bitcast.1.at_ref, bf16[128,2048]{1,0:T(8,128)(2,1)} %rows_ref.1, f32[1,2048]{1,0:T(1,128)} %bitcast.7, bf16[2048,256]{1,0:T(8,128)(2,1)} %refs_0_.3, ...), custom_call_target="tpu_custom_call" | custom-call | flops 2097152 | bytes 1048576 | tf_op jit(solution)/shard_map/pallas_call | solution.py:130
  7.7 3.0 %collective-permute-done.11.refs_1_.refs_2_ = bf16[256,512]{1,0:T(8,128)(2,1)S(1)} collective-permute-done((bf16[256,512]{1,0:T(8,128)(2,1)}, bf16[256,512]{1,0:T(8,128)(2,1)S(1)}, u32[]{:S(2)}, u32[]{:S(2)}) %collective-permute-start.11) | collective-permute-done | bytes 262176 | tf_op jit(solution)/shard_map/ppermute | solution.py:39
  10.7 1.4 %collective-permute-start.14 = (bf16[256,512]{1,0:T(8,128)(2,1)S(1)}, bf16[256,512]{1,0:T(8,128)(2,1)S(1)}, u32[]{:S(2)}, u32[]{:S(2)}) collective-permute-start(bf16[256,512]{1,0:T(8,128)(2,1)S(1)} %collective-permute-done.11.refs_1_.refs_2_), channel_id=1, source_target_pairs={{0,2},{1,3},{2,0},{3,1},{4,6},{5,7},{6,4},{7,5},{8,10},{9,11},{10,... | collective-permute-start | bytes 786440 | tf_op jit(solution)/shard_map/ppermute | solution.py:39
  12.1 0.9 collective-permute-done.12.refs_3_.refs_5_
  13.1 1.4 %collective-permute-start.16 = (bf16[256,512]{1,0:T(8,128)(2,1)S(1)}, bf16[256,512]{1,0:T(8,128)(2,1)S(1)}, u32[]{:S(2)}, u32[]{:S(2)}) collective-permute-start(bf16[256,512]{1,0:T(8,128)(2,1)S(1)} %collective-permute-done.12.refs_3_.refs_5_), channel_id=1, source_target_pairs={{0,4},{1,5},{2,6},{3,7},{4,0},{5,1},{6,2},{7,3},{8,12},{9,13},{10,... | collective-permute-start | bytes 786440 | tf_op jit(solution)/shard_map/ppermute | solution.py:39
  14.5 1.6 %collective-permute-start.35 = (bf16[24,2048]{1,0:T(8,128)(2,1)}, bf16[24,2048]{1,0:T(8,128)(2,1)S(1)}, u32[]{:S(2)}, u32[]{:S(2)}) collective-permute-start(bf16[24,2048]{1,0:T(8,128)(2,1)} %refs_5_.1), channel_id=1, source_target_pairs={{0,8},{8,0},{16,24},{24,16},{1,9},{9,1},{17,25},{25,17},{2,10},{10... | collective-permute-start | bytes 294920 | tf_op jit(solution)/shard_map/ppermute | solution.py:39
  16.1 2.6 %collective-permute-done.13.refs_2_.refs_1_ = bf16[256,512]{1,0:T(8,128)(2,1)S(1)} collective-permute-done((bf16[256,512]{1,0:T(8,128)(2,1)S(1)}, bf16[256,512]{1,0:T(8,128)(2,1)S(1)}, u32[]{:S(2)}, u32[]{:S(2)}) %collective-permute-start.13) | collective-permute-done | bytes 262176 | tf_op jit(solution)/shard_map/ppermute | solution.py:39
  18.7 2.6 %collective-permute-start.36 = (bf16[24,2048]{1,0:T(8,128)(2,1)}, bf16[24,2048]{1,0:T(8,128)(2,1)S(1)}, u32[]{:S(2)}, u32[]{:S(2)}) collective-permute-start(bf16[24,2048]{1,0:T(8,128)(2,1)} %refs_5_.1), channel_id=1, source_target_pairs={{0,16},{8,24},{16,0},{24,8},{1,17},{9,25},{17,1},{25,9},{2,18},{10... | collective-permute-start | bytes 294920 | tf_op jit(solution)/shard_map/ppermute | solution.py:39
  21.3 1.3 collective-permute-start.37
  22.7 1.0 shard_map.112.refs_0_
  23.7 1.6 %collective-permute-start = (bf16[2,24,2048]{2,1,0:T(8,128)(2,1)S(1)}, bf16[2,24,2048]{2,1,0:T(8,128)(2,1)S(1)}, u32[]{:S(2)}, u32[]{:S(2)}) collective-permute-start(bf16[2,24,2048]{2,1,0:T(8,128)(2,1)S(1)} %shard_map.112.refs_0_), channel_id=1, source_target_pairs={{0,2},{1,3},{2,0},{3,1},{4,6},{5,7},{6,4},{7,5},{8,10},{9,11},{10,... | collective-permute-start | bytes 589832 | tf_op jit(solution)/shard_map/ppermute | solution.py:39
  26.2 1.5 %shard_map.125.held_ref = bf16[2,4,256,512]{3,2,1,0:T(8,128)(2,1)} custom-call(bf16[256,512]{1,0:T(8,128)(2,1)S(1)} %copy-done.1, bf16[256,512]{1,0:T(8,128)(2,1)S(1)} %collective-permute-done.13.refs_2_.refs_1_, bf16[256,512]{1,0:T(8,128)(2,1)S(1)} %collective-permute-done.11.refs_1_.refs_2_, bf16[256,512]{1,0:T(8,128)(2,1)S(1)} %collective-permute-done.14.refs_3_, ...), custom_call_target="tpu_custom_call" | custom-call | flops 1048576 | bytes 1048576 | tf_op jit(solution)/shard_map/pallas_call | solution.py:130
  27.7 1.5 %collective-permute-start.2 = (bf16[2,24,2048]{2,1,0:T(8,128)(2,1)S(1)}, bf16[2,24,2048]{2,1,0:T(8,128)(2,1)S(1)}, u32[]{:S(2)}, u32[]{:S(2)}) collective-permute-start(bf16[2,24,2048]{2,1,0:T(8,128)(2,1)S(1)} %shard_map.112.refs_0_), channel_id=1, source_target_pairs={{0,6},{1,7},{2,4},{3,5},{4,2},{5,3},{6,0},{7,1},{8,14},{9,15},{10,... | collective-permute-start | bytes 589832 | tf_op jit(solution)/shard_map/ppermute | solution.py:39
  30.5 4.5 %collective-permute-done.1.refs_2_ = bf16[2,24,2048]{2,1,0:T(8,128)(2,1)S(1)} collective-permute-done((bf16[2,24,2048]{2,1,0:T(8,128)(2,1)S(1)}, bf16[2,24,2048]{2,1,0:T(8,128)(2,1)S(1)}, u32[]{:S(2)}, u32[]{:S(2)}) %collective-permute-start.1) | collective-permute-done | bytes 196640 | tf_op jit(solution)/shard_map/ppermute | solution.py:39
  35.5 0.7 shard_map.128.refs_3_
  36.2 0.7 copy-done.7
  37.5 0.7 copy-done.9
  39.5 2.4 %collective-permute-start.40 = (bf16[3,24,2048]{2,1,0:T(8,128)(2,1)}, bf16[3,24,2048]{2,1,0:T(8,128)(2,1)}, u32[]{:S(2)}, u32[]{:S(2)}) collective-permute-start(bf16[3,24,2048]{2,1,0:T(8,128)(2,1)} %shard_map.128.refs_3_), channel_id=1, source_target_pairs={{0,6},{1,7},{2,4},{3,5},{4,2},{5,3},{6,0},{7,1},{8,14},{9,15},{10,... | collective-permute-start | bytes 884744 | tf_op jit(solution)/shard_map/ppermute | solution.py:39
  41.9 0.7 shard_map.117
  42.6 3.6 %all-to-all-start = ((bf16[8,128,128]{2,1,0:T(8,128)(2,1)}), bf16[8,128,128]{2,1,0:T(8,128)(2,1)S(1)}, u32[]{:S(2)}, u32[]{:S(2)}) async-start(bf16[8,128,128]{2,1,0:T(8,128)(2,1)} %shard_map.117), calls=%async_computation | async-start | bytes 524288 | tf_op jit(solution)/shard_map/all_to_all | solution.py:693
  46.2 0.9 copy-done.4
  47.2 0.9 copy-done.6
  48.1 0.9 copy-done.8
  49.0 0.9 copy-done.10
  49.9 0.9 copy-done.12
  50.9 2.4 %shard_map.114 = (bf16[128,768]{1,0:T(8,128)(2,1)}, bf16[192,2048]{1,0:T(8,128)(2,1)}) custom-call(bf16[2,24,2048]{2,1,0:T(8,128)(2,1)S(1)} %shard_map.112.refs_0_, bf16[2,24,2048]{2,1,0:T(8,128)(2,1)S(1)} %collective-permute-done.refs_1_, bf16[2,24,2048]{2,1,0:T(8,128)(2,1)S(1)} %copy-done.4, bf16[2,24,2048]{2,1,0:T(8,128)(2,1)S(1)} %copy-done.6, ...), custom_call_target="tpu_custom_call" | custom-call | flops 402653184 | bytes 1048576 | tf_op jit(solution)/shard_map/pallas_call | solution.py:130
  53.2 1.9 %collective-permute-start.7 = (bf16[128,768]{1,0:T(8,128)(2,1)}, bf16[128,768]{1,0:T(8,128)(2,1)S(1)}, u32[]{:S(2)}, u32[]{:S(2)}) collective-permute-start(bf16[128,768]{1,0:T(8,128)(2,1)} %get-tuple-element.38.refs_0_.refs_1_), channel_id=1, source_target_pairs={{0,16},{8,24},{16,0},{24,8},{1,17},{9,25},{17,1},{25,9},{2,18},{10... | collective-permute-start | bytes 589832 | tf_op jit(solution)/shard_map/ppermute | solution.py:39
  55.1 1.3 collective-permute-start.8
  56.8 2.3 %shard_map.129.refs_5_ = bf16[288,2048]{1,0:T(8,128)(2,1)} custom-call(bf16[3,24,2048]{2,1,0:T(8,128)(2,1)S(1)} %collective-permute-done.38.refs_0_, bf16[3,24,2048]{2,1,0:T(8,128)(2,1)} %collective-permute-done.39.refs_1_, bf16[3,24,2048]{2,1,0:T(8,128)(2,1)} %collective-permute-done.40.refs_2_, bf16[3,24,2048]{2,1,0:T(8,128)(2,1)} %shard_map.128.refs_3_), custom_call_target="tpu_custom_call" | custom-call | flops 1048576 | bytes 1048576 | tf_op jit(solution)/shard_map/pallas_call | solution.py:130
  59.1 11.2 %collective-permute-done.7.refs_2_.refs_0_ = bf16[128,768]{1,0:T(8,128)(2,1)S(1)} collective-permute-done((bf16[128,768]{1,0:T(8,128)(2,1)}, bf16[128,768]{1,0:T(8,128)(2,1)S(1)}, u32[]{:S(2)}, u32[]{:S(2)}) %collective-permute-start.7) | collective-permute-done | bytes 196640 | tf_op jit(solution)/shard_map/ppermute | solution.py:39
  70.3 0.9 collective-permute-done.9.refs_1_.refs_0_
  71.2 4.0 %shard_map.118 = (f32[4,64,768]{2,1,0:T(8,128)S(1)}, f32[8,768]{1,0:T(8,128)S(1)}, f32[1024,768]{1,0:T(8,128)S(1)}, f32[1024,768]{1,0:T(8,128)S(1)}, f32[1024,768]{1,0:T(8,128)S(1)}, /*index=5*/f32[1024,768]{1,0:T(8,128)S(1)}) custom-call(bf16[128,768]{1,0:T(8,128)(2,1)S(1)} %copy-done.13, bf16[128,768]{1,0:T(8,128)(2,1)S(1)} %collective-permute-done.9.refs_1_.refs_0_, ...), custom_call_target="tpu_custom_call" | custom-call | flops 1610612736 | bytes 1048576 | tf_op jit(solution)/shard_map/pallas_call | solution.py:130
  75.2 3.5 %collective-permute-start.18 = (f32[8,768]{1,0:T(8,128)S(1)}, f32[8,768]{1,0:T(8,128)S(1)}, u32[]{:S(2)}, u32[]{:S(2)}) collective-permute-start(f32[8,768]{1,0:T(8,128)S(1)} %get-tuple-element.47.refs_0_), channel_id=1, source_target_pairs={{0,8},{8,0},{16,24},{24,16},{1,9},{9,1},{17,25},{25,17},{2,10},{10... | collective-permute-start | bytes 73736 | tf_op jit(solution)/shard_map/ppermute | solution.py:39
  78.7 1.4 collective-permute-start.19
  80.1 1.4 collective-permute-start.20
  81.5 2.2 %collective-permute-done.19.refs_2_ = f32[8,768]{1,0:T(8,128)S(1)} collective-permute-done((f32[8,768]{1,0:T(8,128)S(1)}, f32[8,768]{1,0:T(8,128)S(1)}, u32[]{:S(2)}, u32[]{:S(2)}) %collective-permute-start.19) | collective-permute-done | bytes 24608 | tf_op jit(solution)/shard_map/ppermute | solution.py:39
  83.7 2.0 %collective-permute-done.20.refs_3_ = f32[8,768]{1,0:T(8,128)S(1)} collective-permute-done((f32[8,768]{1,0:T(8,128)S(1)}, f32[8,768]{1,0:T(8,128)S(1)}, u32[]{:S(2)}, u32[]{:S(2)}) %collective-permute-start.20) | collective-permute-done | bytes 24608 | tf_op jit(solution)/shard_map/ppermute | solution.py:39
  85.8 0.8 shard_map.119
  86.5 3.9 %shard_map.120 = (f32[1024,128]{1,0:T(8,128)S(1)}, bf16[64,768]{1,0:T(8,128)(2,1)}, bf16[64,768]{1,0:T(8,128)(2,1)}) custom-call(bf16[128,768]{1,0:T(8,128)(2,1)S(1)} %collective-permute-done.7.refs_2_.refs_0_, bf16[128,768]{1,0:T(8,128)(2,1)S(1)} %collective-permute-done.8.refs_3_.refs_1_, f32[1024,768]{1,0:T(8,128)S(1)} %get-tuple-element.45.refs_2_, ...), custom_call_target="tpu_custom_call" | custom-call | flops 2013265920 | bytes 1048576 | tf_op jit(solution)/shard_map/pallas_call | solution.py:130
  90.4 2.5 %collective-permute-start.22 = (bf16[64,768]{1,0:T(8,128)(2,1)}, bf16[64,768]{1,0:T(8,128)(2,1)S(1)}, u32[]{:S(2)}, u32[]{:S(2)}) collective-permute-start(bf16[64,768]{1,0:T(8,128)(2,1)} %get-tuple-element.51), channel_id=1, source_target_pairs={{0,24},{8,16},{16,8},{24,0},{1,25},{9,17},{17,9},{25,1},{2,26},{10... | collective-permute-start | bytes 294920 | tf_op jit(solution)/shard_map/ppermute | solution.py:39
  92.9 4.0 %shard_map.121 = (bf16[8,128,128]{2,1,0:T(8,128)(2,1)}, bf16[64,768]{1,0:T(8,128)(2,1)}, bf16[64,768]{1,0:T(8,128)(2,1)}) custom-call(bf16[128,768]{1,0:T(8,128)(2,1)S(1)} %collective-permute-done.9.refs_1_.refs_0_, bf16[128,768]{1,0:T(8,128)(2,1)S(1)} %copy-done.13, f32[1024,768]{1,0:T(8,128)S(1)} %get-tuple-element.52.refs_2_, ...), custom_call_target="tpu_custom_call" | custom-call | flops 2013265920 | bytes 1048576 | tf_op jit(solution)/shard_map/pallas_call | solution.py:130
  96.9 1.0 collective-permute-start.23
  97.9 1.0 collective-permute-done.21.refs_0_
  98.9 2.8 %collective-permute-done.23.refs_2_ = bf16[64,768]{1,0:T(8,128)(2,1)S(1)} collective-permute-done((bf16[64,768]{1,0:T(8,128)(2,1)}, bf16[64,768]{1,0:T(8,128)(2,1)S(1)}, u32[]{:S(2)}, u32[]{:S(2)}) %collective-permute-start.23) | collective-permute-done | bytes 98336 | tf_op jit(solution)/shard_map/ppermute | solution.py:39
  101.7 1.5 %shard_map.122 = (f32[96,2048]{1,0:T(8,128)S(1)}, bf16[96,2048]{1,0:T(8,128)(2,1)S(1)}) custom-call(bf16[64,768]{1,0:T(8,128)(2,1)S(1)} %collective-permute-done.21.refs_0_, bf16[64,768]{1,0:T(8,128)(2,1)S(1)} %collective-permute-done.22.refs_1_, bf16[64,768]{1,0:T(8,128)(2,1)S(1)} %collective-permute-done.23.refs_2_, ...), custom_call_target="tpu_custom_call" | custom-call | flops 201326592 | bytes 1048576 | tf_op jit(solution)/shard_map/pallas_call | solution.py:130
  103.3 1.0 collective-permute-start.29
  104.3 0.9 collective-permute-start.30
  105.2 4.2 %collective-permute-done.29.refs_0_ = bf16[64,768]{1,0:T(8,128)(2,1)S(1)} collective-permute-done((bf16[64,768]{1,0:T(8,128)(2,1)S(1)}, bf16[64,768]{1,0:T(8,128)(2,1)S(1)}, u32[]{:S(2)}, u32[]{:S(2)}) %collective-permute-start.29) | collective-permute-done | bytes 98336 | tf_op jit(solution)/shard_map/ppermute | solution.py:39
  109.4 2.1 %collective-permute-start.31 = (bf16[64,768]{1,0:T(8,128)(2,1)S(1)}, bf16[64,768]{1,0:T(8,128)(2,1)S(1)}, u32[]{:S(2)}, u32[]{:S(2)}) collective-permute-start(bf16[64,768]{1,0:T(8,128)(2,1)S(1)} %copy-done.14), channel_id=1, source_target_pairs={{0,24},{8,16},{16,8},{24,0},{1,25},{9,17},{17,9},{25,1},{2,26},{10... | collective-permute-start | bytes 294920 | tf_op jit(solution)/shard_map/ppermute | solution.py:39
  111.5 3.8 %all-to-all-start.1 = ((bf16[8,128,128]{2,1,0:T(8,128)(2,1)}), bf16[8,128,128]{2,1,0:T(8,128)(2,1)S(1)}, u32[]{:S(2)}, u32[]{:S(2)}) async-start(bf16[8,128,128]{2,1,0:T(8,128)(2,1)} %get-tuple-element.63), calls=%async_computation.1 | async-start | bytes 524288 | tf_op jit(solution)/shard_map/all_to_all | solution.py:713
  115.9 0.9 shard_map.127.refs_0_
  116.9 1.1 collective-permute-start.32
  118.0 1.5 %collective-permute-start.33 = (bf16[64,768]{1,0:T(8,128)(2,1)S(1)}, bf16[64,768]{1,0:T(8,128)(2,1)S(1)}, u32[]{:S(2)}, u32[]{:S(2)}) collective-permute-start(bf16[64,768]{1,0:T(8,128)(2,1)S(1)} %shard_map.127.refs_0_), channel_id=1, source_target_pairs={{0,16},{8,24},{16,0},{24,8},{1,17},{9,25},{17,1},{25,9},{2,18},{10... | collective-permute-start | bytes 294920 | tf_op jit(solution)/shard_map/ppermute | solution.py:39
  119.5 1.9 %collective-permute-start.34 = (bf16[64,768]{1,0:T(8,128)(2,1)S(1)}, bf16[64,768]{1,0:T(8,128)(2,1)S(1)}, u32[]{:S(2)}, u32[]{:S(2)}) collective-permute-start(bf16[64,768]{1,0:T(8,128)(2,1)S(1)} %shard_map.127.refs_0_), channel_id=1, source_target_pairs={{0,24},{8,16},{16,8},{24,0},{1,25},{9,17},{17,9},{25,1},{2,26},{10... | collective-permute-start | bytes 294920 | tf_op jit(solution)/shard_map/ppermute | solution.py:39
  121.3 0.8 shard_map.123
  122.6 1.6 %collective-permute-start.25 = (bf16[24,2048]{1,0:T(8,128)(2,1)}, bf16[24,2048]{1,0:T(8,128)(2,1)S(1)}, u32[]{:S(2)}, u32[]{:S(2)}) collective-permute-start(bf16[24,2048]{1,0:T(8,128)(2,1)} %get-tuple-element.59), channel_id=1, source_target_pairs={{0,2},{1,3},{2,0},{3,1},{4,6},{5,7},{6,4},{7,5},{8,10},{9,11},{10,... | collective-permute-start | bytes 294920 | tf_op jit(solution)/shard_map/ppermute | solution.py:39
  124.3 3.6 %collective-permute-done.33.refs_2_ = bf16[64,768]{1,0:T(8,128)(2,1)S(1)} collective-permute-done((bf16[64,768]{1,0:T(8,128)(2,1)S(1)}, bf16[64,768]{1,0:T(8,128)(2,1)S(1)}, u32[]{:S(2)}, u32[]{:S(2)}) %collective-permute-start.33) | collective-permute-done | bytes 98336 | tf_op jit(solution)/shard_map/ppermute | solution.py:39
  127.9 1.6 %collective-permute-start.26 = (bf16[24,2048]{1,0:T(8,128)(2,1)}, bf16[24,2048]{1,0:T(8,128)(2,1)S(1)}, u32[]{:S(2)}, u32[]{:S(2)}) collective-permute-start(bf16[24,2048]{1,0:T(8,128)(2,1)} %get-tuple-element.60), channel_id=1, source_target_pairs={{0,4},{1,5},{2,6},{3,7},{4,0},{5,1},{6,2},{7,3},{8,12},{9,13},{10,... | collective-permute-start | bytes 294920 | tf_op jit(solution)/shard_map/ppermute | solution.py:39
  129.5 1.5 %collective-permute-start.27 = (bf16[24,2048]{1,0:T(8,128)(2,1)}, bf16[24,2048]{1,0:T(8,128)(2,1)S(1)}, u32[]{:S(2)}, u32[]{:S(2)}) collective-permute-start(bf16[24,2048]{1,0:T(8,128)(2,1)} %get-tuple-element.61), channel_id=1, source_target_pairs={{0,6},{1,7},{2,4},{3,5},{4,2},{5,3},{6,0},{7,1},{8,14},{9,15},{10,... | collective-permute-start | bytes 294920 | tf_op jit(solution)/shard_map/ppermute | solution.py:39
  130.9 5.2 %weight_grad.1 = f32[256,2048]{1,0:T(8,128)} custom-call(bf16[64,768]{1,0:T(8,128)(2,1)S(1)} %shard_map.127.refs_0_, bf16[64,768]{1,0:T(8,128)(2,1)S(1)} %collective-permute-done.32.refs_1_, bf16[64,768]{1,0:T(8,128)(2,1)S(1)} %collective-permute-done.33.refs_2_, bf16[64,768]{1,0:T(8,128)(2,1)S(1)} %collective-permute-done.34.refs_3_, ...), custom_call_target="tpu_custom_call" | custom-call | flops 805306368 | bytes 3145728 | tf_op jit(solution)/shard_map/weight_grad/pallas_call | solution.py:562
  136.2 1.9 %shard_map.124 = f32[24,2048]{1,0:T(8,128)} custom-call(bf16[24,2048]{1,0:T(8,128)(2,1)S(1)} %collective-permute-done.25.refs_0_, bf16[24,2048]{1,0:T(8,128)(2,1)S(1)} %collective-permute-done.26.refs_1_, bf16[24,2048]{1,0:T(8,128)(2,1)S(1)} %collective-permute-done.27.refs_2_, f32[24,2048]{1,0:T(8,128)} %get-tuple-element.62.refs_3_, ...), custom_call_target="tpu_custom_call" | custom-call | flops 1048576 | bytes 1048576 | tf_op jit(solution)/shard_map/pallas_call | solution.py:130
  138.1 4.5 %shard_map.126 = f32[128,2048]{1,0:T(8,128)} custom-call(s32[1]{0:T(128)} %bitcast.1.at_ref, bf16[8,128,128]{2,1,0:T(8,128)(2,1)S(1)} %all-to-all-done.1.back_ref, bf16[2,4,256,512]{3,2,1,0:T(8,128)(2,1)S(1)} %copy-done, bf16[2,4,256,512]{3,2,1,0:T(8,128)(2,1)} %collective-permute-done.28.other_ref, bf16[128,2048]{1,0:T(8,128)(2,1)} %rows_ref.1, ...), custom_call_target="tpu_custom_call" | custom-call | flops 536870912 | bytes 1048576 | tf_op jit(solution)/shard_map/pallas_call | solution.py:130
  (77 shorter events, 6.8 us)
Async XLA Ops:
  0.6 6.4 %copy-start.1 = (bf16[256,512]{1,0:T(8,128)(2,1)S(1)}, bf16[256,512]{1,0:T(8,128)(2,1)}, u32[]{:S(2)}) copy-start(bf16[256,512]{1,0:T(8,128)(2,1)} %refs_0_.5) | copy-start | bytes 786436
  0.6 7.0 %copy-start.2 = (bf16[256,512]{1,0:T(8,128)(2,1)S(1)}, bf16[256,512]{1,0:T(8,128)(2,1)}, u32[]{:S(2)}) copy-start(bf16[256,512]{1,0:T(8,128)(2,1)} %refs_4_.3) | copy-start | bytes 786436
  0.7 10.1 %collective-permute-start.11 = (bf16[256,512]{1,0:T(8,128)(2,1)}, bf16[256,512]{1,0:T(8,128)(2,1)S(1)}, u32[]{:S(2)}, u32[]{:S(2)}) collective-permute-start(bf16[256,512]{1,0:T(8,128)(2,1)} %refs_0_.5), channel_id=1, source_target_pairs={{0,4},{1,5},{2,6},{3,7},{4,0},{5,1},{6,2},{7,3},{8,12},{9,13},{10,... | collective-permute-start | bytes 786440 | tf_op jit(solution)/shard_map/ppermute | solution.py:39
  3.7 9.4 %collective-permute-start.12 = (bf16[256,512]{1,0:T(8,128)(2,1)}, bf16[256,512]{1,0:T(8,128)(2,1)S(1)}, u32[]{:S(2)}, u32[]{:S(2)}) collective-permute-start(bf16[256,512]{1,0:T(8,128)(2,1)} %refs_4_.3), channel_id=1, source_target_pairs={{0,2},{1,3},{2,0},{3,1},{4,6},{5,7},{6,4},{7,5},{8,10},{9,11},{10,... | collective-permute-start | bytes 786440 | tf_op jit(solution)/shard_map/ppermute | solution.py:39
  7.0 7.6 %collective-permute-start.10 = (bf16[128,1024]{1,0:T(8,128)(2,1)S(1)}, bf16[128,1024]{1,0:T(8,128)(2,1)S(1)}, u32[]{:S(2)}, u32[]{:S(2)}) collective-permute-start(bf16[128,1024]{1,0:T(8,128)(2,1)S(1)} %get-tuple-element.40), channel_id=1, source_target_pairs={{0,1},{1,0},{2,3},{3,2},{4,5},{5,4},{6,7},{7,6},{8,9},{9,8},{10,11... | collective-permute-start | bytes 786440 | tf_op jit(solution)/shard_map/ppermute | solution.py:39
  7.1 11.7 %collective-permute-start.13 = (bf16[256,512]{1,0:T(8,128)(2,1)S(1)}, bf16[256,512]{1,0:T(8,128)(2,1)S(1)}, u32[]{:S(2)}, u32[]{:S(2)}) collective-permute-start(bf16[256,512]{1,0:T(8,128)(2,1)S(1)} %copy-done.1), channel_id=1, source_target_pairs={{0,2},{1,3},{2,0},{3,1},{4,6},{5,7},{6,4},{7,5},{8,10},{9,11},{10,... | collective-permute-start | bytes 786440 | tf_op jit(solution)/shard_map/ppermute | solution.py:39
  7.7 13.7 %collective-permute-start.15 = (bf16[256,512]{1,0:T(8,128)(2,1)S(1)}, bf16[256,512]{1,0:T(8,128)(2,1)S(1)}, u32[]{:S(2)}, u32[]{:S(2)}) collective-permute-start(bf16[256,512]{1,0:T(8,128)(2,1)S(1)} %copy-done.2), channel_id=1, source_target_pairs={{0,4},{1,5},{2,6},{3,7},{4,0},{5,1},{6,2},{7,3},{8,12},{9,13},{10,... | collective-permute-start | bytes 786440 | tf_op jit(solution)/shard_map/ppermute | solution.py:39
  10.7 13.0 %collective-permute-start.14 = (bf16[256,512]{1,0:T(8,128)(2,1)S(1)}, bf16[256,512]{1,0:T(8,128)(2,1)S(1)}, u32[]{:S(2)}, u32[]{:S(2)}) collective-permute-start(bf16[256,512]{1,0:T(8,128)(2,1)S(1)} %collective-permute-done.11.refs_1_.refs_2_), channel_id=1, source_target_pairs={{0,2},{1,3},{2,0},{3,1},{4,6},{5,7},{6,4},{7,5},{8,10},{9,11},{10,... | collective-permute-start | bytes 786440 | tf_op jit(solution)/shard_map/ppermute | solution.py:39
  13.1 12.2 %collective-permute-start.16 = (bf16[256,512]{1,0:T(8,128)(2,1)S(1)}, bf16[256,512]{1,0:T(8,128)(2,1)S(1)}, u32[]{:S(2)}, u32[]{:S(2)}) collective-permute-start(bf16[256,512]{1,0:T(8,128)(2,1)S(1)} %collective-permute-done.12.refs_3_.refs_5_), channel_id=1, source_target_pairs={{0,4},{1,5},{2,6},{3,7},{4,0},{5,1},{6,2},{7,3},{8,12},{9,13},{10,... | collective-permute-start | bytes 786440 | tf_op jit(solution)/shard_map/ppermute | solution.py:39
  14.5 13.2 %collective-permute-start.35 = (bf16[24,2048]{1,0:T(8,128)(2,1)}, bf16[24,2048]{1,0:T(8,128)(2,1)S(1)}, u32[]{:S(2)}, u32[]{:S(2)}) collective-permute-start(bf16[24,2048]{1,0:T(8,128)(2,1)} %refs_5_.1), channel_id=1, source_target_pairs={{0,8},{8,0},{16,24},{24,16},{1,9},{9,1},{17,25},{25,17},{2,10},{10... | collective-permute-start | bytes 294920 | tf_op jit(solution)/shard_map/ppermute | solution.py:39
  18.7 10.5 %collective-permute-start.36 = (bf16[24,2048]{1,0:T(8,128)(2,1)}, bf16[24,2048]{1,0:T(8,128)(2,1)S(1)}, u32[]{:S(2)}, u32[]{:S(2)}) collective-permute-start(bf16[24,2048]{1,0:T(8,128)(2,1)} %refs_5_.1), channel_id=1, source_target_pairs={{0,16},{8,24},{16,0},{24,8},{1,17},{9,25},{17,1},{25,9},{2,18},{10... | collective-permute-start | bytes 294920 | tf_op jit(solution)/shard_map/ppermute | solution.py:39
  21.3 8.5 %collective-permute-start.37 = (bf16[24,2048]{1,0:T(8,128)(2,1)}, bf16[24,2048]{1,0:T(8,128)(2,1)S(1)}, u32[]{:S(2)}, u32[]{:S(2)}) collective-permute-start(bf16[24,2048]{1,0:T(8,128)(2,1)} %refs_5_.1), channel_id=1, source_target_pairs={{0,24},{8,16},{16,8},{24,0},{1,25},{9,17},{17,9},{25,1},{2,26},{10... | collective-permute-start | bytes 294920 | tf_op jit(solution)/shard_map/ppermute | solution.py:39
  23.7 6.7 %collective-permute-start = (bf16[2,24,2048]{2,1,0:T(8,128)(2,1)S(1)}, bf16[2,24,2048]{2,1,0:T(8,128)(2,1)S(1)}, u32[]{:S(2)}, u32[]{:S(2)}) collective-permute-start(bf16[2,24,2048]{2,1,0:T(8,128)(2,1)S(1)} %shard_map.112.refs_0_), channel_id=1, source_target_pairs={{0,2},{1,3},{2,0},{3,1},{4,6},{5,7},{6,4},{7,5},{8,10},{9,11},{10,... | collective-permute-start | bytes 589832 | tf_op jit(solution)/shard_map/ppermute | solution.py:39
  25.3 9.7 %collective-permute-start.1 = (bf16[2,24,2048]{2,1,0:T(8,128)(2,1)S(1)}, bf16[2,24,2048]{2,1,0:T(8,128)(2,1)S(1)}, u32[]{:S(2)}, u32[]{:S(2)}) collective-permute-start(bf16[2,24,2048]{2,1,0:T(8,128)(2,1)S(1)} %shard_map.112.refs_0_), channel_id=1, source_target_pairs={{0,4},{1,5},{2,6},{3,7},{4,0},{5,1},{6,2},{7,3},{8,12},{9,13},{10,... | collective-permute-start | bytes 589832 | tf_op jit(solution)/shard_map/ppermute | solution.py:39
  27.7 7.3 %collective-permute-start.2 = (bf16[2,24,2048]{2,1,0:T(8,128)(2,1)S(1)}, bf16[2,24,2048]{2,1,0:T(8,128)(2,1)S(1)}, u32[]{:S(2)}, u32[]{:S(2)}) collective-permute-start(bf16[2,24,2048]{2,1,0:T(8,128)(2,1)S(1)} %shard_map.112.refs_0_), channel_id=1, source_target_pairs={{0,6},{1,7},{2,4},{3,5},{4,2},{5,3},{6,0},{7,1},{8,14},{9,15},{10,... | collective-permute-start | bytes 589832 | tf_op jit(solution)/shard_map/ppermute | solution.py:39
  29.2 108.8 %collective-permute-start.28 = (bf16[2,4,256,512]{3,2,1,0:T(8,128)(2,1)}, bf16[2,4,256,512]{3,2,1,0:T(8,128)(2,1)}, u32[]{:S(2)}, u32[]{:S(2)}) collective-permute-start(bf16[2,4,256,512]{3,2,1,0:T(8,128)(2,1)} %shard_map.125.held_ref), channel_id=1, source_target_pairs={{0,1},{1,0},{2,3},{3,2},{4,5},{5,4},{6,7},{7,6},{8,9},{9,8},{10,11... | collective-permute-start | bytes 6291464 | tf_op jit(solution)/shard_map/ppermute | solution.py:39
  29.8 9.7 %collective-permute-start.17 = (f32[8,128,128]{2,1,0:T(8,128)S(1)}, f32[8,128,128]{2,1,0:T(8,128)S(1)}, u32[]{:S(2)}, u32[]{:S(2)}) collective-permute-start(f32[8,128,128]{2,1,0:T(8,128)S(1)} %get-tuple-element.44), channel_id=1, source_target_pairs={{0,1},{1,0},{2,3},{3,2},{4,5},{5,4},{6,7},{7,6},{8,9},{9,8},{10,11... | collective-permute-start | bytes 1572872 | tf_op jit(solution)/shard_map/ppermute | solution.py:39
  30.4 5.9 %collective-permute-start.3 = (bf16[2,24,2048]{2,1,0:T(8,128)(2,1)S(1)}, bf16[2,24,2048]{2,1,0:T(8,128)(2,1)S(1)}, u32[]{:S(2)}, u32[]{:S(2)}) collective-permute-start(bf16[2,24,2048]{2,1,0:T(8,128)(2,1)S(1)} %shard_map.112.refs_0_), channel_id=1, source_target_pairs={{0,1},{1,0},{2,3},{3,2},{4,5},{5,4},{6,7},{7,6},{8,9},{9,8},{10,11... | collective-permute-start | bytes 589832 | tf_op jit(solution)/shard_map/ppermute | solution.py:39
  35.0 4.5 %copy-start.3 = (bf16[2,24,2048]{2,1,0:T(8,128)(2,1)}, bf16[2,24,2048]{2,1,0:T(8,128)(2,1)S(1)}, u32[]{:S(2)}) copy-start(bf16[2,24,2048]{2,1,0:T(8,128)(2,1)S(1)} %collective-permute-done.1.refs_2_) | copy-start | bytes 589828
  35.0 2.5 %collective-permute-start.4 = (bf16[2,24,2048]{2,1,0:T(8,128)(2,1)S(1)}, bf16[2,24,2048]{2,1,0:T(8,128)(2,1)S(1)}, u32[]{:S(2)}, u32[]{:S(2)}) collective-permute-start(bf16[2,24,2048]{2,1,0:T(8,128)(2,1)S(1)} %collective-permute-done.refs_1_), channel_id=1, source_target_pairs={{0,1},{1,0},{2,3},{3,2},{4,5},{5,4},{6,7},{7,6},{8,9},{9,8},{10,11... | collective-permute-start | bytes 589832 | tf_op jit(solution)/shard_map/ppermute | solution.py:39
  35.0 11.2 %copy-start.5 = (bf16[2,24,2048]{2,1,0:T(8,128)(2,1)}, bf16[2,24,2048]{2,1,0:T(8,128)(2,1)S(1)}, u32[]{:S(2)}) copy-start(bf16[2,24,2048]{2,1,0:T(8,128)(2,1)S(1)} %collective-permute-done.2.refs_3_) | copy-start | bytes 589828
  35.0 3.8 %collective-permute-start.5 = (bf16[2,24,2048]{2,1,0:T(8,128)(2,1)S(1)}, bf16[2,24,2048]{2,1,0:T(8,128)(2,1)S(1)}, u32[]{:S(2)}, u32[]{:S(2)}) collective-permute-start(bf16[2,24,2048]{2,1,0:T(8,128)(2,1)S(1)} %collective-permute-done.1.refs_2_), channel_id=1, source_target_pairs={{0,1},{1,0},{2,3},{3,2},{4,5},{5,4},{6,7},{7,6},{8,9},{9,8},{10,11... | collective-permute-start | bytes 589832 | tf_op jit(solution)/shard_map/ppermute | solution.py:39
  36.2 0.7 copy-start.7
  36.9 18.2 %collective-permute-start.38 = (bf16[3,24,2048]{2,1,0:T(8,128)(2,1)}, bf16[3,24,2048]{2,1,0:T(8,128)(2,1)S(1)}, u32[]{:S(2)}, u32[]{:S(2)}) collective-permute-start(bf16[3,24,2048]{2,1,0:T(8,128)(2,1)} %shard_map.128.refs_3_), channel_id=1, source_target_pairs={{0,2},{1,3},{2,0},{3,1},{4,6},{5,7},{6,4},{7,5},{8,10},{9,11},{10,... | collective-permute-start | bytes 884744 | tf_op jit(solution)/shard_map/ppermute | solution.py:39
  37.5 0.7 copy-start.9
  38.2 18.3 %collective-permute-start.39 = (bf16[3,24,2048]{2,1,0:T(8,128)(2,1)}, bf16[3,24,2048]{2,1,0:T(8,128)(2,1)}, u32[]{:S(2)}, u32[]{:S(2)}) collective-permute-start(bf16[3,24,2048]{2,1,0:T(8,128)(2,1)} %shard_map.128.refs_3_), channel_id=1, source_target_pairs={{0,4},{1,5},{2,6},{3,7},{4,0},{5,1},{6,2},{7,3},{8,12},{9,13},{10,... | collective-permute-start | bytes 884744 | tf_op jit(solution)/shard_map/ppermute | solution.py:39
  38.8 0.7 copy-start.11
  39.5 6.7 %collective-permute-start.6 = (bf16[2,24,2048]{2,1,0:T(8,128)(2,1)S(1)}, bf16[2,24,2048]{2,1,0:T(8,128)(2,1)}, u32[]{:S(2)}, u32[]{:S(2)}) collective-permute-start(bf16[2,24,2048]{2,1,0:T(8,128)(2,1)S(1)} %collective-permute-done.2.refs_3_), channel_id=1, source_target_pairs={{0,1},{1,0},{2,3},{3,2},{4,5},{5,4},{6,7},{7,6},{8,9},{9,8},{10,11... | collective-permute-start | bytes 589832 | tf_op jit(solution)/shard_map/ppermute | solution.py:39
  39.5 17.3 %collective-permute-start.40 = (bf16[3,24,2048]{2,1,0:T(8,128)(2,1)}, bf16[3,24,2048]{2,1,0:T(8,128)(2,1)}, u32[]{:S(2)}, u32[]{:S(2)}) collective-permute-start(bf16[3,24,2048]{2,1,0:T(8,128)(2,1)} %shard_map.128.refs_3_), channel_id=1, source_target_pairs={{0,6},{1,7},{2,4},{3,5},{4,2},{5,3},{6,0},{7,1},{8,14},{9,15},{10,... | collective-permute-start | bytes 884744 | tf_op jit(solution)/shard_map/ppermute | solution.py:39
  42.6 28.5 %all-to-all-start = ((bf16[8,128,128]{2,1,0:T(8,128)(2,1)}), bf16[8,128,128]{2,1,0:T(8,128)(2,1)S(1)}, u32[]{:S(2)}, u32[]{:S(2)}) async-start(bf16[8,128,128]{2,1,0:T(8,128)(2,1)} %shard_map.117), calls=%async_computation | async-start | bytes 524288 | tf_op jit(solution)/shard_map/all_to_all | solution.py:693
  46.2 0.9 copy-start.4
  47.2 0.9 copy-start.6
  48.1 0.9 copy-start.8
  49.0 0.9 copy-start.10
  49.9 0.9 copy-start.12
  53.2 17.9 %copy-start.13 = (bf16[128,768]{1,0:T(8,128)(2,1)S(1)}, bf16[128,768]{1,0:T(8,128)(2,1)}, u32[]{:S(2)}) copy-start(bf16[128,768]{1,0:T(8,128)(2,1)} %get-tuple-element.38.refs_0_.refs_1_) | copy-start | bytes 589828
  53.2 17.0 %collective-permute-start.7 = (bf16[128,768]{1,0:T(8,128)(2,1)}, bf16[128,768]{1,0:T(8,128)(2,1)S(1)}, u32[]{:S(2)}, u32[]{:S(2)}) collective-permute-start(bf16[128,768]{1,0:T(8,128)(2,1)} %get-tuple-element.38.refs_0_.refs_1_), channel_id=1, source_target_pairs={{0,16},{8,24},{16,0},{24,8},{1,17},{9,25},{17,1},{25,9},{2,18},{10... | collective-permute-start | bytes 589832 | tf_op jit(solution)/shard_map/ppermute | solution.py:39
  55.1 15.1 %collective-permute-start.8 = (bf16[128,768]{1,0:T(8,128)(2,1)}, bf16[128,768]{1,0:T(8,128)(2,1)S(1)}, u32[]{:S(2)}, u32[]{:S(2)}) collective-permute-start(bf16[128,768]{1,0:T(8,128)(2,1)} %get-tuple-element.38.refs_0_.refs_1_), channel_id=1, source_target_pairs={{0,24},{8,16},{16,8},{24,0},{1,25},{9,17},{17,9},{25,1},{2,26},{10... | collective-permute-start | bytes 589832 | tf_op jit(solution)/shard_map/ppermute | solution.py:39
  56.5 14.7 %collective-permute-start.9 = (bf16[128,768]{1,0:T(8,128)(2,1)}, bf16[128,768]{1,0:T(8,128)(2,1)S(1)}, u32[]{:S(2)}, u32[]{:S(2)}) collective-permute-start(bf16[128,768]{1,0:T(8,128)(2,1)} %get-tuple-element.38.refs_0_.refs_1_), channel_id=1, source_target_pairs={{0,8},{8,0},{16,24},{24,16},{1,9},{9,1},{17,25},{25,17},{2,10},{10... | collective-permute-start | bytes 589832 | tf_op jit(solution)/shard_map/ppermute | solution.py:39
  59.1 71.9 %collective-permute-start.41 = (bf16[288,2048]{1,0:T(8,128)(2,1)}, bf16[288,2048]{1,0:T(8,128)(2,1)}, u32[]{:S(2)}, u32[]{:S(2)}) collective-permute-start(bf16[288,2048]{1,0:T(8,128)(2,1)} %shard_map.129.refs_5_), channel_id=1, source_target_pairs={{0,1},{1,0},{2,3},{3,2},{4,5},{5,4},{6,7},{7,6},{8,9},{9,8},{10,11... | collective-permute-start | bytes 3538952 | tf_op jit(solution)/shard_map/ppermute | solution.py:39
  75.2 6.3 %collective-permute-start.18 = (f32[8,768]{1,0:T(8,128)S(1)}, f32[8,768]{1,0:T(8,128)S(1)}, u32[]{:S(2)}, u32[]{:S(2)}) collective-permute-start(f32[8,768]{1,0:T(8,128)S(1)} %get-tuple-element.47.refs_0_), channel_id=1, source_target_pairs={{0,8},{8,0},{16,24},{24,16},{1,9},{9,1},{17,25},{25,17},{2,10},{10... | collective-permute-start | bytes 73736 | tf_op jit(solution)/shard_map/ppermute | solution.py:39
  78.7 5.0 %collective-permute-start.19 = (f32[8,768]{1,0:T(8,128)S(1)}, f32[8,768]{1,0:T(8,128)S(1)}, u32[]{:S(2)}, u32[]{:S(2)}) collective-permute-start(f32[8,768]{1,0:T(8,128)S(1)} %get-tuple-element.47.refs_0_), channel_id=1, source_target_pairs={{0,16},{8,24},{16,0},{24,8},{1,17},{9,25},{17,1},{25,9},{2,18},{10... | collective-permute-start | bytes 73736 | tf_op jit(solution)/shard_map/ppermute | solution.py:39
  80.1 5.6 %collective-permute-start.20 = (f32[8,768]{1,0:T(8,128)S(1)}, f32[8,768]{1,0:T(8,128)S(1)}, u32[]{:S(2)}, u32[]{:S(2)}) collective-permute-start(f32[8,768]{1,0:T(8,128)S(1)} %get-tuple-element.47.refs_0_), channel_id=1, source_target_pairs={{0,24},{8,16},{16,8},{24,0},{1,25},{9,17},{17,9},{25,1},{2,26},{10... | collective-permute-start | bytes 73736 | tf_op jit(solution)/shard_map/ppermute | solution.py:39
  90.4 8.5 %collective-permute-start.21 = (bf16[64,768]{1,0:T(8,128)(2,1)}, bf16[64,768]{1,0:T(8,128)(2,1)S(1)}, u32[]{:S(2)}, u32[]{:S(2)}) collective-permute-start(bf16[64,768]{1,0:T(8,128)(2,1)} %get-tuple-element.50), channel_id=1, source_target_pairs={{0,16},{8,24},{16,0},{24,8},{1,17},{9,25},{17,1},{25,9},{2,18},{10... | collective-permute-start | bytes 294920 | tf_op jit(solution)/shard_map/ppermute | solution.py:39
  90.4 8.5 %collective-permute-start.22 = (bf16[64,768]{1,0:T(8,128)(2,1)}, bf16[64,768]{1,0:T(8,128)(2,1)S(1)}, u32[]{:S(2)}, u32[]{:S(2)}) collective-permute-start(bf16[64,768]{1,0:T(8,128)(2,1)} %get-tuple-element.51), channel_id=1, source_target_pairs={{0,24},{8,16},{16,8},{24,0},{1,25},{9,17},{17,9},{25,1},{2,26},{10... | collective-permute-start | bytes 294920 | tf_op jit(solution)/shard_map/ppermute | solution.py:39
  92.9 10.4 %copy-start.16 = (bf16[64,768]{1,0:T(8,128)(2,1)S(1)}, bf16[64,768]{1,0:T(8,128)(2,1)}, u32[]{:S(2)}) copy-start(bf16[64,768]{1,0:T(8,128)(2,1)} %get-tuple-element.64) | copy-start | bytes 294916
  92.9 11.4 %copy-start.15 = (bf16[64,768]{1,0:T(8,128)(2,1)S(1)}, bf16[64,768]{1,0:T(8,128)(2,1)}, u32[]{:S(2)}) copy-start(bf16[64,768]{1,0:T(8,128)(2,1)} %get-tuple-element.65) | copy-start | bytes 294916
  92.9 16.5 %copy-start.14 = (bf16[64,768]{1,0:T(8,128)(2,1)S(1)}, bf16[64,768]{1,0:T(8,128)(2,1)}, u32[]{:S(2)}) copy-start(bf16[64,768]{1,0:T(8,128)(2,1)} %get-tuple-element.66) | copy-start | bytes 294916
  96.9 4.8 %collective-permute-start.23 = (bf16[64,768]{1,0:T(8,128)(2,1)}, bf16[64,768]{1,0:T(8,128)(2,1)S(1)}, u32[]{:S(2)}, u32[]{:S(2)}) collective-permute-start(bf16[64,768]{1,0:T(8,128)(2,1)} %get-tuple-element.55), channel_id=1, source_target_pairs={{0,8},{8,0},{16,24},{24,16},{1,9},{9,1},{17,25},{25,17},{2,10},{10... | collective-permute-start | bytes 294920 | tf_op jit(solution)/shard_map/ppermute | solution.py:39
  103.2 16.3 %collective-permute-start.24 = (bf16[96,2048]{1,0:T(8,128)(2,1)S(1)}, bf16[96,2048]{1,0:T(8,128)(2,1)S(1)}, u32[]{:S(2)}, u32[]{:S(2)}) collective-permute-start(bf16[96,2048]{1,0:T(8,128)(2,1)S(1)} %get-tuple-element.58), channel_id=1, source_target_pairs={{0,1},{1,0},{2,3},{3,2},{4,5},{5,4},{6,7},{7,6},{8,9},{9,8},{10,11... | collective-permute-start | bytes 1179656 | tf_op jit(solution)/shard_map/ppermute | solution.py:39
  103.3 6.1 %collective-permute-start.29 = (bf16[64,768]{1,0:T(8,128)(2,1)S(1)}, bf16[64,768]{1,0:T(8,128)(2,1)S(1)}, u32[]{:S(2)}, u32[]{:S(2)}) collective-permute-start(bf16[64,768]{1,0:T(8,128)(2,1)S(1)} %copy-done.16), channel_id=1, source_target_pairs={{0,8},{8,0},{16,24},{24,16},{1,9},{9,1},{17,25},{25,17},{2,10},{10... | collective-permute-start | bytes 294920 | tf_op jit(solution)/shard_map/ppermute | solution.py:39
  104.3 11.0 %collective-permute-start.30 = (bf16[64,768]{1,0:T(8,128)(2,1)S(1)}, bf16[64,768]{1,0:T(8,128)(2,1)S(1)}, u32[]{:S(2)}, u32[]{:S(2)}) collective-permute-start(bf16[64,768]{1,0:T(8,128)(2,1)S(1)} %copy-done.15), channel_id=1, source_target_pairs={{0,16},{8,24},{16,0},{24,8},{1,17},{9,25},{17,1},{25,9},{2,18},{10... | collective-permute-start | bytes 294920 | tf_op jit(solution)/shard_map/ppermute | solution.py:39
  109.4 6.5 %collective-permute-start.31 = (bf16[64,768]{1,0:T(8,128)(2,1)S(1)}, bf16[64,768]{1,0:T(8,128)(2,1)S(1)}, u32[]{:S(2)}, u32[]{:S(2)}) collective-permute-start(bf16[64,768]{1,0:T(8,128)(2,1)S(1)} %copy-done.14), channel_id=1, source_target_pairs={{0,24},{8,16},{16,8},{24,0},{1,25},{9,17},{17,9},{25,1},{2,26},{10... | collective-permute-start | bytes 294920 | tf_op jit(solution)/shard_map/ppermute | solution.py:39
  111.5 26.6 %all-to-all-start.1 = ((bf16[8,128,128]{2,1,0:T(8,128)(2,1)}), bf16[8,128,128]{2,1,0:T(8,128)(2,1)S(1)}, u32[]{:S(2)}, u32[]{:S(2)}) async-start(bf16[8,128,128]{2,1,0:T(8,128)(2,1)} %get-tuple-element.63), calls=%async_computation.1 | async-start | bytes 524288 | tf_op jit(solution)/shard_map/all_to_all | solution.py:713
  116.9 5.7 %collective-permute-start.32 = (bf16[64,768]{1,0:T(8,128)(2,1)S(1)}, bf16[64,768]{1,0:T(8,128)(2,1)S(1)}, u32[]{:S(2)}, u32[]{:S(2)}) collective-permute-start(bf16[64,768]{1,0:T(8,128)(2,1)S(1)} %shard_map.127.refs_0_), channel_id=1, source_target_pairs={{0,8},{8,0},{16,24},{24,16},{1,9},{9,1},{17,25},{25,17},{2,10},{10... | collective-permute-start | bytes 294920 | tf_op jit(solution)/shard_map/ppermute | solution.py:39
  118.0 9.9 %collective-permute-start.33 = (bf16[64,768]{1,0:T(8,128)(2,1)S(1)}, bf16[64,768]{1,0:T(8,128)(2,1)S(1)}, u32[]{:S(2)}, u32[]{:S(2)}) collective-permute-start(bf16[64,768]{1,0:T(8,128)(2,1)S(1)} %shard_map.127.refs_0_), channel_id=1, source_target_pairs={{0,16},{8,24},{16,0},{24,8},{1,17},{9,25},{17,1},{25,9},{2,18},{10... | collective-permute-start | bytes 294920 | tf_op jit(solution)/shard_map/ppermute | solution.py:39
  119.5 10.0 %collective-permute-start.34 = (bf16[64,768]{1,0:T(8,128)(2,1)S(1)}, bf16[64,768]{1,0:T(8,128)(2,1)S(1)}, u32[]{:S(2)}, u32[]{:S(2)}) collective-permute-start(bf16[64,768]{1,0:T(8,128)(2,1)S(1)} %shard_map.127.refs_0_), channel_id=1, source_target_pairs={{0,24},{8,16},{16,8},{24,0},{1,25},{9,17},{17,9},{25,1},{2,26},{10... | collective-permute-start | bytes 294920 | tf_op jit(solution)/shard_map/ppermute | solution.py:39
  122.6 13.5 %collective-permute-start.25 = (bf16[24,2048]{1,0:T(8,128)(2,1)}, bf16[24,2048]{1,0:T(8,128)(2,1)S(1)}, u32[]{:S(2)}, u32[]{:S(2)}) collective-permute-start(bf16[24,2048]{1,0:T(8,128)(2,1)} %get-tuple-element.59), channel_id=1, source_target_pairs={{0,2},{1,3},{2,0},{3,1},{4,6},{5,7},{6,4},{7,5},{8,10},{9,11},{10,... | collective-permute-start | bytes 294920 | tf_op jit(solution)/shard_map/ppermute | solution.py:39
  127.9 8.3 %collective-permute-start.26 = (bf16[24,2048]{1,0:T(8,128)(2,1)}, bf16[24,2048]{1,0:T(8,128)(2,1)S(1)}, u32[]{:S(2)}, u32[]{:S(2)}) collective-permute-start(bf16[24,2048]{1,0:T(8,128)(2,1)} %get-tuple-element.60), channel_id=1, source_target_pairs={{0,4},{1,5},{2,6},{3,7},{4,0},{5,1},{6,2},{7,3},{8,12},{9,13},{10,... | collective-permute-start | bytes 294920 | tf_op jit(solution)/shard_map/ppermute | solution.py:39
  129.5 6.7 %collective-permute-start.27 = (bf16[24,2048]{1,0:T(8,128)(2,1)}, bf16[24,2048]{1,0:T(8,128)(2,1)S(1)}, u32[]{:S(2)}, u32[]{:S(2)}) collective-permute-start(bf16[24,2048]{1,0:T(8,128)(2,1)} %get-tuple-element.61), channel_id=1, source_target_pairs={{0,6},{1,7},{2,4},{3,5},{4,2},{5,3},{6,0},{7,1},{8,14},{9,15},{10,... | collective-permute-start | bytes 294920 | tf_op jit(solution)/shard_map/ppermute | solution.py:39
  130.9 7.1 %copy-start = (bf16[2,4,256,512]{3,2,1,0:T(8,128)(2,1)S(1)}, bf16[2,4,256,512]{3,2,1,0:T(8,128)(2,1)}, u32[]{:S(2)}) copy-start(bf16[2,4,256,512]{3,2,1,0:T(8,128)(2,1)} %shard_map.125.held_ref) | copy-start | bytes 6291460

commit v2 on v1

--- a/solution.py
+++ b/solution.py
@@ -312,20 +312,28 @@
     heads = query_weight.shape[1] // HEAD_DIM
 
     def kernel(*refs):
-        piece_refs, (query_ref, weight_ref, out_ref, cot_ref) = refs[:-4], refs[-4:]
+        piece_refs, (query_ref, weight_ref, out_ref) = refs[:-3], refs[-3:]
         rows = jnp.concatenate([ref[0] for ref in piece_refs], axis=0)
         queries = stacked(transposed(dot(rows, query_ref[...]))).astype(BF16)
         out_ref[0:HEAD_DIM, :] = queries * jnp.asarray(SCALE, BF16)
         cot = jnp.concatenate([ref[1] for ref in piece_refs], axis=0)
-        cot_ref[...] = cot
         out_ref[HEAD_DIM:, :] = stacked(nt_dot(weight_ref[...], cot)).astype(BF16)
 
-    out = (
-        shape_of((2 * HEAD_DIM, heads * count), BF16),
-        shape_of((count, pieces[0].shape[2]), BF16),
-    )
+    out = shape_of((2 * HEAD_DIM, heads * count), BF16)
     flops = 4 * count * query_weight.size
     return resident(kernel, out, *pieces, query_weight, out_weight, kept=0, flops=flops)
+
+
+def hold_own(pieces, pair):
+    count = sum(piece.shape[1] for piece in pieces)
+
+    def kernel(*refs):
+        piece_refs, (pair_ref, near_ref, out_ref) = refs[:-3], refs[-3:]
+        near_ref[...] = pair_ref[...]
+        out_ref[...] = jnp.concatenate([ref[1] for ref in piece_refs], axis=0)
+
+    outs = (shape_of(pair.shape, BF16), shape_of((count, pieces[0].shape[2]), BF16))
+    return resident(kernel, outs, *pieces, pair, kept=1, loaded=len(pieces), fetched=1)
 
 
 def gather_cotangents(pieces):
@@ -539,7 +547,7 @@
     blocks = len(attended)
     count, width = cot_parts[0].shape
     half = count // 2
-    step = 512 if width % 512 == 0 else width
+    step = 1024 if width % 1024 == 0 else width
 
     def kernel(*refs):
         attended_refs, cot_refs, (out_ref, wide_ref) = refs[:blocks], refs[blocks:-2], refs[-2:]
@@ -667,7 +675,8 @@
     near_rows = [packed_t if m == 0 else swap(packed_t, "tp", m) for m in chip_masks]
     far_rows = [swap(rows, "tp", 1) for rows in near_rows]
     own_pieces = near_rows + far_rows
-    pair, own_cot = project_target(own_pieces, query_near, out_near)
+    pair = project_target(own_pieces, query_near, out_near)
+    pair_near, own_cot = hold_own(own_pieces, pair)
     pairs = [pair if k == 0 else swap(pair, "sp", k) for k in range(sp_count)]
 
     key_found = doubling(key_weight, "tp", far + near)
@@ -699,7 +708,7 @@
     near_cot = gather_cotangents(cot_near)
     cot_all = [own_cot, near_cot, swap(near_cot, "tp", 1)]
 
-    parts, own_stats, *scores = forward_all(pairs, kv)
+    parts, own_stats, *scores = forward_all([pair_near] + pairs[1:], kv)
     stats = [own_stats if k == 0 else swap(own_stats, "sp", k) for k in range(sp_count)]
     stats, *shares = combine_stats(stats, parts)
     order = list(range(sp_count // 2, sp_count)) + list(range(sp_count // 2 - 1, -1, -1))

time: 143 us -> 138 us (0.965)
  local copies, waits for them, and re-layouts: 6.71 us -> 3.5 us
  waiting for transfers between devices: 40.1 us -> 37.6 us
    unnamed x34 -> x30, local copies, waits for them, and re-layouts: 6.71 us -> 3.5 us
    ppermute x42, waiting for transfers between devices: 40.1 us -> 37.6 us  [swap(): return lax.ppermute(array, axis, [(i, i ^ mask) for i in range(size)])]
    pallas_call x18 -> x19, Pallas kernels: 33.6 us -> 34.6 us  [resident(): pl.pallas_call(kernel, out_shape=outs[0] if single else outs, in_specs=sp...]
  transfers between devices with their start and end apart: 44 -> 44, of which waited for: 14 -> 15; matrix products, arithmetic and copies ran while one was open for 0% -> 0% of each run, Pallas kernels for 24% -> 25%
where the time goes in v2:
time: 138 us; the launch traced here: 137 us
  starting transfers between devices  56.7 us (41%)
  Pallas kernels  38.7 us (28%)
  waiting for transfers between devices  37.6 us (27%)
  local copies, waits for them, and re-layouts  3.5 us (3%)
    ppermute x42, starting transfers between devices, swap(): return lax.ppermute(array, axis, [(i, i ^ mask) for i in range(size)])  49.3 us
    ppermute x42, waiting for transfers between devices, swap(): return lax.ppermute(array, axis, [(i, i ^ mask) for i in range(size)])  37.6 us
    pallas_call x19, Pallas kernels, resident(): pl.pallas_call(kernel, out_shape=outs[0] if single else outs, in_specs=sp...  34.6 us
    pallas_call x1, Pallas kernels, weight_grad(): pl.pallas_call(kernel, grid=(width // step,), in_specs=specs, out_specs=p...  4.06 us
    all_to_all x1, starting transfers between devices, body(): lax.all_to_all(kv_sums, 'tp', split_axis=0, concat_axis=0, tiled=True)  3.85 us
    all_to_all x1, starting transfers between devices, body(): kv = lax.all_to_all(packed, 'tp', split_axis=0, concat_axis=0, tiled=True)  3.59 us
    unnamed x30, local copies, waits for them, and re-layouts  3.5 us
  transfers between devices with their start and end apart: 44, of which 15 were waited for; matrix products, arithmetic and copies ran while one was open for 0% of the time, Pallas kernels for 25%

profile of v2, /device:TPU:0, one launch (start us, length us, event | category | flops | bytes accessed | tf_op | source)
XLA Modules:
  0.0 137.4 jit_solution(11249440976997567074)
XLA Ops:
  0.7 3.1 %collective-permute-start.11 = (bf16[256,512]{1,0:T(8,128)(2,1)}, bf16[256,512]{1,0:T(8,128)(2,1)S(1)}, u32[]{:S(2)}, u32[]{:S(2)}) collective-permute-start(bf16[256,512]{1,0:T(8,128)(2,1)} %refs_0_.5), channel_id=1, source_target_pairs={{0,4},{1,5},{2,6},{3,7},{4,0},{5,1},{6,2},{7,3},{8,12},{9,13},{10,... | collective-permute-start | bytes 786440 | tf_op jit(solution)/shard_map/ppermute | solution.py:39
  3.7 1.5 %collective-permute-start.12 = (bf16[256,512]{1,0:T(8,128)(2,1)}, bf16[256,512]{1,0:T(8,128)(2,1)S(1)}, u32[]{:S(2)}, u32[]{:S(2)}) collective-permute-start(bf16[256,512]{1,0:T(8,128)(2,1)} %refs_4_.3), channel_id=1, source_target_pairs={{0,2},{1,3},{2,0},{3,1},{4,6},{5,7},{6,4},{7,5},{8,10},{9,11},{10,... | collective-permute-start | bytes 786440 | tf_op jit(solution)/shard_map/ppermute | solution.py:39
  5.2 1.8 %shard_map.113 = (bf16[128,1024]{1,0:T(8,128)(2,1)S(1)}, bf16[128,1024]{1,0:T(8,128)(2,1)S(1)}, bf16[2048,256]{1,0:T(8,128)(2,1)S(1)}, bf16[256,2048]{1,0:T(8,128)(2,1)S(1)}) custom-call(s32[1]{0:T(128)} %bitcast.1.at_ref, bf16[128,2048]{1,0:T(8,128)(2,1)} %rows_ref.1, f32[1,2048]{1,0:T(1,128)} %bitcast.7, bf16[2048,256]{1,0:T(8,128)(2,1)} %refs_0_.3, ...), custom_call_target="tpu_custom_call" | custom-call | flops 2097152 | bytes 1048576 | tf_op jit(solution)/shard_map/pallas_call | solution.py:130
  7.7 3.0 %collective-permute-done.11.refs_1_.refs_2_ = bf16[256,512]{1,0:T(8,128)(2,1)S(1)} collective-permute-done((bf16[256,512]{1,0:T(8,128)(2,1)}, bf16[256,512]{1,0:T(8,128)(2,1)S(1)}, u32[]{:S(2)}, u32[]{:S(2)}) %collective-permute-start.11) | collective-permute-done | bytes 262176 | tf_op jit(solution)/shard_map/ppermute | solution.py:39
  10.7 1.4 %collective-permute-start.14 = (bf16[256,512]{1,0:T(8,128)(2,1)S(1)}, bf16[256,512]{1,0:T(8,128)(2,1)S(1)}, u32[]{:S(2)}, u32[]{:S(2)}) collective-permute-start(bf16[256,512]{1,0:T(8,128)(2,1)S(1)} %collective-permute-done.11.refs_1_.refs_2_), channel_id=1, source_target_pairs={{0,2},{1,3},{2,0},{3,1},{4,6},{5,7},{6,4},{7,5},{8,10},{9,11},{10,... | collective-permute-start | bytes 786440 | tf_op jit(solution)/shard_map/ppermute | solution.py:39
  12.1 0.9 collective-permute-done.12.refs_3_.refs_5_
  13.1 1.4 %collective-permute-start.16 = (bf16[256,512]{1,0:T(8,128)(2,1)S(1)}, bf16[256,512]{1,0:T(8,128)(2,1)S(1)}, u32[]{:S(2)}, u32[]{:S(2)}) collective-permute-start(bf16[256,512]{1,0:T(8,128)(2,1)S(1)} %collective-permute-done.12.refs_3_.refs_5_), channel_id=1, source_target_pairs={{0,4},{1,5},{2,6},{3,7},{4,0},{5,1},{6,2},{7,3},{8,12},{9,13},{10,... | collective-permute-start | bytes 786440 | tf_op jit(solution)/shard_map/ppermute | solution.py:39
  14.5 1.6 %collective-permute-start.35 = (bf16[24,2048]{1,0:T(8,128)(2,1)}, bf16[24,2048]{1,0:T(8,128)(2,1)S(1)}, u32[]{:S(2)}, u32[]{:S(2)}) collective-permute-start(bf16[24,2048]{1,0:T(8,128)(2,1)} %refs_5_.1), channel_id=1, source_target_pairs={{0,8},{8,0},{16,24},{24,16},{1,9},{9,1},{17,25},{25,17},{2,10},{10... | collective-permute-start | bytes 294920 | tf_op jit(solution)/shard_map/ppermute | solution.py:39
  16.1 2.6 %collective-permute-done.13.refs_2_.refs_1_ = bf16[256,512]{1,0:T(8,128)(2,1)S(1)} collective-permute-done((bf16[256,512]{1,0:T(8,128)(2,1)S(1)}, bf16[256,512]{1,0:T(8,128)(2,1)S(1)}, u32[]{:S(2)}, u32[]{:S(2)}) %collective-permute-start.13) | collective-permute-done | bytes 262176 | tf_op jit(solution)/shard_map/ppermute | solution.py:39
  18.7 2.6 %collective-permute-start.36 = (bf16[24,2048]{1,0:T(8,128)(2,1)}, bf16[24,2048]{1,0:T(8,128)(2,1)S(1)}, u32[]{:S(2)}, u32[]{:S(2)}) collective-permute-start(bf16[24,2048]{1,0:T(8,128)(2,1)} %refs_5_.1), channel_id=1, source_target_pairs={{0,16},{8,24},{16,0},{24,8},{1,17},{9,25},{17,1},{25,9},{2,18},{10... | collective-permute-start | bytes 294920 | tf_op jit(solution)/shard_map/ppermute | solution.py:39
  21.3 1.3 collective-permute-start.37
  22.7 1.0 shard_map.112.refs_0_
  23.7 1.6 %collective-permute-start = (bf16[2,24,2048]{2,1,0:T(8,128)(2,1)S(1)}, bf16[2,24,2048]{2,1,0:T(8,128)(2,1)S(1)}, u32[]{:S(2)}, u32[]{:S(2)}) collective-permute-start(bf16[2,24,2048]{2,1,0:T(8,128)(2,1)S(1)} %shard_map.112.refs_0_), channel_id=1, source_target_pairs={{0,2},{1,3},{2,0},{3,1},{4,6},{5,7},{6,4},{7,5},{8,10},{9,11},{10,... | collective-permute-start | bytes 589832 | tf_op jit(solution)/shard_map/ppermute | solution.py:39
  26.2 1.5 %shard_map.126.held_ref = bf16[2,4,256,512]{3,2,1,0:T(8,128)(2,1)} custom-call(bf16[256,512]{1,0:T(8,128)(2,1)S(1)} %copy-done.2, bf16[256,512]{1,0:T(8,128)(2,1)S(1)} %collective-permute-done.13.refs_2_.refs_1_, bf16[256,512]{1,0:T(8,128)(2,1)S(1)} %collective-permute-done.11.refs_1_.refs_2_, bf16[256,512]{1,0:T(8,128)(2,1)S(1)} %collective-permute-done.14.refs_3_, ...), custom_call_target="tpu_custom_call" | custom-call | flops 1048576 | bytes 1048576 | tf_op jit(solution)/shard_map/pallas_call | solution.py:130
  27.7 1.5 %collective-permute-start.2 = (bf16[2,24,2048]{2,1,0:T(8,128)(2,1)S(1)}, bf16[2,24,2048]{2,1,0:T(8,128)(2,1)S(1)}, u32[]{:S(2)}, u32[]{:S(2)}) collective-permute-start(bf16[2,24,2048]{2,1,0:T(8,128)(2,1)S(1)} %shard_map.112.refs_0_), channel_id=1, source_target_pairs={{0,6},{1,7},{2,4},{3,5},{4,2},{5,3},{6,0},{7,1},{8,14},{9,15},{10,... | collective-permute-start | bytes 589832 | tf_op jit(solution)/shard_map/ppermute | solution.py:39
  30.5 4.5 %collective-permute-done.1.refs_2_ = bf16[2,24,2048]{2,1,0:T(8,128)(2,1)S(1)} collective-permute-done((bf16[2,24,2048]{2,1,0:T(8,128)(2,1)S(1)}, bf16[2,24,2048]{2,1,0:T(8,128)(2,1)S(1)}, u32[]{:S(2)}, u32[]{:S(2)}) %collective-permute-start.1) | collective-permute-done | bytes 196640 | tf_op jit(solution)/shard_map/ppermute | solution.py:39
  35.5 0.7 shard_map.129.refs_3_
  37.4 2.4 %collective-permute-start.40 = (bf16[3,24,2048]{2,1,0:T(8,128)(2,1)}, bf16[3,24,2048]{2,1,0:T(8,128)(2,1)}, u32[]{:S(2)}, u32[]{:S(2)}) collective-permute-start(bf16[3,24,2048]{2,1,0:T(8,128)(2,1)} %shard_map.129.refs_3_), channel_id=1, source_target_pairs={{0,6},{1,7},{2,4},{3,5},{4,2},{5,3},{6,0},{7,1},{8,14},{9,15},{10,... | collective-permute-start | bytes 884744 | tf_op jit(solution)/shard_map/ppermute | solution.py:39
  39.8 0.7 shard_map.118
  40.6 3.6 %all-to-all-start = ((bf16[8,128,128]{2,1,0:T(8,128)(2,1)}), bf16[8,128,128]{2,1,0:T(8,128)(2,1)S(1)}, u32[]{:S(2)}, u32[]{:S(2)}) async-start(bf16[8,128,128]{2,1,0:T(8,128)(2,1)} %shard_map.118), calls=%async_computation | async-start | bytes 524288 | tf_op jit(solution)/shard_map/all_to_all | solution.py:702
  44.2 0.7 copy-done.9
  44.9 0.9 copy-done.5
  45.8 0.9 copy-done.7
  46.7 0.9 copy-done.10
  47.6 1.4 %shard_map.114.refs_8_.refs_1_ = bf16[128,768]{1,0:T(8,128)(2,1)} custom-call(bf16[2,24,2048]{2,1,0:T(8,128)(2,1)S(1)} %shard_map.112.refs_0_, bf16[2,24,2048]{2,1,0:T(8,128)(2,1)S(1)} %collective-permute-done.refs_1_, bf16[2,24,2048]{2,1,0:T(8,128)(2,1)S(1)} %copy-done.5, bf16[2,24,2048]{2,1,0:T(8,128)(2,1)S(1)} %collective-permute-done.2.refs_3_, ...), custom_call_target="tpu_custom_call" | custom-call | flops 402653184 | bytes 1048576 | tf_op jit(solution)/shard_map/pallas_call | solution.py:130
  49.1 1.9 %collective-permute-start.7 = (bf16[128,768]{1,0:T(8,128)(2,1)}, bf16[128,768]{1,0:T(8,128)(2,1)S(1)}, u32[]{:S(2)}, u32[]{:S(2)}) collective-permute-start(bf16[128,768]{1,0:T(8,128)(2,1)} %shard_map.114.refs_8_.refs_1_), channel_id=1, source_target_pairs={{0,16},{8,24},{16,0},{24,8},{1,17},{9,25},{17,1},{25,9},{2,18},{10... | collective-permute-start | bytes 589832 | tf_op jit(solution)/shard_map/ppermute | solution.py:39
  51.0 1.3 collective-permute-start.8
  52.3 1.0 collective-permute-start.9
  53.4 2.4 %shard_map.130.refs_5_ = bf16[288,2048]{1,0:T(8,128)(2,1)} custom-call(bf16[3,24,2048]{2,1,0:T(8,128)(2,1)} %collective-permute-done.38.refs_0_, bf16[3,24,2048]{2,1,0:T(8,128)(2,1)} %collective-permute-done.39.refs_1_, bf16[3,24,2048]{2,1,0:T(8,128)(2,1)} %collective-permute-done.40.refs_2_, bf16[3,24,2048]{2,1,0:T(8,128)(2,1)} %shard_map.129.refs_3_), custom_call_target="tpu_custom_call" | custom-call | flops 1048576 | bytes 1048576 | tf_op jit(solution)/shard_map/pallas_call | solution.py:130
  55.7 1.9 %shard_map.115 = (bf16[128,768]{1,0:T(8,128)(2,1)S(1)}, bf16[192,2048]{1,0:T(8,128)(2,1)}) custom-call(bf16[2,24,2048]{2,1,0:T(8,128)(2,1)S(1)} %shard_map.112.refs_0_, bf16[2,24,2048]{2,1,0:T(8,128)(2,1)S(1)} %collective-permute-done.refs_1_, bf16[2,24,2048]{2,1,0:T(8,128)(2,1)S(1)} %copy-done.5, bf16[2,24,2048]{2,1,0:T(8,128)(2,1)S(1)} %collective-permute-done.2.refs_3_, ...), custom_call_target="tpu_custom_call" | custom-call | flops 1048576 | bytes 1048576 | tf_op jit(solution)/shard_map/pallas_call | solution.py:130
  57.6 8.5 %collective-permute-done.7.refs_2_.refs_0_ = bf16[128,768]{1,0:T(8,128)(2,1)S(1)} collective-permute-done((bf16[128,768]{1,0:T(8,128)(2,1)}, bf16[128,768]{1,0:T(8,128)(2,1)S(1)}, u32[]{:S(2)}, u32[]{:S(2)}) %collective-permute-start.7) | collective-permute-done | bytes 196640 | tf_op jit(solution)/shard_map/ppermute | solution.py:39
  66.1 0.9 collective-permute-done.9.refs_1_.refs_0_
  67.0 4.0 %shard_map.119 = (f32[4,64,768]{2,1,0:T(8,128)S(1)}, f32[8,768]{1,0:T(8,128)S(1)}, f32[1024,768]{1,0:T(8,128)S(1)}, f32[1024,768]{1,0:T(8,128)S(1)}, f32[1024,768]{1,0:T(8,128)S(1)}, /*index=5*/f32[1024,768]{1,0:T(8,128)S(1)}) custom-call(bf16[128,768]{1,0:T(8,128)(2,1)S(1)} %get-tuple-element.38.refs_0_, ...), custom_call_target="tpu_custom_call" | custom-call | flops 1610612736 | bytes 1048576 | tf_op jit(solution)/shard_map/pallas_call | solution.py:130
  71.0 3.5 %collective-permute-start.18 = (f32[8,768]{1,0:T(8,128)S(1)}, f32[8,768]{1,0:T(8,128)S(1)}, u32[]{:S(2)}, u32[]{:S(2)}) collective-permute-start(f32[8,768]{1,0:T(8,128)S(1)} %get-tuple-element.47.refs_0_), channel_id=1, source_target_pairs={{0,8},{8,0},{16,24},{24,16},{1,9},{9,1},{17,25},{25,17},{2,10},{10... | collective-permute-start | bytes 73736 | tf_op jit(solution)/shard_map/ppermute | solution.py:39
  74.5 1.4 %collective-permute-start.19 = (f32[8,768]{1,0:T(8,128)S(1)}, f32[8,768]{1,0:T(8,128)S(1)}, u32[]{:S(2)}, u32[]{:S(2)}) collective-permute-start(f32[8,768]{1,0:T(8,128)S(1)} %get-tuple-element.47.refs_0_), channel_id=1, source_target_pairs={{0,16},{8,24},{16,0},{24,8},{1,17},{9,25},{17,1},{25,9},{2,18},{10... | collective-permute-start | bytes 73736 | tf_op jit(solution)/shard_map/ppermute | solution.py:39
  76.0 1.4 %collective-permute-start.20 = (f32[8,768]{1,0:T(8,128)S(1)}, f32[8,768]{1,0:T(8,128)S(1)}, u32[]{:S(2)}, u32[]{:S(2)}) collective-permute-start(f32[8,768]{1,0:T(8,128)S(1)} %get-tuple-element.47.refs_0_), channel_id=1, source_target_pairs={{0,24},{8,16},{16,8},{24,0},{1,25},{9,17},{17,9},{25,1},{2,26},{10... | collective-permute-start | bytes 73736 | tf_op jit(solution)/shard_map/ppermute | solution.py:39
  77.4 2.2 %collective-permute-done.19.refs_2_ = f32[8,768]{1,0:T(8,128)S(1)} collective-permute-done((f32[8,768]{1,0:T(8,128)S(1)}, f32[8,768]{1,0:T(8,128)S(1)}, u32[]{:S(2)}, u32[]{:S(2)}) %collective-permute-start.19) | collective-permute-done | bytes 24608 | tf_op jit(solution)/shard_map/ppermute | solution.py:39
  79.5 2.1 %collective-permute-done.20.refs_3_ = f32[8,768]{1,0:T(8,128)S(1)} collective-permute-done((f32[8,768]{1,0:T(8,128)S(1)}, f32[8,768]{1,0:T(8,128)S(1)}, u32[]{:S(2)}, u32[]{:S(2)}) %collective-permute-start.20) | collective-permute-done | bytes 24608 | tf_op jit(solution)/shard_map/ppermute | solution.py:39
  81.6 0.8 shard_map.120
  82.4 3.9 %shard_map.121 = (f32[1024,128]{1,0:T(8,128)S(1)}, bf16[64,768]{1,0:T(8,128)(2,1)}, bf16[64,768]{1,0:T(8,128)(2,1)}) custom-call(bf16[128,768]{1,0:T(8,128)(2,1)S(1)} %collective-permute-done.7.refs_2_.refs_0_, bf16[128,768]{1,0:T(8,128)(2,1)S(1)} %collective-permute-done.8.refs_3_.refs_1_, f32[1024,768]{1,0:T(8,128)S(1)} %get-tuple-element.45.refs_2_, ...), custom_call_target="tpu_custom_call" | custom-call | flops 2013265920 | bytes 1048576 | tf_op jit(solution)/shard_map/pallas_call | solution.py:130
  86.2 2.5 %collective-permute-start.22 = (bf16[64,768]{1,0:T(8,128)(2,1)}, bf16[64,768]{1,0:T(8,128)(2,1)S(1)}, u32[]{:S(2)}, u32[]{:S(2)}) collective-permute-start(bf16[64,768]{1,0:T(8,128)(2,1)} %get-tuple-element.51), channel_id=1, source_target_pairs={{0,24},{8,16},{16,8},{24,0},{1,25},{9,17},{17,9},{25,1},{2,26},{10... | collective-permute-start | bytes 294920 | tf_op jit(solution)/shard_map/ppermute | solution.py:39
  88.8 4.0 %shard_map.122 = (bf16[8,128,128]{2,1,0:T(8,128)(2,1)}, bf16[64,768]{1,0:T(8,128)(2,1)}, bf16[64,768]{1,0:T(8,128)(2,1)}) custom-call(bf16[128,768]{1,0:T(8,128)(2,1)S(1)} %collective-permute-done.9.refs_1_.refs_0_, bf16[128,768]{1,0:T(8,128)(2,1)S(1)} %copy-done.1, f32[1024,768]{1,0:T(8,128)S(1)} %get-tuple-element.52.refs_2_, ...), custom_call_target="tpu_custom_call" | custom-call | flops 2013265920 | bytes 1048576 | tf_op jit(solution)/shard_map/pallas_call | solution.py:130
  92.8 1.0 collective-permute-start.23
  93.7 1.0 collective-permute-done.21.refs_0_
  94.7 2.9 %collective-permute-done.23.refs_2_ = bf16[64,768]{1,0:T(8,128)(2,1)S(1)} collective-permute-done((bf16[64,768]{1,0:T(8,128)(2,1)}, bf16[64,768]{1,0:T(8,128)(2,1)S(1)}, u32[]{:S(2)}, u32[]{:S(2)}) %collective-permute-start.23) | collective-permute-done | bytes 98336 | tf_op jit(solution)/shard_map/ppermute | solution.py:39
  97.6 1.5 %shard_map.123 = (f32[96,2048]{1,0:T(8,128)S(1)}, bf16[96,2048]{1,0:T(8,128)(2,1)S(1)}) custom-call(bf16[64,768]{1,0:T(8,128)(2,1)S(1)} %collective-permute-done.21.refs_0_, bf16[64,768]{1,0:T(8,128)(2,1)S(1)} %collective-permute-done.22.refs_1_, bf16[64,768]{1,0:T(8,128)(2,1)S(1)} %collective-permute-done.23.refs_2_, ...), custom_call_target="tpu_custom_call" | custom-call | flops 201326592 | bytes 1048576 | tf_op jit(solution)/shard_map/pallas_call | solution.py:130
  99.2 1.0 collective-permute-start.29
  100.2 0.9 collective-permute-start.30
  101.1 4.2 %collective-permute-done.29.refs_0_ = bf16[64,768]{1,0:T(8,128)(2,1)S(1)} collective-permute-done((bf16[64,768]{1,0:T(8,128)(2,1)S(1)}, bf16[64,768]{1,0:T(8,128)(2,1)S(1)}, u32[]{:S(2)}, u32[]{:S(2)}) %collective-permute-start.29) | collective-permute-done | bytes 98336 | tf_op jit(solution)/shard_map/ppermute | solution.py:39
  105.3 2.1 %collective-permute-start.31 = (bf16[64,768]{1,0:T(8,128)(2,1)S(1)}, bf16[64,768]{1,0:T(8,128)(2,1)S(1)}, u32[]{:S(2)}, u32[]{:S(2)}) collective-permute-start(bf16[64,768]{1,0:T(8,128)(2,1)S(1)} %copy-done.12), channel_id=1, source_target_pairs={{0,24},{8,16},{16,8},{24,0},{1,25},{9,17},{17,9},{25,1},{2,26},{10... | collective-permute-start | bytes 294920 | tf_op jit(solution)/shard_map/ppermute | solution.py:39
  107.4 3.8 %all-to-all-start.1 = ((bf16[8,128,128]{2,1,0:T(8,128)(2,1)}), bf16[8,128,128]{2,1,0:T(8,128)(2,1)S(1)}, u32[]{:S(2)}, u32[]{:S(2)}) async-start(bf16[8,128,128]{2,1,0:T(8,128)(2,1)} %get-tuple-element.63), calls=%async_computation.1 | async-start | bytes 524288 | tf_op jit(solution)/shard_map/all_to_all | solution.py:722
  111.2 0.6 collective-permute-done.31.refs_2_
  111.8 0.9 shard_map.128.refs_0_
  112.8 1.1 collective-permute-start.32
  113.8 1.5 %collective-permute-start.33 = (bf16[64,768]{1,0:T(8,128)(2,1)S(1)}, bf16[64,768]{1,0:T(8,128)(2,1)S(1)}, u32[]{:S(2)}, u32[]{:S(2)}) collective-permute-start(bf16[64,768]{1,0:T(8,128)(2,1)S(1)} %shard_map.128.refs_0_), channel_id=1, source_target_pairs={{0,16},{8,24},{16,0},{24,8},{1,17},{9,25},{17,1},{25,9},{2,18},{10... | collective-permute-start | bytes 294920 | tf_op jit(solution)/shard_map/ppermute | solution.py:39
  115.3 1.9 %collective-permute-start.34 = (bf16[64,768]{1,0:T(8,128)(2,1)S(1)}, bf16[64,768]{1,0:T(8,128)(2,1)S(1)}, u32[]{:S(2)}, u32[]{:S(2)}) collective-permute-start(bf16[64,768]{1,0:T(8,128)(2,1)S(1)} %shard_map.128.refs_0_), channel_id=1, source_target_pairs={{0,24},{8,16},{16,8},{24,0},{1,25},{9,17},{17,9},{25,1},{2,26},{10... | collective-permute-start | bytes 294920 | tf_op jit(solution)/shard_map/ppermute | solution.py:39
  117.2 0.8 shard_map.124
  118.5 1.6 %collective-permute-start.25 = (bf16[24,2048]{1,0:T(8,128)(2,1)}, bf16[24,2048]{1,0:T(8,128)(2,1)S(1)}, u32[]{:S(2)}, u32[]{:S(2)}) collective-permute-start(bf16[24,2048]{1,0:T(8,128)(2,1)} %get-tuple-element.59), channel_id=1, source_target_pairs={{0,2},{1,3},{2,0},{3,1},{4,6},{5,7},{6,4},{7,5},{8,10},{9,11},{10,... | collective-permute-start | bytes 294920 | tf_op jit(solution)/shard_map/ppermute | solution.py:39
  120.1 3.6 %collective-permute-done.33.refs_2_ = bf16[64,768]{1,0:T(8,128)(2,1)S(1)} collective-permute-done((bf16[64,768]{1,0:T(8,128)(2,1)S(1)}, bf16[64,768]{1,0:T(8,128)(2,1)S(1)}, u32[]{:S(2)}, u32[]{:S(2)}) %collective-permute-start.33) | collective-permute-done | bytes 98336 | tf_op jit(solution)/shard_map/ppermute | solution.py:39
  123.7 1.6 %collective-permute-start.26 = (bf16[24,2048]{1,0:T(8,128)(2,1)}, bf16[24,2048]{1,0:T(8,128)(2,1)S(1)}, u32[]{:S(2)}, u32[]{:S(2)}) collective-permute-start(bf16[24,2048]{1,0:T(8,128)(2,1)} %get-tuple-element.60), channel_id=1, source_target_pairs={{0,4},{1,5},{2,6},{3,7},{4,0},{5,1},{6,2},{7,3},{8,12},{9,13},{10,... | collective-permute-start | bytes 294920 | tf_op jit(solution)/shard_map/ppermute | solution.py:39
  125.3 1.5 %collective-permute-start.27 = (bf16[24,2048]{1,0:T(8,128)(2,1)}, bf16[24,2048]{1,0:T(8,128)(2,1)S(1)}, u32[]{:S(2)}, u32[]{:S(2)}) collective-permute-start(bf16[24,2048]{1,0:T(8,128)(2,1)} %get-tuple-element.61), channel_id=1, source_target_pairs={{0,6},{1,7},{2,4},{3,5},{4,2},{5,3},{6,0},{7,1},{8,14},{9,15},{10,... | collective-permute-start | bytes 294920 | tf_op jit(solution)/shard_map/ppermute | solution.py:39
  126.8 4.1 %weight_grad.1 = f32[256,2048]{1,0:T(8,128)} custom-call(bf16[64,768]{1,0:T(8,128)(2,1)S(1)} %shard_map.128.refs_0_, bf16[64,768]{1,0:T(8,128)(2,1)S(1)} %collective-permute-done.32.refs_1_, bf16[64,768]{1,0:T(8,128)(2,1)S(1)} %collective-permute-done.33.refs_2_, bf16[64,768]{1,0:T(8,128)(2,1)S(1)} %collective-permute-done.34.refs_3_, ...), custom_call_target="tpu_custom_call" | custom-call | flops 805306368 | bytes 3145728 | tf_op jit(solution)/shard_map/weight_grad/pallas_call | solution.py:570
  131.1 1.9 %shard_map.125 = f32[24,2048]{1,0:T(8,128)} custom-call(bf16[24,2048]{1,0:T(8,128)(2,1)S(1)} %collective-permute-done.25.refs_0_, bf16[24,2048]{1,0:T(8,128)(2,1)S(1)} %collective-permute-done.26.refs_1_, bf16[24,2048]{1,0:T(8,128)(2,1)S(1)} %collective-permute-done.27.refs_2_, f32[24,2048]{1,0:T(8,128)} %get-tuple-element.62.refs_3_, ...), custom_call_target="tpu_custom_call" | custom-call | flops 1048576 | bytes 1048576 | tf_op jit(solution)/shard_map/pallas_call | solution.py:130
  133.0 4.5 %shard_map.127 = f32[128,2048]{1,0:T(8,128)} custom-call(s32[1]{0:T(128)} %bitcast.1.at_ref, bf16[8,128,128]{2,1,0:T(8,128)(2,1)S(1)} %all-to-all-done.1.back_ref, bf16[2,4,256,512]{3,2,1,0:T(8,128)(2,1)S(1)} %copy-done, bf16[2,4,256,512]{3,2,1,0:T(8,128)(2,1)} %collective-permute-done.28.other_ref, bf16[128,2048]{1,0:T(8,128)(2,1)} %rows_ref.1, ...), custom_call_target="tpu_custom_call" | custom-call | flops 536870912 | bytes 1048576 | tf_op jit(solution)/shard_map/pallas_call | solution.py:130
  (74 shorter events, 5.4 us)
Async XLA Ops:
  0.6 6.4 %copy-start.2 = (bf16[256,512]{1,0:T(8,128)(2,1)S(1)}, bf16[256,512]{1,0:T(8,128)(2,1)}, u32[]{:S(2)}) copy-start(bf16[256,512]{1,0:T(8,128)(2,1)} %refs_0_.5) | copy-start | bytes 786436
  0.6 7.0 %copy-start.3 = (bf16[256,512]{1,0:T(8,128)(2,1)S(1)}, bf16[256,512]{1,0:T(8,128)(2,1)}, u32[]{:S(2)}) copy-start(bf16[256,512]{1,0:T(8,128)(2,1)} %refs_4_.3) | copy-start | bytes 786436
  0.7 10.1 %collective-permute-start.11 = (bf16[256,512]{1,0:T(8,128)(2,1)}, bf16[256,512]{1,0:T(8,128)(2,1)S(1)}, u32[]{:S(2)}, u32[]{:S(2)}) collective-permute-start(bf16[256,512]{1,0:T(8,128)(2,1)} %refs_0_.5), channel_id=1, source_target_pairs={{0,4},{1,5},{2,6},{3,7},{4,0},{5,1},{6,2},{7,3},{8,12},{9,13},{10,... | collective-permute-start | bytes 786440 | tf_op jit(solution)/shard_map/ppermute | solution.py:39
  3.7 9.4 %collective-permute-start.12 = (bf16[256,512]{1,0:T(8,128)(2,1)}, bf16[256,512]{1,0:T(8,128)(2,1)S(1)}, u32[]{:S(2)}, u32[]{:S(2)}) collective-permute-start(bf16[256,512]{1,0:T(8,128)(2,1)} %refs_4_.3), channel_id=1, source_target_pairs={{0,2},{1,3},{2,0},{3,1},{4,6},{5,7},{6,4},{7,5},{8,10},{9,11},{10,... | collective-permute-start | bytes 786440 | tf_op jit(solution)/shard_map/ppermute | solution.py:39
  7.0 7.6 %collective-permute-start.10 = (bf16[128,1024]{1,0:T(8,128)(2,1)S(1)}, bf16[128,1024]{1,0:T(8,128)(2,1)S(1)}, u32[]{:S(2)}, u32[]{:S(2)}) collective-permute-start(bf16[128,1024]{1,0:T(8,128)(2,1)S(1)} %get-tuple-element.40), channel_id=1, source_target_pairs={{0,1},{1,0},{2,3},{3,2},{4,5},{5,4},{6,7},{7,6},{8,9},{9,8},{10,11... | collective-permute-start | bytes 786440 | tf_op jit(solution)/shard_map/ppermute | solution.py:39
  7.1 11.7 %collective-permute-start.13 = (bf16[256,512]{1,0:T(8,128)(2,1)S(1)}, bf16[256,512]{1,0:T(8,128)(2,1)S(1)}, u32[]{:S(2)}, u32[]{:S(2)}) collective-permute-start(bf16[256,512]{1,0:T(8,128)(2,1)S(1)} %copy-done.2), channel_id=1, source_target_pairs={{0,2},{1,3},{2,0},{3,1},{4,6},{5,7},{6,4},{7,5},{8,10},{9,11},{10,... | collective-permute-start | bytes 786440 | tf_op jit(solution)/shard_map/ppermute | solution.py:39
  7.7 13.7 %collective-permute-start.15 = (bf16[256,512]{1,0:T(8,128)(2,1)S(1)}, bf16[256,512]{1,0:T(8,128)(2,1)S(1)}, u32[]{:S(2)}, u32[]{:S(2)}) collective-permute-start(bf16[256,512]{1,0:T(8,128)(2,1)S(1)} %copy-done.3), channel_id=1, source_target_pairs={{0,4},{1,5},{2,6},{3,7},{4,0},{5,1},{6,2},{7,3},{8,12},{9,13},{10,... | collective-permute-start | bytes 786440 | tf_op jit(solution)/shard_map/ppermute | solution.py:39
  10.7 13.0 %collective-permute-start.14 = (bf16[256,512]{1,0:T(8,128)(2,1)S(1)}, bf16[256,512]{1,0:T(8,128)(2,1)S(1)}, u32[]{:S(2)}, u32[]{:S(2)}) collective-permute-start(bf16[256,512]{1,0:T(8,128)(2,1)S(1)} %collective-permute-done.11.refs_1_.refs_2_), channel_id=1, source_target_pairs={{0,2},{1,3},{2,0},{3,1},{4,6},{5,7},{6,4},{7,5},{8,10},{9,11},{10,... | collective-permute-start | bytes 786440 | tf_op jit(solution)/shard_map/ppermute | solution.py:39
  13.1 12.2 %collective-permute-start.16 = (bf16[256,512]{1,0:T(8,128)(2,1)S(1)}, bf16[256,512]{1,0:T(8,128)(2,1)S(1)}, u32[]{:S(2)}, u32[]{:S(2)}) collective-permute-start(bf16[256,512]{1,0:T(8,128)(2,1)S(1)} %collective-permute-done.12.refs_3_.refs_5_), channel_id=1, source_target_pairs={{0,4},{1,5},{2,6},{3,7},{4,0},{5,1},{6,2},{7,3},{8,12},{9,13},{10,... | collective-permute-start | bytes 786440 | tf_op jit(solution)/shard_map/ppermute | solution.py:39
  14.5 13.2 %collective-permute-start.35 = (bf16[24,2048]{1,0:T(8,128)(2,1)}, bf16[24,2048]{1,0:T(8,128)(2,1)S(1)}, u32[]{:S(2)}, u32[]{:S(2)}) collective-permute-start(bf16[24,2048]{1,0:T(8,128)(2,1)} %refs_5_.1), channel_id=1, source_target_pairs={{0,8},{8,0},{16,24},{24,16},{1,9},{9,1},{17,25},{25,17},{2,10},{10... | collective-permute-start | bytes 294920 | tf_op jit(solution)/shard_map/ppermute | solution.py:39
  18.7 10.5 %collective-permute-start.36 = (bf16[24,2048]{1,0:T(8,128)(2,1)}, bf16[24,2048]{1,0:T(8,128)(2,1)S(1)}, u32[]{:S(2)}, u32[]{:S(2)}) collective-permute-start(bf16[24,2048]{1,0:T(8,128)(2,1)} %refs_5_.1), channel_id=1, source_target_pairs={{0,16},{8,24},{16,0},{24,8},{1,17},{9,25},{17,1},{25,9},{2,18},{10... | collective-permute-start | bytes 294920 | tf_op jit(solution)/shard_map/ppermute | solution.py:39
  21.3 8.5 %collective-permute-start.37 = (bf16[24,2048]{1,0:T(8,128)(2,1)}, bf16[24,2048]{1,0:T(8,128)(2,1)S(1)}, u32[]{:S(2)}, u32[]{:S(2)}) collective-permute-start(bf16[24,2048]{1,0:T(8,128)(2,1)} %refs_5_.1), channel_id=1, source_target_pairs={{0,24},{8,16},{16,8},{24,0},{1,25},{9,17},{17,9},{25,1},{2,26},{10... | collective-permute-start | bytes 294920 | tf_op jit(solution)/shard_map/ppermute | solution.py:39
  23.7 6.7 %collective-permute-start = (bf16[2,24,2048]{2,1,0:T(8,128)(2,1)S(1)}, bf16[2,24,2048]{2,1,0:T(8,128)(2,1)S(1)}, u32[]{:S(2)}, u32[]{:S(2)}) collective-permute-start(bf16[2,24,2048]{2,1,0:T(8,128)(2,1)S(1)} %shard_map.112.refs_0_), channel_id=1, source_target_pairs={{0,2},{1,3},{2,0},{3,1},{4,6},{5,7},{6,4},{7,5},{8,10},{9,11},{10,... | collective-permute-start | bytes 589832 | tf_op jit(solution)/shard_map/ppermute | solution.py:39
  25.3 9.7 %collective-permute-start.1 = (bf16[2,24,2048]{2,1,0:T(8,128)(2,1)S(1)}, bf16[2,24,2048]{2,1,0:T(8,128)(2,1)S(1)}, u32[]{:S(2)}, u32[]{:S(2)}) collective-permute-start(bf16[2,24,2048]{2,1,0:T(8,128)(2,1)S(1)} %shard_map.112.refs_0_), channel_id=1, source_target_pairs={{0,4},{1,5},{2,6},{3,7},{4,0},{5,1},{6,2},{7,3},{8,12},{9,13},{10,... | collective-permute-start | bytes 589832 | tf_op jit(solution)/shard_map/ppermute | solution.py:39
  27.7 7.3 %collective-permute-start.2 = (bf16[2,24,2048]{2,1,0:T(8,128)(2,1)S(1)}, bf16[2,24,2048]{2,1,0:T(8,128)(2,1)S(1)}, u32[]{:S(2)}, u32[]{:S(2)}) collective-permute-start(bf16[2,24,2048]{2,1,0:T(8,128)(2,1)S(1)} %shard_map.112.refs_0_), channel_id=1, source_target_pairs={{0,6},{1,7},{2,4},{3,5},{4,2},{5,3},{6,0},{7,1},{8,14},{9,15},{10,... | collective-permute-start | bytes 589832 | tf_op jit(solution)/shard_map/ppermute | solution.py:39
  29.2 103.8 %collective-permute-start.28 = (bf16[2,4,256,512]{3,2,1,0:T(8,128)(2,1)}, bf16[2,4,256,512]{3,2,1,0:T(8,128)(2,1)}, u32[]{:S(2)}, u32[]{:S(2)}) collective-permute-start(bf16[2,4,256,512]{3,2,1,0:T(8,128)(2,1)} %shard_map.126.held_ref), channel_id=1, source_target_pairs={{0,1},{1,0},{2,3},{3,2},{4,5},{5,4},{6,7},{7,6},{8,9},{9,8},{10,11... | collective-permute-start | bytes 6291464 | tf_op jit(solution)/shard_map/ppermute | solution.py:39
  29.8 7.6 %collective-permute-start.17 = (f32[8,128,128]{2,1,0:T(8,128)S(1)}, f32[8,128,128]{2,1,0:T(8,128)S(1)}, u32[]{:S(2)}, u32[]{:S(2)}) collective-permute-start(f32[8,128,128]{2,1,0:T(8,128)S(1)} %get-tuple-element.44), channel_id=1, source_target_pairs={{0,1},{1,0},{2,3},{3,2},{4,5},{5,4},{6,7},{7,6},{8,9},{9,8},{10,11... | collective-permute-start | bytes 1572872 | tf_op jit(solution)/shard_map/ppermute | solution.py:39
  30.4 5.8 %collective-permute-start.3 = (bf16[2,24,2048]{2,1,0:T(8,128)(2,1)S(1)}, bf16[2,24,2048]{2,1,0:T(8,128)(2,1)S(1)}, u32[]{:S(2)}, u32[]{:S(2)}) collective-permute-start(bf16[2,24,2048]{2,1,0:T(8,128)(2,1)S(1)} %shard_map.112.refs_0_), channel_id=1, source_target_pairs={{0,1},{1,0},{2,3},{3,2},{4,5},{5,4},{6,7},{7,6},{8,9},{9,8},{10,11... | collective-permute-start | bytes 589832 | tf_op jit(solution)/shard_map/ppermute | solution.py:39
  35.0 1.9 %copy-start.4 = (bf16[2,24,2048]{2,1,0:T(8,128)(2,1)}, bf16[2,24,2048]{2,1,0:T(8,128)(2,1)S(1)}, u32[]{:S(2)}) copy-start(bf16[2,24,2048]{2,1,0:T(8,128)(2,1)S(1)} %collective-permute-done.1.refs_2_) | copy-start | bytes 589828
  35.0 1.9 %collective-permute-start.4 = (bf16[2,24,2048]{2,1,0:T(8,128)(2,1)S(1)}, bf16[2,24,2048]{2,1,0:T(8,128)(2,1)S(1)}, u32[]{:S(2)}, u32[]{:S(2)}) collective-permute-start(bf16[2,24,2048]{2,1,0:T(8,128)(2,1)S(1)} %collective-permute-done.refs_1_), channel_id=1, source_target_pairs={{0,1},{1,0},{2,3},{3,2},{4,5},{5,4},{6,7},{7,6},{8,9},{9,8},{10,11... | collective-permute-start | bytes 589832 | tf_op jit(solution)/shard_map/ppermute | solution.py:39
  35.0 2.4 %collective-permute-start.5 = (bf16[2,24,2048]{2,1,0:T(8,128)(2,1)S(1)}, bf16[2,24,2048]{2,1,0:T(8,128)(2,1)S(1)}, u32[]{:S(2)}, u32[]{:S(2)}) collective-permute-start(bf16[2,24,2048]{2,1,0:T(8,128)(2,1)S(1)} %collective-permute-done.1.refs_2_), channel_id=1, source_target_pairs={{0,1},{1,0},{2,3},{3,2},{4,5},{5,4},{6,7},{7,6},{8,9},{9,8},{10,11... | collective-permute-start | bytes 589832 | tf_op jit(solution)/shard_map/ppermute | solution.py:39
  36.2 14.7 %collective-permute-start.38 = (bf16[3,24,2048]{2,1,0:T(8,128)(2,1)}, bf16[3,24,2048]{2,1,0:T(8,128)(2,1)}, u32[]{:S(2)}, u32[]{:S(2)}) collective-permute-start(bf16[3,24,2048]{2,1,0:T(8,128)(2,1)} %shard_map.129.refs_3_), channel_id=1, source_target_pairs={{0,2},{1,3},{2,0},{3,1},{4,6},{5,7},{6,4},{7,5},{8,10},{9,11},{10,... | collective-permute-start | bytes 884744 | tf_op jit(solution)/shard_map/ppermute | solution.py:39
  36.8 15.5 %collective-permute-start.39 = (bf16[3,24,2048]{2,1,0:T(8,128)(2,1)}, bf16[3,24,2048]{2,1,0:T(8,128)(2,1)}, u32[]{:S(2)}, u32[]{:S(2)}) collective-permute-start(bf16[3,24,2048]{2,1,0:T(8,128)(2,1)} %shard_map.129.refs_3_), channel_id=1, source_target_pairs={{0,4},{1,5},{2,6},{3,7},{4,0},{5,1},{6,2},{7,3},{8,12},{9,13},{10,... | collective-permute-start | bytes 884744 | tf_op jit(solution)/shard_map/ppermute | solution.py:39
  37.4 3.2 %copy-start.6 = (bf16[2,24,2048]{2,1,0:T(8,128)(2,1)}, bf16[2,24,2048]{2,1,0:T(8,128)(2,1)S(1)}, u32[]{:S(2)}) copy-start(bf16[2,24,2048]{2,1,0:T(8,128)(2,1)S(1)} %collective-permute-done.5.refs_6_) | copy-start | bytes 589828
  37.4 6.8 %collective-permute-start.6 = (bf16[2,24,2048]{2,1,0:T(8,128)(2,1)S(1)}, bf16[2,24,2048]{2,1,0:T(8,128)(2,1)S(1)}, u32[]{:S(2)}, u32[]{:S(2)}) collective-permute-start(bf16[2,24,2048]{2,1,0:T(8,128)(2,1)S(1)} %collective-permute-done.2.refs_3_), channel_id=1, source_target_pairs={{0,1},{1,0},{2,3},{3,2},{4,5},{5,4},{6,7},{7,6},{8,9},{9,8},{10,11... | collective-permute-start | bytes 589832 | tf_op jit(solution)/shard_map/ppermute | solution.py:39
  37.4 16.0 %collective-permute-start.40 = (bf16[3,24,2048]{2,1,0:T(8,128)(2,1)}, bf16[3,24,2048]{2,1,0:T(8,128)(2,1)}, u32[]{:S(2)}, u32[]{:S(2)}) collective-permute-start(bf16[3,24,2048]{2,1,0:T(8,128)(2,1)} %shard_map.129.refs_3_), channel_id=1, source_target_pairs={{0,6},{1,7},{2,4},{3,5},{4,2},{5,3},{6,0},{7,1},{8,14},{9,15},{10,... | collective-permute-start | bytes 884744 | tf_op jit(solution)/shard_map/ppermute | solution.py:39
  40.6 26.4 %all-to-all-start = ((bf16[8,128,128]{2,1,0:T(8,128)(2,1)}), bf16[8,128,128]{2,1,0:T(8,128)(2,1)S(1)}, u32[]{:S(2)}, u32[]{:S(2)}) async-start(bf16[8,128,128]{2,1,0:T(8,128)(2,1)} %shard_map.118), calls=%async_computation | async-start | bytes 524288 | tf_op jit(solution)/shard_map/all_to_all | solution.py:702
  44.2 0.7 copy-start.9
  44.9 0.9 copy-start.5
  45.8 0.9 copy-start.7
  46.7 0.9 copy-start.10
  49.1 6.7 %copy-start.8 = (bf16[2,24,2048]{2,1,0:T(8,128)(2,1)S(1)}, bf16[2,24,2048]{2,1,0:T(8,128)(2,1)}, u32[]{:S(2)}) copy-start(bf16[2,24,2048]{2,1,0:T(8,128)(2,1)} %copy-done.6) | copy-start | bytes 589828
  49.1 6.7 %copy-start.11 = (bf16[2,24,2048]{2,1,0:T(8,128)(2,1)S(1)}, bf16[2,24,2048]{2,1,0:T(8,128)(2,1)}, u32[]{:S(2)}) copy-start(bf16[2,24,2048]{2,1,0:T(8,128)(2,1)} %copy-done.9) | copy-start | bytes 589828
  49.1 17.0 %collective-permute-start.7 = (bf16[128,768]{1,0:T(8,128)(2,1)}, bf16[128,768]{1,0:T(8,128)(2,1)S(1)}, u32[]{:S(2)}, u32[]{:S(2)}) collective-permute-start(bf16[128,768]{1,0:T(8,128)(2,1)} %shard_map.114.refs_8_.refs_1_), channel_id=1, source_target_pairs={{0,16},{8,24},{16,0},{24,8},{1,17},{9,25},{17,1},{25,9},{2,18},{10... | collective-permute-start | bytes 589832 | tf_op jit(solution)/shard_map/ppermute | solution.py:39
  51.0 15.1 %collective-permute-start.8 = (bf16[128,768]{1,0:T(8,128)(2,1)}, bf16[128,768]{1,0:T(8,128)(2,1)S(1)}, u32[]{:S(2)}, u32[]{:S(2)}) collective-permute-start(bf16[128,768]{1,0:T(8,128)(2,1)} %shard_map.114.refs_8_.refs_1_), channel_id=1, source_target_pairs={{0,24},{8,16},{16,8},{24,0},{1,25},{9,17},{17,9},{25,1},{2,26},{10... | collective-permute-start | bytes 589832 | tf_op jit(solution)/shard_map/ppermute | solution.py:39
  52.3 14.7 %collective-permute-start.9 = (bf16[128,768]{1,0:T(8,128)(2,1)}, bf16[128,768]{1,0:T(8,128)(2,1)S(1)}, u32[]{:S(2)}, u32[]{:S(2)}) collective-permute-start(bf16[128,768]{1,0:T(8,128)(2,1)} %shard_map.114.refs_8_.refs_1_), channel_id=1, source_target_pairs={{0,8},{8,0},{16,24},{24,16},{1,9},{9,1},{17,25},{25,17},{2,10},{10... | collective-permute-start | bytes 589832 | tf_op jit(solution)/shard_map/ppermute | solution.py:39
  55.7 71.1 %collective-permute-start.41 = (bf16[288,2048]{1,0:T(8,128)(2,1)}, bf16[288,2048]{1,0:T(8,128)(2,1)}, u32[]{:S(2)}, u32[]{:S(2)}) collective-permute-start(bf16[288,2048]{1,0:T(8,128)(2,1)} %shard_map.130.refs_5_), channel_id=1, source_target_pairs={{0,1},{1,0},{2,3},{3,2},{4,5},{5,4},{6,7},{7,6},{8,9},{9,8},{10,11... | collective-permute-start | bytes 3538952 | tf_op jit(solution)/shard_map/ppermute | solution.py:39
  71.0 6.3 %collective-permute-start.18 = (f32[8,768]{1,0:T(8,128)S(1)}, f32[8,768]{1,0:T(8,128)S(1)}, u32[]{:S(2)}, u32[]{:S(2)}) collective-permute-start(f32[8,768]{1,0:T(8,128)S(1)} %get-tuple-element.47.refs_0_), channel_id=1, source_target_pairs={{0,8},{8,0},{16,24},{24,16},{1,9},{9,1},{17,25},{25,17},{2,10},{10... | collective-permute-start | bytes 73736 | tf_op jit(solution)/shard_map/ppermute | solution.py:39
  74.5 5.0 %collective-permute-start.19 = (f32[8,768]{1,0:T(8,128)S(1)}, f32[8,768]{1,0:T(8,128)S(1)}, u32[]{:S(2)}, u32[]{:S(2)}) collective-permute-start(f32[8,768]{1,0:T(8,128)S(1)} %get-tuple-element.47.refs_0_), channel_id=1, source_target_pairs={{0,16},{8,24},{16,0},{24,8},{1,17},{9,25},{17,1},{25,9},{2,18},{10... | collective-permute-start | bytes 73736 | tf_op jit(solution)/shard_map/ppermute | solution.py:39
  76.0 5.6 %collective-permute-start.20 = (f32[8,768]{1,0:T(8,128)S(1)}, f32[8,768]{1,0:T(8,128)S(1)}, u32[]{:S(2)}, u32[]{:S(2)}) collective-permute-start(f32[8,768]{1,0:T(8,128)S(1)} %get-tuple-element.47.refs_0_), channel_id=1, source_target_pairs={{0,24},{8,16},{16,8},{24,0},{1,25},{9,17},{17,9},{25,1},{2,26},{10... | collective-permute-start | bytes 73736 | tf_op jit(solution)/shard_map/ppermute | solution.py:39
  82.4 6.4 %copy-start.1 = (bf16[128,768]{1,0:T(8,128)(2,1)S(1)}, bf16[128,768]{1,0:T(8,128)(2,1)}, u32[]{:S(2)}) copy-start(bf16[128,768]{1,0:T(8,128)(2,1)} %shard_map.114.refs_8_.refs_1_) | copy-start | bytes 589828
  86.2 8.5 %collective-permute-start.21 = (bf16[64,768]{1,0:T(8,128)(2,1)}, bf16[64,768]{1,0:T(8,128)(2,1)S(1)}, u32[]{:S(2)}, u32[]{:S(2)}) collective-permute-start(bf16[64,768]{1,0:T(8,128)(2,1)} %get-tuple-element.50), channel_id=1, source_target_pairs={{0,16},{8,24},{16,0},{24,8},{1,17},{9,25},{17,1},{25,9},{2,18},{10... | collective-permute-start | bytes 294920 | tf_op jit(solution)/shard_map/ppermute | solution.py:39
  86.2 8.5 %collective-permute-start.22 = (bf16[64,768]{1,0:T(8,128)(2,1)}, bf16[64,768]{1,0:T(8,128)(2,1)S(1)}, u32[]{:S(2)}, u32[]{:S(2)}) collective-permute-start(bf16[64,768]{1,0:T(8,128)(2,1)} %get-tuple-element.51), channel_id=1, source_target_pairs={{0,24},{8,16},{16,8},{24,0},{1,25},{9,17},{17,9},{25,1},{2,26},{10... | collective-permute-start | bytes 294920 | tf_op jit(solution)/shard_map/ppermute | solution.py:39
  88.8 10.4 %copy-start.14 = (bf16[64,768]{1,0:T(8,128)(2,1)S(1)}, bf16[64,768]{1,0:T(8,128)(2,1)}, u32[]{:S(2)}) copy-start(bf16[64,768]{1,0:T(8,128)(2,1)} %get-tuple-element.64) | copy-start | bytes 294916
  88.8 11.4 %copy-start.13 = (bf16[64,768]{1,0:T(8,128)(2,1)S(1)}, bf16[64,768]{1,0:T(8,128)(2,1)}, u32[]{:S(2)}) copy-start(bf16[64,768]{1,0:T(8,128)(2,1)} %get-tuple-element.65) | copy-start | bytes 294916
  88.8 16.5 %copy-start.12 = (bf16[64,768]{1,0:T(8,128)(2,1)S(1)}, bf16[64,768]{1,0:T(8,128)(2,1)}, u32[]{:S(2)}) copy-start(bf16[64,768]{1,0:T(8,128)(2,1)} %get-tuple-element.66) | copy-start | bytes 294916
  92.8 4.8 %collective-permute-start.23 = (bf16[64,768]{1,0:T(8,128)(2,1)}, bf16[64,768]{1,0:T(8,128)(2,1)S(1)}, u32[]{:S(2)}, u32[]{:S(2)}) collective-permute-start(bf16[64,768]{1,0:T(8,128)(2,1)} %get-tuple-element.55), channel_id=1, source_target_pairs={{0,8},{8,0},{16,24},{24,16},{1,9},{9,1},{17,25},{25,17},{2,10},{10... | collective-permute-start | bytes 294920 | tf_op jit(solution)/shard_map/ppermute | solution.py:39
  99.1 16.3 %collective-permute-start.24 = (bf16[96,2048]{1,0:T(8,128)(2,1)S(1)}, bf16[96,2048]{1,0:T(8,128)(2,1)S(1)}, u32[]{:S(2)}, u32[]{:S(2)}) collective-permute-start(bf16[96,2048]{1,0:T(8,128)(2,1)S(1)} %get-tuple-element.58), channel_id=1, source_target_pairs={{0,1},{1,0},{2,3},{3,2},{4,5},{5,4},{6,7},{7,6},{8,9},{9,8},{10,11... | collective-permute-start | bytes 1179656 | tf_op jit(solution)/shard_map/ppermute | solution.py:39
  99.2 6.1 %collective-permute-start.29 = (bf16[64,768]{1,0:T(8,128)(2,1)S(1)}, bf16[64,768]{1,0:T(8,128)(2,1)S(1)}, u32[]{:S(2)}, u32[]{:S(2)}) collective-permute-start(bf16[64,768]{1,0:T(8,128)(2,1)S(1)} %copy-done.14), channel_id=1, source_target_pairs={{0,8},{8,0},{16,24},{24,16},{1,9},{9,1},{17,25},{25,17},{2,10},{10... | collective-permute-start | bytes 294920 | tf_op jit(solution)/shard_map/ppermute | solution.py:39
  100.2 11.0 %collective-permute-start.30 = (bf16[64,768]{1,0:T(8,128)(2,1)S(1)}, bf16[64,768]{1,0:T(8,128)(2,1)S(1)}, u32[]{:S(2)}, u32[]{:S(2)}) collective-permute-start(bf16[64,768]{1,0:T(8,128)(2,1)S(1)} %copy-done.13), channel_id=1, source_target_pairs={{0,16},{8,24},{16,0},{24,8},{1,17},{9,25},{17,1},{25,9},{2,18},{10... | collective-permute-start | bytes 294920 | tf_op jit(solution)/shard_map/ppermute | solution.py:39
  105.3 6.5 %collective-permute-start.31 = (bf16[64,768]{1,0:T(8,128)(2,1)S(1)}, bf16[64,768]{1,0:T(8,128)(2,1)S(1)}, u32[]{:S(2)}, u32[]{:S(2)}) collective-permute-start(bf16[64,768]{1,0:T(8,128)(2,1)S(1)} %copy-done.12), channel_id=1, source_target_pairs={{0,24},{8,16},{16,8},{24,0},{1,25},{9,17},{17,9},{25,1},{2,26},{10... | collective-permute-start | bytes 294920 | tf_op jit(solution)/shard_map/ppermute | solution.py:39
  107.4 25.6 %all-to-all-start.1 = ((bf16[8,128,128]{2,1,0:T(8,128)(2,1)}), bf16[8,128,128]{2,1,0:T(8,128)(2,1)S(1)}, u32[]{:S(2)}, u32[]{:S(2)}) async-start(bf16[8,128,128]{2,1,0:T(8,128)(2,1)} %get-tuple-element.63), calls=%async_computation.1 | async-start | bytes 524288 | tf_op jit(solution)/shard_map/all_to_all | solution.py:722
  112.8 5.7 %collective-permute-start.32 = (bf16[64,768]{1,0:T(8,128)(2,1)S(1)}, bf16[64,768]{1,0:T(8,128)(2,1)S(1)}, u32[]{:S(2)}, u32[]{:S(2)}) collective-permute-start(bf16[64,768]{1,0:T(8,128)(2,1)S(1)} %shard_map.128.refs_0_), channel_id=1, source_target_pairs={{0,8},{8,0},{16,24},{24,16},{1,9},{9,1},{17,25},{25,17},{2,10},{10... | collective-permute-start | bytes 294920 | tf_op jit(solution)/shard_map/ppermute | solution.py:39
  113.8 9.9 %collective-permute-start.33 = (bf16[64,768]{1,0:T(8,128)(2,1)S(1)}, bf16[64,768]{1,0:T(8,128)(2,1)S(1)}, u32[]{:S(2)}, u32[]{:S(2)}) collective-permute-start(bf16[64,768]{1,0:T(8,128)(2,1)S(1)} %shard_map.128.refs_0_), channel_id=1, source_target_pairs={{0,16},{8,24},{16,0},{24,8},{1,17},{9,25},{17,1},{25,9},{2,18},{10... | collective-permute-start | bytes 294920 | tf_op jit(solution)/shard_map/ppermute | solution.py:39
  115.3 10.0 %collective-permute-start.34 = (bf16[64,768]{1,0:T(8,128)(2,1)S(1)}, bf16[64,768]{1,0:T(8,128)(2,1)S(1)}, u32[]{:S(2)}, u32[]{:S(2)}) collective-permute-start(bf16[64,768]{1,0:T(8,128)(2,1)S(1)} %shard_map.128.refs_0_), channel_id=1, source_target_pairs={{0,24},{8,16},{16,8},{24,0},{1,25},{9,17},{17,9},{25,1},{2,26},{10... | collective-permute-start | bytes 294920 | tf_op jit(solution)/shard_map/ppermute | solution.py:39
  118.5 12.4 %collective-permute-start.25 = (bf16[24,2048]{1,0:T(8,128)(2,1)}, bf16[24,2048]{1,0:T(8,128)(2,1)S(1)}, u32[]{:S(2)}, u32[]{:S(2)}) collective-permute-start(bf16[24,2048]{1,0:T(8,128)(2,1)} %get-tuple-element.59), channel_id=1, source_target_pairs={{0,2},{1,3},{2,0},{3,1},{4,6},{5,7},{6,4},{7,5},{8,10},{9,11},{10,... | collective-permute-start | bytes 294920 | tf_op jit(solution)/shard_map/ppermute | solution.py:39
  123.7 7.2 %collective-permute-start.26 = (bf16[24,2048]{1,0:T(8,128)(2,1)}, bf16[24,2048]{1,0:T(8,128)(2,1)S(1)}, u32[]{:S(2)}, u32[]{:S(2)}) collective-permute-start(bf16[24,2048]{1,0:T(8,128)(2,1)} %get-tuple-element.60), channel_id=1, source_target_pairs={{0,4},{1,5},{2,6},{3,7},{4,0},{5,1},{6,2},{7,3},{8,12},{9,13},{10,... | collective-permute-start | bytes 294920 | tf_op jit(solution)/shard_map/ppermute | solution.py:39
  125.3 5.7 %collective-permute-start.27 = (bf16[24,2048]{1,0:T(8,128)(2,1)}, bf16[24,2048]{1,0:T(8,128)(2,1)S(1)}, u32[]{:S(2)}, u32[]{:S(2)}) collective-permute-start(bf16[24,2048]{1,0:T(8,128)(2,1)} %get-tuple-element.61), channel_id=1, source_target_pairs={{0,6},{1,7},{2,4},{3,5},{4,2},{5,3},{6,0},{7,1},{8,14},{9,15},{10,... | collective-permute-start | bytes 294920 | tf_op jit(solution)/shard_map/ppermute | solution.py:39
  126.8 6.2 %copy-start = (bf16[2,4,256,512]{3,2,1,0:T(8,128)(2,1)S(1)}, bf16[2,4,256,512]{3,2,1,0:T(8,128)(2,1)}, u32[]{:S(2)}) copy-start(bf16[2,4,256,512]{3,2,1,0:T(8,128)(2,1)} %shard_map.126.held_ref) | copy-start | bytes 6291460

commit v3 on v2

--- a/solution.py
+++ b/solution.py
@@ -712,11 +712,8 @@
     stats = [own_stats if k == 0 else swap(own_stats, "sp", k) for k in range(sp_count)]
     stats, *shares = combine_stats(stats, parts)
     order = list(range(sp_count // 2, sp_count)) + list(range(sp_count // 2 - 1, -1, -1))
-    first, second = order[: sp_count // 2], order[sp_count // 2 :]
-    found, kv_sums = backward_some(first, pairs, scores, stats, kv, None, 0)
-    query_parts = [swap(part, "sp", k) for k, part in zip(first, found)]
-    found, kv_sums = backward_some(second, pairs, scores, stats, kv, kv_sums, tp_count)
-    query_parts += [part if k == 0 else swap(part, "sp", k) for k, part in zip(second, found)]
+    found, kv_sums = backward_some(order, pairs, scores, stats, kv, None, tp_count)
+    query_parts = [part if k == 0 else swap(part, "sp", k) for k, part in zip(order, found)]
 
     others = swap(held, "tp", 1)
     back = lax.all_to_all(

time: 138 us -> 140 us (1.014)
  waiting for transfers between devices: 37.6 us -> 40.2 us
  local copies, waits for them, and re-layouts: 3.5 us -> 0.95 us
    ppermute x42, waiting for transfers between devices: 37.6 us -> 40.2 us  [swap(): return lax.ppermute(array, axis, [(i, i ^ mask) for i in range(size)])]
    unnamed x30 -> x18, local copies, waits for them, and re-layouts: 3.5 us -> 0.95 us
    pallas_call x19 -> x18, Pallas kernels: 34.6 us -> 35.6 us  [resident(): pl.pallas_call(kernel, out_shape=outs[0] if single else outs, in_specs=sp...]
where the time goes in v3:
time: 140 us; the launch traced here: 139 us
  starting transfers between devices  57.2 us (41%)
  waiting for transfers between devices  40.2 us (29%)
  Pallas kernels  39.7 us (28%)
    ppermute x42, starting transfers between devices, swap(): return lax.ppermute(array, axis, [(i, i ^ mask) for i in range(size)])  49.2 us
    ppermute x42, waiting for transfers between devices, swap(): return lax.ppermute(array, axis, [(i, i ^ mask) for i in range(size)])  40.2 us
    pallas_call x18, Pallas kernels, resident(): pl.pallas_call(kernel, out_shape=outs[0] if single else outs, in_specs=sp...  35.6 us
    all_to_all x1, starting transfers between devices, body(): kv = lax.all_to_all(packed, 'tp', split_axis=0, concat_axis=0, tiled=True)  4.22 us
    pallas_call x1, Pallas kernels, weight_grad(): pl.pallas_call(kernel, grid=(width // step,), in_specs=specs, out_specs=p...  4.06 us
    all_to_all x1, starting transfers between devices, body(): lax.all_to_all(kv_sums, 'tp', split_axis=0, concat_axis=0, tiled=True)  3.84 us
  transfers between devices with their start and end apart: 44, of which 15 were waited for; matrix products, arithmetic and copies ran while one was open for 0% of the time, Pallas kernels for 25%

profile of v3, /device:TPU:0, one launch (start us, length us, event | category | flops | bytes accessed | tf_op | source)
XLA Modules:
  0.0 138.9 jit_solution(5947128394488901219)
XLA Ops:
  0.7 3.1 %collective-permute-start.11 = (bf16[256,512]{1,0:T(8,128)(2,1)}, bf16[256,512]{1,0:T(8,128)(2,1)S(1)}, u32[]{:S(2)}, u32[]{:S(2)}) collective-permute-start(bf16[256,512]{1,0:T(8,128)(2,1)} %refs_0_.5), channel_id=1, source_target_pairs={{0,4},{1,5},{2,6},{3,7},{4,0},{5,1},{6,2},{7,3},{8,12},{9,13},{10,... | collective-permute-start | bytes 786440 | tf_op jit(solution)/shard_map/ppermute | solution.py:39
  3.7 1.5 %collective-permute-start.12 = (bf16[256,512]{1,0:T(8,128)(2,1)}, bf16[256,512]{1,0:T(8,128)(2,1)S(1)}, u32[]{:S(2)}, u32[]{:S(2)}) collective-permute-start(bf16[256,512]{1,0:T(8,128)(2,1)} %refs_4_.3), channel_id=1, source_target_pairs={{0,2},{1,3},{2,0},{3,1},{4,6},{5,7},{6,4},{7,5},{8,10},{9,11},{10,... | collective-permute-start | bytes 786440 | tf_op jit(solution)/shard_map/ppermute | solution.py:39
  5.2 1.8 %shard_map.113 = (bf16[128,1024]{1,0:T(8,128)(2,1)S(1)}, bf16[128,1024]{1,0:T(8,128)(2,1)S(1)}, bf16[2048,256]{1,0:T(8,128)(2,1)S(1)}, bf16[256,2048]{1,0:T(8,128)(2,1)S(1)}) custom-call(s32[1]{0:T(128)} %bitcast.1.at_ref, bf16[128,2048]{1,0:T(8,128)(2,1)} %rows_ref.1, f32[1,2048]{1,0:T(1,128)} %bitcast.4, bf16[2048,256]{1,0:T(8,128)(2,1)} %refs_0_.3, ...), custom_call_target="tpu_custom_call" | custom-call | flops 2097152 | bytes 1048576 | tf_op jit(solution)/shard_map/pallas_call | solution.py:130
  7.1 0.6 collective-permute-start.13
  7.7 3.0 %collective-permute-done.11.refs_1_.refs_2_ = bf16[256,512]{1,0:T(8,128)(2,1)S(1)} collective-permute-done((bf16[256,512]{1,0:T(8,128)(2,1)}, bf16[256,512]{1,0:T(8,128)(2,1)S(1)}, u32[]{:S(2)}, u32[]{:S(2)}) %collective-permute-start.11) | collective-permute-done | bytes 262176 | tf_op jit(solution)/shard_map/ppermute | solution.py:39
  10.7 1.4 %collective-permute-start.14 = (bf16[256,512]{1,0:T(8,128)(2,1)S(1)}, bf16[256,512]{1,0:T(8,128)(2,1)S(1)}, u32[]{:S(2)}, u32[]{:S(2)}) collective-permute-start(bf16[256,512]{1,0:T(8,128)(2,1)S(1)} %collective-permute-done.11.refs_1_.refs_2_), channel_id=1, source_target_pairs={{0,2},{1,3},{2,0},{3,1},{4,6},{5,7},{6,4},{7,5},{8,10},{9,11},{10,... | collective-permute-start | bytes 786440 | tf_op jit(solution)/shard_map/ppermute | solution.py:39
  12.1 0.9 collective-permute-done.12.refs_3_.refs_5_
  13.1 1.4 %collective-permute-start.16 = (bf16[256,512]{1,0:T(8,128)(2,1)S(1)}, bf16[256,512]{1,0:T(8,128)(2,1)S(1)}, u32[]{:S(2)}, u32[]{:S(2)}) collective-permute-start(bf16[256,512]{1,0:T(8,128)(2,1)S(1)} %collective-permute-done.12.refs_3_.refs_5_), channel_id=1, source_target_pairs={{0,4},{1,5},{2,6},{3,7},{4,0},{5,1},{6,2},{7,3},{8,12},{9,13},{10,... | collective-permute-start | bytes 786440 | tf_op jit(solution)/shard_map/ppermute | solution.py:39
  14.5 1.6 %collective-permute-start.35 = (bf16[24,2048]{1,0:T(8,128)(2,1)}, bf16[24,2048]{1,0:T(8,128)(2,1)S(1)}, u32[]{:S(2)}, u32[]{:S(2)}) collective-permute-start(bf16[24,2048]{1,0:T(8,128)(2,1)} %refs_5_.1), channel_id=1, source_target_pairs={{0,8},{8,0},{16,24},{24,16},{1,9},{9,1},{17,25},{25,17},{2,10},{10... | collective-permute-start | bytes 294920 | tf_op jit(solution)/shard_map/ppermute | solution.py:39
  16.1 2.6 %collective-permute-done.13.refs_2_.refs_1_ = bf16[256,512]{1,0:T(8,128)(2,1)S(1)} collective-permute-done((bf16[256,512]{1,0:T(8,128)(2,1)S(1)}, bf16[256,512]{1,0:T(8,128)(2,1)S(1)}, u32[]{:S(2)}, u32[]{:S(2)}) %collective-permute-start.13) | collective-permute-done | bytes 262176 | tf_op jit(solution)/shard_map/ppermute | solution.py:39
  18.7 2.6 %collective-permute-start.36 = (bf16[24,2048]{1,0:T(8,128)(2,1)}, bf16[24,2048]{1,0:T(8,128)(2,1)S(1)}, u32[]{:S(2)}, u32[]{:S(2)}) collective-permute-start(bf16[24,2048]{1,0:T(8,128)(2,1)} %refs_5_.1), channel_id=1, source_target_pairs={{0,16},{8,24},{16,0},{24,8},{1,17},{9,25},{17,1},{25,9},{2,18},{10... | collective-permute-start | bytes 294920 | tf_op jit(solution)/shard_map/ppermute | solution.py:39
  21.3 1.3 collective-permute-start.37
  22.7 1.0 shard_map.112.refs_0_
  23.7 1.6 %collective-permute-start = (bf16[2,24,2048]{2,1,0:T(8,128)(2,1)S(1)}, bf16[2,24,2048]{2,1,0:T(8,128)(2,1)S(1)}, u32[]{:S(2)}, u32[]{:S(2)}) collective-permute-start(bf16[2,24,2048]{2,1,0:T(8,128)(2,1)S(1)} %shard_map.112.refs_0_), channel_id=1, source_target_pairs={{0,2},{1,3},{2,0},{3,1},{4,6},{5,7},{6,4},{7,5},{8,10},{9,11},{10,... | collective-permute-start | bytes 589832 | tf_op jit(solution)/shard_map/ppermute | solution.py:39
  26.2 1.5 %shard_map.125.held_ref = bf16[2,4,256,512]{3,2,1,0:T(8,128)(2,1)} custom-call(bf16[256,512]{1,0:T(8,128)(2,1)S(1)} %copy-done.1, bf16[256,512]{1,0:T(8,128)(2,1)S(1)} %collective-permute-done.13.refs_2_.refs_1_, bf16[256,512]{1,0:T(8,128)(2,1)S(1)} %collective-permute-done.11.refs_1_.refs_2_, bf16[256,512]{1,0:T(8,128)(2,1)S(1)} %collective-permute-done.14.refs_3_, ...), custom_call_target="tpu_custom_call" | custom-call | flops 1048576 | bytes 1048576 | tf_op jit(solution)/shard_map/pallas_call | solution.py:130
  27.7 1.5 %collective-permute-start.2 = (bf16[2,24,2048]{2,1,0:T(8,128)(2,1)S(1)}, bf16[2,24,2048]{2,1,0:T(8,128)(2,1)S(1)}, u32[]{:S(2)}, u32[]{:S(2)}) collective-permute-start(bf16[2,24,2048]{2,1,0:T(8,128)(2,1)S(1)} %shard_map.112.refs_0_), channel_id=1, source_target_pairs={{0,6},{1,7},{2,4},{3,5},{4,2},{5,3},{6,0},{7,1},{8,14},{9,15},{10,... | collective-permute-start | bytes 589832 | tf_op jit(solution)/shard_map/ppermute | solution.py:39
  29.2 0.6 shard_map.117
  29.8 0.6 collective-permute-start.17
  30.5 4.5 %collective-permute-done.1.refs_2_ = bf16[2,24,2048]{2,1,0:T(8,128)(2,1)S(1)} collective-permute-done((bf16[2,24,2048]{2,1,0:T(8,128)(2,1)S(1)}, bf16[2,24,2048]{2,1,0:T(8,128)(2,1)S(1)}, u32[]{:S(2)}, u32[]{:S(2)}) %collective-permute-start.1) | collective-permute-done | bytes 196640 | tf_op jit(solution)/shard_map/ppermute | solution.py:39
  35.5 0.7 shard_map.128.refs_3_
  36.3 0.6 collective-permute-start.38
  36.9 0.5 collective-permute-start.39
  37.4 2.4 %collective-permute-start.40 = (bf16[3,24,2048]{2,1,0:T(8,128)(2,1)}, bf16[3,24,2048]{2,1,0:T(8,128)(2,1)}, u32[]{:S(2)}, u32[]{:S(2)}) collective-permute-start(bf16[3,24,2048]{2,1,0:T(8,128)(2,1)} %shard_map.128.refs_3_), channel_id=1, source_target_pairs={{0,6},{1,7},{2,4},{3,5},{4,2},{5,3},{6,0},{7,1},{8,14},{9,15},{10,... | collective-permute-start | bytes 884744 | tf_op jit(solution)/shard_map/ppermute | solution.py:39
  39.8 0.7 shard_map.118
  40.6 4.2 %all-to-all-start = ((bf16[8,128,128]{2,1,0:T(8,128)(2,1)}), bf16[8,128,128]{2,1,0:T(8,128)(2,1)}, u32[]{:S(2)}, u32[]{:S(2)}) async-start(bf16[8,128,128]{2,1,0:T(8,128)(2,1)} %shard_map.118), calls=%async_computation | async-start | bytes 524288 | tf_op jit(solution)/shard_map/all_to_all | solution.py:702
  44.8 0.9 copy-done.4
  45.7 1.4 %shard_map.114.refs_8_.refs_3_ = bf16[128,768]{1,0:T(8,128)(2,1)} custom-call(bf16[2,24,2048]{2,1,0:T(8,128)(2,1)S(1)} %shard_map.112.refs_0_, bf16[2,24,2048]{2,1,0:T(8,128)(2,1)S(1)} %collective-permute-done.refs_1_, bf16[2,24,2048]{2,1,0:T(8,128)(2,1)S(1)} %copy-done.4, bf16[2,24,2048]{2,1,0:T(8,128)(2,1)S(1)} %collective-permute-done.2.refs_3_, ...), custom_call_target="tpu_custom_call" | custom-call | flops 402653184 | bytes 1048576 | tf_op jit(solution)/shard_map/pallas_call | solution.py:130
  47.2 1.9 %collective-permute-start.7 = (bf16[128,768]{1,0:T(8,128)(2,1)}, bf16[128,768]{1,0:T(8,128)(2,1)S(1)}, u32[]{:S(2)}, u32[]{:S(2)}) collective-permute-start(bf16[128,768]{1,0:T(8,128)(2,1)} %shard_map.114.refs_8_.refs_3_), channel_id=1, source_target_pairs={{0,16},{8,24},{16,0},{24,8},{1,17},{9,25},{17,1},{25,9},{2,18},{10... | collective-permute-start | bytes 589832 | tf_op jit(solution)/shard_map/ppermute | solution.py:39
  49.1 1.3 collective-permute-start.8
  50.4 1.5 %collective-permute-done.39.refs_1_ = bf16[3,24,2048]{2,1,0:T(8,128)(2,1)} collective-permute-done((bf16[3,24,2048]{2,1,0:T(8,128)(2,1)}, bf16[3,24,2048]{2,1,0:T(8,128)(2,1)}, u32[]{:S(2)}, u32[]{:S(2)}) %collective-permute-start.39) | collective-permute-done | bytes 294944 | tf_op jit(solution)/shard_map/ppermute | solution.py:39
  51.9 1.1 collective-permute-start.9
  53.0 2.4 %shard_map.129.refs_5_ = bf16[288,2048]{1,0:T(8,128)(2,1)} custom-call(bf16[3,24,2048]{2,1,0:T(8,128)(2,1)} %collective-permute-done.38.refs_0_, bf16[3,24,2048]{2,1,0:T(8,128)(2,1)} %collective-permute-done.39.refs_1_, bf16[3,24,2048]{2,1,0:T(8,128)(2,1)} %collective-permute-done.40.refs_2_, bf16[3,24,2048]{2,1,0:T(8,128)(2,1)} %shard_map.128.refs_3_), custom_call_target="tpu_custom_call" | custom-call | flops 1048576 | bytes 1048576 | tf_op jit(solution)/shard_map/pallas_call | solution.py:130
  55.4 1.9 %shard_map.115 = (bf16[128,768]{1,0:T(8,128)(2,1)S(1)}, bf16[192,2048]{1,0:T(8,128)(2,1)}) custom-call(bf16[2,24,2048]{2,1,0:T(8,128)(2,1)S(1)} %shard_map.112.refs_0_, bf16[2,24,2048]{2,1,0:T(8,128)(2,1)S(1)} %collective-permute-done.refs_1_, bf16[2,24,2048]{2,1,0:T(8,128)(2,1)S(1)} %copy-done.4, bf16[2,24,2048]{2,1,0:T(8,128)(2,1)S(1)} %collective-permute-done.2.refs_3_, ...), custom_call_target="tpu_custom_call" | custom-call | flops 1048576 | bytes 1048576 | tf_op jit(solution)/shard_map/pallas_call | solution.py:130
  57.3 6.9 %collective-permute-done.7.refs_2_.refs_0_ = bf16[128,768]{1,0:T(8,128)(2,1)S(1)} collective-permute-done((bf16[128,768]{1,0:T(8,128)(2,1)}, bf16[128,768]{1,0:T(8,128)(2,1)S(1)}, u32[]{:S(2)}, u32[]{:S(2)}) %collective-permute-start.7) | collective-permute-done | bytes 196640 | tf_op jit(solution)/shard_map/ppermute | solution.py:39
  64.1 1.2 collective-permute-done.9.refs_1_.refs_2_
  65.4 5.0 %shard_map.119 = (f32[4,64,768]{2,1,0:T(8,128)S(1)}, f32[8,768]{1,0:T(8,128)S(1)}, f32[1024,768]{1,0:T(8,128)S(1)}, f32[1024,768]{1,0:T(8,128)S(1)}, f32[1024,768]{1,0:T(8,128)S(1)}, /*index=5*/f32[1024,768]{1,0:T(8,128)S(1)}) custom-call(bf16[128,768]{1,0:T(8,128)(2,1)S(1)} %get-tuple-element.37.refs_0_, ...), custom_call_target="tpu_custom_call" | custom-call | flops 1610612736 | bytes 1048576 | tf_op jit(solution)/shard_map/pallas_call | solution.py:130
  70.4 3.2 %collective-permute-start.18 = (f32[8,768]{1,0:T(8,128)S(1)}, f32[8,768]{1,0:T(8,128)S(1)}, u32[]{:S(2)}, u32[]{:S(2)}) collective-permute-start(f32[8,768]{1,0:T(8,128)S(1)} %get-tuple-element.48.refs_0_), channel_id=1, source_target_pairs={{0,8},{8,0},{16,24},{24,16},{1,9},{9,1},{17,25},{25,17},{2,10},{10... | collective-permute-start | bytes 73736 | tf_op jit(solution)/shard_map/ppermute | solution.py:39
  73.6 1.4 %collective-permute-start.19 = (f32[8,768]{1,0:T(8,128)S(1)}, f32[8,768]{1,0:T(8,128)S(1)}, u32[]{:S(2)}, u32[]{:S(2)}) collective-permute-start(f32[8,768]{1,0:T(8,128)S(1)} %get-tuple-element.48.refs_0_), channel_id=1, source_target_pairs={{0,16},{8,24},{16,0},{24,8},{1,17},{9,25},{17,1},{25,9},{2,18},{10... | collective-permute-start | bytes 73736 | tf_op jit(solution)/shard_map/ppermute | solution.py:39
  75.0 1.4 collective-permute-start.20
  76.4 2.2 %collective-permute-done.19.refs_2_ = f32[8,768]{1,0:T(8,128)S(1)} collective-permute-done((f32[8,768]{1,0:T(8,128)S(1)}, f32[8,768]{1,0:T(8,128)S(1)}, u32[]{:S(2)}, u32[]{:S(2)}) %collective-permute-start.19) | collective-permute-done | bytes 24608 | tf_op jit(solution)/shard_map/ppermute | solution.py:39
  78.6 2.0 %collective-permute-done.20.refs_3_ = f32[8,768]{1,0:T(8,128)S(1)} collective-permute-done((f32[8,768]{1,0:T(8,128)S(1)}, f32[8,768]{1,0:T(8,128)S(1)}, u32[]{:S(2)}, u32[]{:S(2)}) %collective-permute-start.20) | collective-permute-done | bytes 24608 | tf_op jit(solution)/shard_map/ppermute | solution.py:39
  80.6 0.8 shard_map.120
  81.4 7.8 %shard_map.121 = (bf16[8,128,128]{2,1,0:T(8,128)(2,1)}, bf16[64,768]{1,0:T(8,128)(2,1)}, bf16[64,768]{1,0:T(8,128)(2,1)}, bf16[64,768]{1,0:T(8,128)(2,1)}, bf16[64,768]{1,0:T(8,128)(2,1)}) custom-call(bf16[128,768]{1,0:T(8,128)(2,1)S(1)} %collective-permute-done.7.refs_2_.refs_0_, bf16[128,768]{1,0:T(8,128)(2,1)S(1)} %collective-permute-done.8.refs_3_.refs_1_, ...), custom_call_target="tpu_custom_call" | custom-call | flops 4026531840 | bytes 1048576 | tf_op jit(solution)/shard_map/pallas_call | solution.py:130
  89.3 2.5 %collective-permute-start.22 = (bf16[64,768]{1,0:T(8,128)(2,1)}, bf16[64,768]{1,0:T(8,128)(2,1)S(1)}, u32[]{:S(2)}, u32[]{:S(2)}) collective-permute-start(bf16[64,768]{1,0:T(8,128)(2,1)} %get-tuple-element.52), channel_id=1, source_target_pairs={{0,24},{8,16},{16,8},{24,0},{1,25},{9,17},{17,9},{25,1},{2,26},{10... | collective-permute-start | bytes 294920 | tf_op jit(solution)/shard_map/ppermute | solution.py:39
  91.8 1.0 collective-permute-start.23
  92.8 5.2 %collective-permute-done.21.refs_0_ = bf16[64,768]{1,0:T(8,128)(2,1)S(1)} collective-permute-done((bf16[64,768]{1,0:T(8,128)(2,1)}, bf16[64,768]{1,0:T(8,128)(2,1)S(1)}, u32[]{:S(2)}, u32[]{:S(2)}) %collective-permute-start.21) | collective-permute-done | bytes 98336 | tf_op jit(solution)/shard_map/ppermute | solution.py:39
  98.4 1.5 %shard_map.122 = (f32[96,2048]{1,0:T(8,128)S(1)}, bf16[96,2048]{1,0:T(8,128)(2,1)S(1)}) custom-call(bf16[64,768]{1,0:T(8,128)(2,1)S(1)} %collective-permute-done.21.refs_0_, bf16[64,768]{1,0:T(8,128)(2,1)S(1)} %collective-permute-done.22.refs_1_, bf16[64,768]{1,0:T(8,128)(2,1)S(1)} %collective-permute-done.23.refs_2_, ...), custom_call_target="tpu_custom_call" | custom-call | flops 201326592 | bytes 1048576 | tf_op jit(solution)/shard_map/pallas_call | solution.py:130
  100.0 1.7 %collective-permute-start.29 = (bf16[64,768]{1,0:T(8,128)(2,1)S(1)}, bf16[64,768]{1,0:T(8,128)(2,1)S(1)}, u32[]{:S(2)}, u32[]{:S(2)}) collective-permute-start(bf16[64,768]{1,0:T(8,128)(2,1)S(1)} %copy-done.8), channel_id=1, source_target_pairs={{0,8},{8,0},{16,24},{24,16},{1,9},{9,1},{17,25},{25,17},{2,10},{10... | collective-permute-start | bytes 294920 | tf_op jit(solution)/shard_map/ppermute | solution.py:39
  101.6 0.7 collective-permute-start.30
  102.3 2.8 %collective-permute-done.29.refs_0_ = bf16[64,768]{1,0:T(8,128)(2,1)S(1)} collective-permute-done((bf16[64,768]{1,0:T(8,128)(2,1)S(1)}, bf16[64,768]{1,0:T(8,128)(2,1)S(1)}, u32[]{:S(2)}, u32[]{:S(2)}) %collective-permute-start.29) | collective-permute-done | bytes 98336 | tf_op jit(solution)/shard_map/ppermute | solution.py:39
  105.2 1.7 %collective-permute-start.31 = (bf16[64,768]{1,0:T(8,128)(2,1)S(1)}, bf16[64,768]{1,0:T(8,128)(2,1)S(1)}, u32[]{:S(2)}, u32[]{:S(2)}) collective-permute-start(bf16[64,768]{1,0:T(8,128)(2,1)S(1)} %copy-done.6), channel_id=1, source_target_pairs={{0,24},{8,16},{16,8},{24,0},{1,25},{9,17},{17,9},{25,1},{2,26},{10... | collective-permute-start | bytes 294920 | tf_op jit(solution)/shard_map/ppermute | solution.py:39
  106.9 3.8 %all-to-all-start.1 = ((bf16[8,128,128]{2,1,0:T(8,128)(2,1)}), bf16[8,128,128]{2,1,0:T(8,128)(2,1)S(1)}, u32[]{:S(2)}, u32[]{:S(2)}) async-start(bf16[8,128,128]{2,1,0:T(8,128)(2,1)} %get-tuple-element.61), calls=%async_computation.1 | async-start | bytes 524288 | tf_op jit(solution)/shard_map/all_to_all | solution.py:719
  110.7 1.6 %collective-permute-done.30.refs_1_ = bf16[64,768]{1,0:T(8,128)(2,1)S(1)} collective-permute-done((bf16[64,768]{1,0:T(8,128)(2,1)S(1)}, bf16[64,768]{1,0:T(8,128)(2,1)S(1)}, u32[]{:S(2)}, u32[]{:S(2)}) %collective-permute-start.30) | collective-permute-done | bytes 98336 | tf_op jit(solution)/shard_map/ppermute | solution.py:39
  112.3 0.9 shard_map.127.refs_0_
  113.3 2.0 %collective-permute-start.32 = (bf16[64,768]{1,0:T(8,128)(2,1)S(1)}, bf16[64,768]{1,0:T(8,128)(2,1)S(1)}, u32[]{:S(2)}, u32[]{:S(2)}) collective-permute-start(bf16[64,768]{1,0:T(8,128)(2,1)S(1)} %shard_map.127.refs_0_), channel_id=1, source_target_pairs={{0,8},{8,0},{16,24},{24,16},{1,9},{9,1},{17,25},{25,17},{2,10},{10... | collective-permute-start | bytes 294920 | tf_op jit(solution)/shard_map/ppermute | solution.py:39
  115.6 2.1 %collective-permute-start.34 = (bf16[64,768]{1,0:T(8,128)(2,1)S(1)}, bf16[64,768]{1,0:T(8,128)(2,1)S(1)}, u32[]{:S(2)}, u32[]{:S(2)}) collective-permute-start(bf16[64,768]{1,0:T(8,128)(2,1)S(1)} %shard_map.127.refs_0_), channel_id=1, source_target_pairs={{0,24},{8,16},{16,8},{24,0},{1,25},{9,17},{17,9},{25,1},{2,26},{10... | collective-permute-start | bytes 294920 | tf_op jit(solution)/shard_map/ppermute | solution.py:39
  117.7 0.8 shard_map.123
  118.6 1.6 %collective-permute-start.25 = (bf16[24,2048]{1,0:T(8,128)(2,1)}, bf16[24,2048]{1,0:T(8,128)(2,1)S(1)}, u32[]{:S(2)}, u32[]{:S(2)}) collective-permute-start(bf16[24,2048]{1,0:T(8,128)(2,1)} %get-tuple-element.57), channel_id=1, source_target_pairs={{0,2},{1,3},{2,0},{3,1},{4,6},{5,7},{6,4},{7,5},{8,10},{9,11},{10,... | collective-permute-start | bytes 294920 | tf_op jit(solution)/shard_map/ppermute | solution.py:39
  120.2 5.0 %collective-permute-done.33.refs_2_ = bf16[64,768]{1,0:T(8,128)(2,1)S(1)} collective-permute-done((bf16[64,768]{1,0:T(8,128)(2,1)S(1)}, bf16[64,768]{1,0:T(8,128)(2,1)S(1)}, u32[]{:S(2)}, u32[]{:S(2)}) %collective-permute-start.33) | collective-permute-done | bytes 98336 | tf_op jit(solution)/shard_map/ppermute | solution.py:39
  125.2 1.7 %collective-permute-start.26 = (bf16[24,2048]{1,0:T(8,128)(2,1)}, bf16[24,2048]{1,0:T(8,128)(2,1)S(1)}, u32[]{:S(2)}, u32[]{:S(2)}) collective-permute-start(bf16[24,2048]{1,0:T(8,128)(2,1)} %get-tuple-element.58), channel_id=1, source_target_pairs={{0,4},{1,5},{2,6},{3,7},{4,0},{5,1},{6,2},{7,3},{8,12},{9,13},{10,... | collective-permute-start | bytes 294920 | tf_op jit(solution)/shard_map/ppermute | solution.py:39
  126.9 1.4 %collective-permute-start.27 = (bf16[24,2048]{1,0:T(8,128)(2,1)}, bf16[24,2048]{1,0:T(8,128)(2,1)S(1)}, u32[]{:S(2)}, u32[]{:S(2)}) collective-permute-start(bf16[24,2048]{1,0:T(8,128)(2,1)} %get-tuple-element.59), channel_id=1, source_target_pairs={{0,6},{1,7},{2,4},{3,5},{4,2},{5,3},{6,0},{7,1},{8,14},{9,15},{10,... | collective-permute-start | bytes 294920 | tf_op jit(solution)/shard_map/ppermute | solution.py:39
  128.3 4.1 %weight_grad.1 = f32[256,2048]{1,0:T(8,128)} custom-call(bf16[64,768]{1,0:T(8,128)(2,1)S(1)} %shard_map.127.refs_0_, bf16[64,768]{1,0:T(8,128)(2,1)S(1)} %collective-permute-done.32.refs_1_, bf16[64,768]{1,0:T(8,128)(2,1)S(1)} %collective-permute-done.33.refs_2_, bf16[64,768]{1,0:T(8,128)(2,1)S(1)} %collective-permute-done.34.refs_3_, ...), custom_call_target="tpu_custom_call" | custom-call | flops 805306368 | bytes 3145728 | tf_op jit(solution)/shard_map/weight_grad/pallas_call | solution.py:570
  132.6 1.9 %shard_map.124 = f32[24,2048]{1,0:T(8,128)} custom-call(bf16[24,2048]{1,0:T(8,128)(2,1)S(1)} %collective-permute-done.25.refs_0_, bf16[24,2048]{1,0:T(8,128)(2,1)S(1)} %collective-permute-done.26.refs_1_, bf16[24,2048]{1,0:T(8,128)(2,1)S(1)} %collective-permute-done.27.refs_2_, f32[24,2048]{1,0:T(8,128)} %get-tuple-element.60.refs_3_, ...), custom_call_target="tpu_custom_call" | custom-call | flops 1048576 | bytes 1048576 | tf_op jit(solution)/shard_map/pallas_call | solution.py:130
  134.5 4.5 %shard_map.126 = f32[128,2048]{1,0:T(8,128)} custom-call(s32[1]{0:T(128)} %bitcast.1.at_ref, bf16[8,128,128]{2,1,0:T(8,128)(2,1)S(1)} %all-to-all-done.1.back_ref, bf16[2,4,256,512]{3,2,1,0:T(8,128)(2,1)S(1)} %copy-done, bf16[2,4,256,512]{3,2,1,0:T(8,128)(2,1)} %collective-permute-done.28.other_ref, bf16[128,2048]{1,0:T(8,128)(2,1)} %rows_ref.1, ...), custom_call_target="tpu_custom_call" | custom-call | flops 536870912 | bytes 1048576 | tf_op jit(solution)/shard_map/pallas_call | solution.py:130
  (61 shorter events, 2.9 us)
Async XLA Ops:
  0.6 6.4 %copy-start.1 = (bf16[256,512]{1,0:T(8,128)(2,1)S(1)}, bf16[256,512]{1,0:T(8,128)(2,1)}, u32[]{:S(2)}) copy-start(bf16[256,512]{1,0:T(8,128)(2,1)} %refs_0_.5) | copy-start | bytes 786436
  0.6 7.0 %copy-start.2 = (bf16[256,512]{1,0:T(8,128)(2,1)S(1)}, bf16[256,512]{1,0:T(8,128)(2,1)}, u32[]{:S(2)}) copy-start(bf16[256,512]{1,0:T(8,128)(2,1)} %refs_4_.3) | copy-start | bytes 786436
  0.7 10.1 %collective-permute-start.11 = (bf16[256,512]{1,0:T(8,128)(2,1)}, bf16[256,512]{1,0:T(8,128)(2,1)S(1)}, u32[]{:S(2)}, u32[]{:S(2)}) collective-permute-start(bf16[256,512]{1,0:T(8,128)(2,1)} %refs_0_.5), channel_id=1, source_target_pairs={{0,4},{1,5},{2,6},{3,7},{4,0},{5,1},{6,2},{7,3},{8,12},{9,13},{10,... | collective-permute-start | bytes 786440 | tf_op jit(solution)/shard_map/ppermute | solution.py:39
  3.7 9.4 %collective-permute-start.12 = (bf16[256,512]{1,0:T(8,128)(2,1)}, bf16[256,512]{1,0:T(8,128)(2,1)S(1)}, u32[]{:S(2)}, u32[]{:S(2)}) collective-permute-start(bf16[256,512]{1,0:T(8,128)(2,1)} %refs_4_.3), channel_id=1, source_target_pairs={{0,2},{1,3},{2,0},{3,1},{4,6},{5,7},{6,4},{7,5},{8,10},{9,11},{10,... | collective-permute-start | bytes 786440 | tf_op jit(solution)/shard_map/ppermute | solution.py:39
  7.0 7.6 %collective-permute-start.10 = (bf16[128,1024]{1,0:T(8,128)(2,1)S(1)}, bf16[128,1024]{1,0:T(8,128)(2,1)S(1)}, u32[]{:S(2)}, u32[]{:S(2)}) collective-permute-start(bf16[128,1024]{1,0:T(8,128)(2,1)S(1)} %get-tuple-element.39), channel_id=1, source_target_pairs={{0,1},{1,0},{2,3},{3,2},{4,5},{5,4},{6,7},{7,6},{8,9},{9,8},{10,11... | collective-permute-start | bytes 786440 | tf_op jit(solution)/shard_map/ppermute | solution.py:39
  7.1 11.7 %collective-permute-start.13 = (bf16[256,512]{1,0:T(8,128)(2,1)S(1)}, bf16[256,512]{1,0:T(8,128)(2,1)S(1)}, u32[]{:S(2)}, u32[]{:S(2)}) collective-permute-start(bf16[256,512]{1,0:T(8,128)(2,1)S(1)} %copy-done.1), channel_id=1, source_target_pairs={{0,2},{1,3},{2,0},{3,1},{4,6},{5,7},{6,4},{7,5},{8,10},{9,11},{10,... | collective-permute-start | bytes 786440 | tf_op jit(solution)/shard_map/ppermute | solution.py:39
  7.7 13.7 %collective-permute-start.15 = (bf16[256,512]{1,0:T(8,128)(2,1)S(1)}, bf16[256,512]{1,0:T(8,128)(2,1)S(1)}, u32[]{:S(2)}, u32[]{:S(2)}) collective-permute-start(bf16[256,512]{1,0:T(8,128)(2,1)S(1)} %copy-done.2), channel_id=1, source_target_pairs={{0,4},{1,5},{2,6},{3,7},{4,0},{5,1},{6,2},{7,3},{8,12},{9,13},{10,... | collective-permute-start | bytes 786440 | tf_op jit(solution)/shard_map/ppermute | solution.py:39
  10.7 13.0 %collective-permute-start.14 = (bf16[256,512]{1,0:T(8,128)(2,1)S(1)}, bf16[256,512]{1,0:T(8,128)(2,1)S(1)}, u32[]{:S(2)}, u32[]{:S(2)}) collective-permute-start(bf16[256,512]{1,0:T(8,128)(2,1)S(1)} %collective-permute-done.11.refs_1_.refs_2_), channel_id=1, source_target_pairs={{0,2},{1,3},{2,0},{3,1},{4,6},{5,7},{6,4},{7,5},{8,10},{9,11},{10,... | collective-permute-start | bytes 786440 | tf_op jit(solution)/shard_map/ppermute | solution.py:39
  13.1 12.2 %collective-permute-start.16 = (bf16[256,512]{1,0:T(8,128)(2,1)S(1)}, bf16[256,512]{1,0:T(8,128)(2,1)S(1)}, u32[]{:S(2)}, u32[]{:S(2)}) collective-permute-start(bf16[256,512]{1,0:T(8,128)(2,1)S(1)} %collective-permute-done.12.refs_3_.refs_5_), channel_id=1, source_target_pairs={{0,4},{1,5},{2,6},{3,7},{4,0},{5,1},{6,2},{7,3},{8,12},{9,13},{10,... | collective-permute-start | bytes 786440 | tf_op jit(solution)/shard_map/ppermute | solution.py:39
  14.5 13.2 %collective-permute-start.35 = (bf16[24,2048]{1,0:T(8,128)(2,1)}, bf16[24,2048]{1,0:T(8,128)(2,1)S(1)}, u32[]{:S(2)}, u32[]{:S(2)}) collective-permute-start(bf16[24,2048]{1,0:T(8,128)(2,1)} %refs_5_.1), channel_id=1, source_target_pairs={{0,8},{8,0},{16,24},{24,16},{1,9},{9,1},{17,25},{25,17},{2,10},{10... | collective-permute-start | bytes 294920 | tf_op jit(solution)/shard_map/ppermute | solution.py:39
  18.7 10.5 %collective-permute-start.36 = (bf16[24,2048]{1,0:T(8,128)(2,1)}, bf16[24,2048]{1,0:T(8,128)(2,1)S(1)}, u32[]{:S(2)}, u32[]{:S(2)}) collective-permute-start(bf16[24,2048]{1,0:T(8,128)(2,1)} %refs_5_.1), channel_id=1, source_target_pairs={{0,16},{8,24},{16,0},{24,8},{1,17},{9,25},{17,1},{25,9},{2,18},{10... | collective-permute-start | bytes 294920 | tf_op jit(solution)/shard_map/ppermute | solution.py:39
  21.3 8.5 %collective-permute-start.37 = (bf16[24,2048]{1,0:T(8,128)(2,1)}, bf16[24,2048]{1,0:T(8,128)(2,1)S(1)}, u32[]{:S(2)}, u32[]{:S(2)}) collective-permute-start(bf16[24,2048]{1,0:T(8,128)(2,1)} %refs_5_.1), channel_id=1, source_target_pairs={{0,24},{8,16},{16,8},{24,0},{1,25},{9,17},{17,9},{25,1},{2,26},{10... | collective-permute-start | bytes 294920 | tf_op jit(solution)/shard_map/ppermute | solution.py:39
  23.7 6.7 %collective-permute-start = (bf16[2,24,2048]{2,1,0:T(8,128)(2,1)S(1)}, bf16[2,24,2048]{2,1,0:T(8,128)(2,1)S(1)}, u32[]{:S(2)}, u32[]{:S(2)}) collective-permute-start(bf16[2,24,2048]{2,1,0:T(8,128)(2,1)S(1)} %shard_map.112.refs_0_), channel_id=1, source_target_pairs={{0,2},{1,3},{2,0},{3,1},{4,6},{5,7},{6,4},{7,5},{8,10},{9,11},{10,... | collective-permute-start | bytes 589832 | tf_op jit(solution)/shard_map/ppermute | solution.py:39
  25.3 9.7 %collective-permute-start.1 = (bf16[2,24,2048]{2,1,0:T(8,128)(2,1)S(1)}, bf16[2,24,2048]{2,1,0:T(8,128)(2,1)S(1)}, u32[]{:S(2)}, u32[]{:S(2)}) collective-permute-start(bf16[2,24,2048]{2,1,0:T(8,128)(2,1)S(1)} %shard_map.112.refs_0_), channel_id=1, source_target_pairs={{0,4},{1,5},{2,6},{3,7},{4,0},{5,1},{6,2},{7,3},{8,12},{9,13},{10,... | collective-permute-start | bytes 589832 | tf_op jit(solution)/shard_map/ppermute | solution.py:39
  27.7 7.3 %collective-permute-start.2 = (bf16[2,24,2048]{2,1,0:T(8,128)(2,1)S(1)}, bf16[2,24,2048]{2,1,0:T(8,128)(2,1)S(1)}, u32[]{:S(2)}, u32[]{:S(2)}) collective-permute-start(bf16[2,24,2048]{2,1,0:T(8,128)(2,1)S(1)} %shard_map.112.refs_0_), channel_id=1, source_target_pairs={{0,6},{1,7},{2,4},{3,5},{4,2},{5,3},{6,0},{7,1},{8,14},{9,15},{10,... | collective-permute-start | bytes 589832 | tf_op jit(solution)/shard_map/ppermute | solution.py:39
  29.2 105.2 %collective-permute-start.28 = (bf16[2,4,256,512]{3,2,1,0:T(8,128)(2,1)}, bf16[2,4,256,512]{3,2,1,0:T(8,128)(2,1)}, u32[]{:S(2)}, u32[]{:S(2)}) collective-permute-start(bf16[2,4,256,512]{3,2,1,0:T(8,128)(2,1)} %shard_map.125.held_ref), channel_id=1, source_target_pairs={{0,1},{1,0},{2,3},{3,2},{4,5},{5,4},{6,7},{7,6},{8,9},{9,8},{10,11... | collective-permute-start | bytes 6291464 | tf_op jit(solution)/shard_map/ppermute | solution.py:39
  29.8 7.6 %collective-permute-start.17 = (f32[8,128,128]{2,1,0:T(8,128)S(1)}, f32[8,128,128]{2,1,0:T(8,128)S(1)}, u32[]{:S(2)}, u32[]{:S(2)}) collective-permute-start(f32[8,128,128]{2,1,0:T(8,128)S(1)} %get-tuple-element.43), channel_id=1, source_target_pairs={{0,1},{1,0},{2,3},{3,2},{4,5},{5,4},{6,7},{7,6},{8,9},{9,8},{10,11... | collective-permute-start | bytes 1572872 | tf_op jit(solution)/shard_map/ppermute | solution.py:39
  30.4 5.8 %collective-permute-start.3 = (bf16[2,24,2048]{2,1,0:T(8,128)(2,1)S(1)}, bf16[2,24,2048]{2,1,0:T(8,128)(2,1)S(1)}, u32[]{:S(2)}, u32[]{:S(2)}) collective-permute-start(bf16[2,24,2048]{2,1,0:T(8,128)(2,1)S(1)} %shard_map.112.refs_0_), channel_id=1, source_target_pairs={{0,1},{1,0},{2,3},{3,2},{4,5},{5,4},{6,7},{7,6},{8,9},{9,8},{10,11... | collective-permute-start | bytes 589832 | tf_op jit(solution)/shard_map/ppermute | solution.py:39
  35.0 1.9 %copy-start.3 = (bf16[2,24,2048]{2,1,0:T(8,128)(2,1)}, bf16[2,24,2048]{2,1,0:T(8,128)(2,1)S(1)}, u32[]{:S(2)}) copy-start(bf16[2,24,2048]{2,1,0:T(8,128)(2,1)S(1)} %collective-permute-done.1.refs_2_) | copy-start | bytes 589828
  35.0 1.9 %collective-permute-start.4 = (bf16[2,24,2048]{2,1,0:T(8,128)(2,1)S(1)}, bf16[2,24,2048]{2,1,0:T(8,128)(2,1)S(1)}, u32[]{:S(2)}, u32[]{:S(2)}) collective-permute-start(bf16[2,24,2048]{2,1,0:T(8,128)(2,1)S(1)} %collective-permute-done.refs_1_), channel_id=1, source_target_pairs={{0,1},{1,0},{2,3},{3,2},{4,5},{5,4},{6,7},{7,6},{8,9},{9,8},{10,11... | collective-permute-start | bytes 589832 | tf_op jit(solution)/shard_map/ppermute | solution.py:39
  35.0 2.4 %collective-permute-start.5 = (bf16[2,24,2048]{2,1,0:T(8,128)(2,1)S(1)}, bf16[2,24,2048]{2,1,0:T(8,128)(2,1)S(1)}, u32[]{:S(2)}, u32[]{:S(2)}) collective-permute-start(bf16[2,24,2048]{2,1,0:T(8,128)(2,1)S(1)} %collective-permute-done.1.refs_2_), channel_id=1, source_target_pairs={{0,1},{1,0},{2,3},{3,2},{4,5},{5,4},{6,7},{7,6},{8,9},{9,8},{10,11... | collective-permute-start | bytes 589832 | tf_op jit(solution)/shard_map/ppermute | solution.py:39
  36.3 12.8 %collective-permute-start.38 = (bf16[3,24,2048]{2,1,0:T(8,128)(2,1)}, bf16[3,24,2048]{2,1,0:T(8,128)(2,1)}, u32[]{:S(2)}, u32[]{:S(2)}) collective-permute-start(bf16[3,24,2048]{2,1,0:T(8,128)(2,1)} %shard_map.128.refs_3_), channel_id=1, source_target_pairs={{0,2},{1,3},{2,0},{3,1},{4,6},{5,7},{6,4},{7,5},{8,10},{9,11},{10,... | collective-permute-start | bytes 884744 | tf_op jit(solution)/shard_map/ppermute | solution.py:39
  36.9 15.0 %collective-permute-start.39 = (bf16[3,24,2048]{2,1,0:T(8,128)(2,1)}, bf16[3,24,2048]{2,1,0:T(8,128)(2,1)}, u32[]{:S(2)}, u32[]{:S(2)}) collective-permute-start(bf16[3,24,2048]{2,1,0:T(8,128)(2,1)} %shard_map.128.refs_3_), channel_id=1, source_target_pairs={{0,4},{1,5},{2,6},{3,7},{4,0},{5,1},{6,2},{7,3},{8,12},{9,13},{10,... | collective-permute-start | bytes 884744 | tf_op jit(solution)/shard_map/ppermute | solution.py:39
  37.4 7.4 %collective-permute-start.6 = (bf16[2,24,2048]{2,1,0:T(8,128)(2,1)S(1)}, bf16[2,24,2048]{2,1,0:T(8,128)(2,1)S(1)}, u32[]{:S(2)}, u32[]{:S(2)}) collective-permute-start(bf16[2,24,2048]{2,1,0:T(8,128)(2,1)S(1)} %collective-permute-done.2.refs_3_), channel_id=1, source_target_pairs={{0,1},{1,0},{2,3},{3,2},{4,5},{5,4},{6,7},{7,6},{8,9},{9,8},{10,11... | collective-permute-start | bytes 589832 | tf_op jit(solution)/shard_map/ppermute | solution.py:39
  37.4 15.6 %collective-permute-start.40 = (bf16[3,24,2048]{2,1,0:T(8,128)(2,1)}, bf16[3,24,2048]{2,1,0:T(8,128)(2,1)}, u32[]{:S(2)}, u32[]{:S(2)}) collective-permute-start(bf16[3,24,2048]{2,1,0:T(8,128)(2,1)} %shard_map.128.refs_3_), channel_id=1, source_target_pairs={{0,6},{1,7},{2,4},{3,5},{4,2},{5,3},{6,0},{7,1},{8,14},{9,15},{10,... | collective-permute-start | bytes 884744 | tf_op jit(solution)/shard_map/ppermute | solution.py:39
  40.6 24.8 %all-to-all-start = ((bf16[8,128,128]{2,1,0:T(8,128)(2,1)}), bf16[8,128,128]{2,1,0:T(8,128)(2,1)}, u32[]{:S(2)}, u32[]{:S(2)}) async-start(bf16[8,128,128]{2,1,0:T(8,128)(2,1)} %shard_map.118), calls=%async_computation | async-start | bytes 524288 | tf_op jit(solution)/shard_map/all_to_all | solution.py:702
  44.8 0.9 copy-start.4
  47.2 17.0 %collective-permute-start.7 = (bf16[128,768]{1,0:T(8,128)(2,1)}, bf16[128,768]{1,0:T(8,128)(2,1)S(1)}, u32[]{:S(2)}, u32[]{:S(2)}) collective-permute-start(bf16[128,768]{1,0:T(8,128)(2,1)} %shard_map.114.refs_8_.refs_3_), channel_id=1, source_target_pairs={{0,16},{8,24},{16,0},{24,8},{1,17},{9,25},{17,1},{25,9},{2,18},{10... | collective-permute-start | bytes 589832 | tf_op jit(solution)/shard_map/ppermute | solution.py:39
  49.1 15.1 %collective-permute-start.8 = (bf16[128,768]{1,0:T(8,128)(2,1)}, bf16[128,768]{1,0:T(8,128)(2,1)S(1)}, u32[]{:S(2)}, u32[]{:S(2)}) collective-permute-start(bf16[128,768]{1,0:T(8,128)(2,1)} %shard_map.114.refs_8_.refs_3_), channel_id=1, source_target_pairs={{0,24},{8,16},{16,8},{24,0},{1,25},{9,17},{17,9},{25,1},{2,26},{10... | collective-permute-start | bytes 589832 | tf_op jit(solution)/shard_map/ppermute | solution.py:39
  51.9 13.5 %collective-permute-start.9 = (bf16[128,768]{1,0:T(8,128)(2,1)}, bf16[128,768]{1,0:T(8,128)(2,1)S(1)}, u32[]{:S(2)}, u32[]{:S(2)}) collective-permute-start(bf16[128,768]{1,0:T(8,128)(2,1)} %shard_map.114.refs_8_.refs_3_), channel_id=1, source_target_pairs={{0,8},{8,0},{16,24},{24,16},{1,9},{9,1},{17,25},{25,17},{2,10},{10... | collective-permute-start | bytes 589832 | tf_op jit(solution)/shard_map/ppermute | solution.py:39
  55.4 72.9 %collective-permute-start.41 = (bf16[288,2048]{1,0:T(8,128)(2,1)}, bf16[288,2048]{1,0:T(8,128)(2,1)}, u32[]{:S(2)}, u32[]{:S(2)}) collective-permute-start(bf16[288,2048]{1,0:T(8,128)(2,1)} %shard_map.129.refs_5_), channel_id=1, source_target_pairs={{0,1},{1,0},{2,3},{3,2},{4,5},{5,4},{6,7},{7,6},{8,9},{9,8},{10,11... | collective-permute-start | bytes 3538952 | tf_op jit(solution)/shard_map/ppermute | solution.py:39
  65.4 16.0 %copy-start.5 = (bf16[128,768]{1,0:T(8,128)(2,1)S(1)}, bf16[128,768]{1,0:T(8,128)(2,1)}, u32[]{:S(2)}) copy-start(bf16[128,768]{1,0:T(8,128)(2,1)} %shard_map.114.refs_8_.refs_3_) | copy-start | bytes 589828
  70.4 6.0 %collective-permute-start.18 = (f32[8,768]{1,0:T(8,128)S(1)}, f32[8,768]{1,0:T(8,128)S(1)}, u32[]{:S(2)}, u32[]{:S(2)}) collective-permute-start(f32[8,768]{1,0:T(8,128)S(1)} %get-tuple-element.48.refs_0_), channel_id=1, source_target_pairs={{0,8},{8,0},{16,24},{24,16},{1,9},{9,1},{17,25},{25,17},{2,10},{10... | collective-permute-start | bytes 73736 | tf_op jit(solution)/shard_map/ppermute | solution.py:39
  73.6 5.0 %collective-permute-start.19 = (f32[8,768]{1,0:T(8,128)S(1)}, f32[8,768]{1,0:T(8,128)S(1)}, u32[]{:S(2)}, u32[]{:S(2)}) collective-permute-start(f32[8,768]{1,0:T(8,128)S(1)} %get-tuple-element.48.refs_0_), channel_id=1, source_target_pairs={{0,16},{8,24},{16,0},{24,8},{1,17},{9,25},{17,1},{25,9},{2,18},{10... | collective-permute-start | bytes 73736 | tf_op jit(solution)/shard_map/ppermute | solution.py:39
  75.0 5.6 %collective-permute-start.20 = (f32[8,768]{1,0:T(8,128)S(1)}, f32[8,768]{1,0:T(8,128)S(1)}, u32[]{:S(2)}, u32[]{:S(2)}) collective-permute-start(f32[8,768]{1,0:T(8,128)S(1)} %get-tuple-element.48.refs_0_), channel_id=1, source_target_pairs={{0,24},{8,16},{16,8},{24,0},{1,25},{9,17},{17,9},{25,1},{2,26},{10... | collective-permute-start | bytes 73736 | tf_op jit(solution)/shard_map/ppermute | solution.py:39
  81.4 18.5 %copy-start.8 = (bf16[64,768]{1,0:T(8,128)(2,1)S(1)}, bf16[64,768]{1,0:T(8,128)(2,1)}, u32[]{:S(2)}) copy-start(bf16[64,768]{1,0:T(8,128)(2,1)} %get-tuple-element.62) | copy-start | bytes 294916
  81.4 20.2 %copy-start.7 = (bf16[64,768]{1,0:T(8,128)(2,1)S(1)}, bf16[64,768]{1,0:T(8,128)(2,1)}, u32[]{:S(2)}) copy-start(bf16[64,768]{1,0:T(8,128)(2,1)} %get-tuple-element.63) | copy-start | bytes 294916
  81.4 23.7 %copy-start.6 = (bf16[64,768]{1,0:T(8,128)(2,1)S(1)}, bf16[64,768]{1,0:T(8,128)(2,1)}, u32[]{:S(2)}) copy-start(bf16[64,768]{1,0:T(8,128)(2,1)} %get-tuple-element.64) | copy-start | bytes 294916
  89.3 8.7 %collective-permute-start.21 = (bf16[64,768]{1,0:T(8,128)(2,1)}, bf16[64,768]{1,0:T(8,128)(2,1)S(1)}, u32[]{:S(2)}, u32[]{:S(2)}) collective-permute-start(bf16[64,768]{1,0:T(8,128)(2,1)} %get-tuple-element.51), channel_id=1, source_target_pairs={{0,16},{8,24},{16,0},{24,8},{1,17},{9,25},{17,1},{25,9},{2,18},{10... | collective-permute-start | bytes 294920 | tf_op jit(solution)/shard_map/ppermute | solution.py:39
  89.3 8.7 %collective-permute-start.22 = (bf16[64,768]{1,0:T(8,128)(2,1)}, bf16[64,768]{1,0:T(8,128)(2,1)S(1)}, u32[]{:S(2)}, u32[]{:S(2)}) collective-permute-start(bf16[64,768]{1,0:T(8,128)(2,1)} %get-tuple-element.52), channel_id=1, source_target_pairs={{0,24},{8,16},{16,8},{24,0},{1,25},{9,17},{17,9},{25,1},{2,26},{10... | collective-permute-start | bytes 294920 | tf_op jit(solution)/shard_map/ppermute | solution.py:39
  91.8 6.6 %collective-permute-start.23 = (bf16[64,768]{1,0:T(8,128)(2,1)}, bf16[64,768]{1,0:T(8,128)(2,1)S(1)}, u32[]{:S(2)}, u32[]{:S(2)}) collective-permute-start(bf16[64,768]{1,0:T(8,128)(2,1)} %get-tuple-element.53), channel_id=1, source_target_pairs={{0,8},{8,0},{16,24},{24,16},{1,9},{9,1},{17,25},{25,17},{2,10},{10... | collective-permute-start | bytes 294920 | tf_op jit(solution)/shard_map/ppermute | solution.py:39
  99.9 15.8 %collective-permute-start.24 = (bf16[96,2048]{1,0:T(8,128)(2,1)S(1)}, bf16[96,2048]{1,0:T(8,128)(2,1)S(1)}, u32[]{:S(2)}, u32[]{:S(2)}) collective-permute-start(bf16[96,2048]{1,0:T(8,128)(2,1)S(1)} %get-tuple-element.56), channel_id=1, source_target_pairs={{0,1},{1,0},{2,3},{3,2},{4,5},{5,4},{6,7},{7,6},{8,9},{9,8},{10,11... | collective-permute-start | bytes 1179656 | tf_op jit(solution)/shard_map/ppermute | solution.py:39
  100.0 5.2 %collective-permute-start.29 = (bf16[64,768]{1,0:T(8,128)(2,1)S(1)}, bf16[64,768]{1,0:T(8,128)(2,1)S(1)}, u32[]{:S(2)}, u32[]{:S(2)}) collective-permute-start(bf16[64,768]{1,0:T(8,128)(2,1)S(1)} %copy-done.8), channel_id=1, source_target_pairs={{0,8},{8,0},{16,24},{24,16},{1,9},{9,1},{17,25},{25,17},{2,10},{10... | collective-permute-start | bytes 294920 | tf_op jit(solution)/shard_map/ppermute | solution.py:39
  101.6 10.7 %collective-permute-start.30 = (bf16[64,768]{1,0:T(8,128)(2,1)S(1)}, bf16[64,768]{1,0:T(8,128)(2,1)S(1)}, u32[]{:S(2)}, u32[]{:S(2)}) collective-permute-start(bf16[64,768]{1,0:T(8,128)(2,1)S(1)} %copy-done.7), channel_id=1, source_target_pairs={{0,16},{8,24},{16,0},{24,8},{1,17},{9,25},{17,1},{25,9},{2,18},{10... | collective-permute-start | bytes 294920 | tf_op jit(solution)/shard_map/ppermute | solution.py:39
  105.2 7.2 %collective-permute-start.31 = (bf16[64,768]{1,0:T(8,128)(2,1)S(1)}, bf16[64,768]{1,0:T(8,128)(2,1)S(1)}, u32[]{:S(2)}, u32[]{:S(2)}) collective-permute-start(bf16[64,768]{1,0:T(8,128)(2,1)S(1)} %copy-done.6), channel_id=1, source_target_pairs={{0,24},{8,16},{16,8},{24,0},{1,25},{9,17},{17,9},{25,1},{2,26},{10... | collective-permute-start | bytes 294920 | tf_op jit(solution)/shard_map/ppermute | solution.py:39
  106.9 27.6 %all-to-all-start.1 = ((bf16[8,128,128]{2,1,0:T(8,128)(2,1)}), bf16[8,128,128]{2,1,0:T(8,128)(2,1)S(1)}, u32[]{:S(2)}, u32[]{:S(2)}) async-start(bf16[8,128,128]{2,1,0:T(8,128)(2,1)} %get-tuple-element.61), calls=%async_computation.1 | async-start | bytes 524288 | tf_op jit(solution)/shard_map/all_to_all | solution.py:719
  113.3 5.3 %collective-permute-start.32 = (bf16[64,768]{1,0:T(8,128)(2,1)S(1)}, bf16[64,768]{1,0:T(8,128)(2,1)S(1)}, u32[]{:S(2)}, u32[]{:S(2)}) collective-permute-start(bf16[64,768]{1,0:T(8,128)(2,1)S(1)} %shard_map.127.refs_0_), channel_id=1, source_target_pairs={{0,8},{8,0},{16,24},{24,16},{1,9},{9,1},{17,25},{25,17},{2,10},{10... | collective-permute-start | bytes 294920 | tf_op jit(solution)/shard_map/ppermute | solution.py:39
  115.3 9.9 %collective-permute-start.33 = (bf16[64,768]{1,0:T(8,128)(2,1)S(1)}, bf16[64,768]{1,0:T(8,128)(2,1)S(1)}, u32[]{:S(2)}, u32[]{:S(2)}) collective-permute-start(bf16[64,768]{1,0:T(8,128)(2,1)S(1)} %shard_map.127.refs_0_), channel_id=1, source_target_pairs={{0,16},{8,24},{16,0},{24,8},{1,17},{9,25},{17,1},{25,9},{2,18},{10... | collective-permute-start | bytes 294920 | tf_op jit(solution)/shard_map/ppermute | solution.py:39
  115.6 11.2 %collective-permute-start.34 = (bf16[64,768]{1,0:T(8,128)(2,1)S(1)}, bf16[64,768]{1,0:T(8,128)(2,1)S(1)}, u32[]{:S(2)}, u32[]{:S(2)}) collective-permute-start(bf16[64,768]{1,0:T(8,128)(2,1)S(1)} %shard_map.127.refs_0_), channel_id=1, source_target_pairs={{0,24},{8,16},{16,8},{24,0},{1,25},{9,17},{17,9},{25,1},{2,26},{10... | collective-permute-start | bytes 294920 | tf_op jit(solution)/shard_map/ppermute | solution.py:39
  118.6 13.8 %collective-permute-start.25 = (bf16[24,2048]{1,0:T(8,128)(2,1)}, bf16[24,2048]{1,0:T(8,128)(2,1)S(1)}, u32[]{:S(2)}, u32[]{:S(2)}) collective-permute-start(bf16[24,2048]{1,0:T(8,128)(2,1)} %get-tuple-element.57), channel_id=1, source_target_pairs={{0,2},{1,3},{2,0},{3,1},{4,6},{5,7},{6,4},{7,5},{8,10},{9,11},{10,... | collective-permute-start | bytes 294920 | tf_op jit(solution)/shard_map/ppermute | solution.py:39
  125.2 7.2 %collective-permute-start.26 = (bf16[24,2048]{1,0:T(8,128)(2,1)}, bf16[24,2048]{1,0:T(8,128)(2,1)S(1)}, u32[]{:S(2)}, u32[]{:S(2)}) collective-permute-start(bf16[24,2048]{1,0:T(8,128)(2,1)} %get-tuple-element.58), channel_id=1, source_target_pairs={{0,4},{1,5},{2,6},{3,7},{4,0},{5,1},{6,2},{7,3},{8,12},{9,13},{10,... | collective-permute-start | bytes 294920 | tf_op jit(solution)/shard_map/ppermute | solution.py:39
  126.9 5.7 %collective-permute-start.27 = (bf16[24,2048]{1,0:T(8,128)(2,1)}, bf16[24,2048]{1,0:T(8,128)(2,1)S(1)}, u32[]{:S(2)}, u32[]{:S(2)}) collective-permute-start(bf16[24,2048]{1,0:T(8,128)(2,1)} %get-tuple-element.59), channel_id=1, source_target_pairs={{0,6},{1,7},{2,4},{3,5},{4,2},{5,3},{6,0},{7,1},{8,14},{9,15},{10,... | collective-permute-start | bytes 294920 | tf_op jit(solution)/shard_map/ppermute | solution.py:39
  128.3 6.2 %copy-start = (bf16[2,4,256,512]{3,2,1,0:T(8,128)(2,1)S(1)}, bf16[2,4,256,512]{3,2,1,0:T(8,128)(2,1)}, u32[]{:S(2)}) copy-start(bf16[2,4,256,512]{3,2,1,0:T(8,128)(2,1)} %shard_map.125.held_ref) | copy-start | bytes 6291460
